TPU v7x, 512 devices: a whole 4x8x8 slice. The times are simulated.
512 devices in a mesh: dp: 4 (over x), kv: 64 (over z, y), tp: 2 (over core).
Axes of the slice: x: 4, y: 8, z: 8, core: 2. Of those that a mesh axis runs over, the one named last changes fastest.
Arguments:
- tokens: bfloat16 [512, 4096], P('dp', ('kv', 'tp')), may hold values from -6 to 6
- w_query: bfloat16 [4096, 2, 1024], P(None, 'tp', 'kv'), may hold values from -0.09375 to 0.09375
- w_forget: bfloat16 [4096, 2, 1024], P(None, 'tp', 'kv'), may hold values from -0.09375 to 0.09375
- w_input: bfloat16 [4096, 2, 1024], P(None, 'tp', 'kv'), may hold values from -0.09375 to 0.09375
- w_output_gate: bfloat16 [4096, 2, 1024], P(None, 'tp', 'kv'), may hold values from -0.09375 to 0.09375
- gate_floor: float32 [2048], P('tp'), may hold values from 0 to 0.9
- head_gain: float32 [128], replicated, may hold values from 0.1 to 1.9
- w_out: bfloat16 [2048, 4096], P(None, ('kv', 'tp')), may hold values from -0.125 to 0.125
- mix_gain: float32 [4096], replicated, may hold values from 0.1 to 1.9
- ffn_gain: float32 [4096], replicated, may hold values from 0.1 to 1.9
- w_up: bfloat16 [4096, 16384], P(None, ('kv', 'tp')), may hold values from -0.09375 to 0.09375
- w_down: bfloat16 [16384, 4096], P(('kv', 'tp')), may hold values from -0.1875 to 0.1875
- state: float32 [512, 16, 128, 128], P(('dp', 'kv'), 'tp'), may hold values from -6 to 6
Outputs:
- mixed: bfloat16 [512, 4096], P('dp', ('kv', 'tp'))
- new_state: float32 [512, 16, 128, 128], P(('dp', 'kv'), 'tp')
All inputs are finite; a program needn't handle non-finite values.
Results may differ from a plain program's by a relative error of at most 0.014.
Values may be sent and summed in bfloat16 or wider, within the bound.
No kernel may reach another device: no remote copies, remote signals or barrier semaphores. Data moves between devices by JAX's collectives and lax.ppermute only.
A program may use at most 64 MiB of HBM per device.

v0:
```python
import jax
import jax.numpy as jnp
from jax import lax
from jax.sharding import Mesh
from jax.sharding import PartitionSpec as P

KV = ("kv_0", "kv_1")
KV_TP = ("kv_0", "kv_1", "tp")
DP_KV = ("dp", "kv_0", "kv_1")


EPSILON = 1e-06


def sent_to_all(x, axis):
    devices = lax.axis_size(axis)
    return lax.all_to_all(jnp.broadcast_to(x[None], (devices, *x.shape)), axis, 0, 0, tiled=True)


def joined_along(parts, dim):
    parts = jnp.moveaxis(parts, 0, dim)
    lengths = parts.shape
    return parts.reshape(*lengths[:dim], lengths[dim] * lengths[dim + 1], *lengths[dim + 2 :])


def gathered_by_axis(x, axes, dim):
    far, near = axes
    leading = sent_to_all(x, far)
    parts = jnp.swapaxes(sent_to_all(leading, near), 0, 1)
    return joined_along(parts.reshape(-1, *x.shape), dim)


def in_blocks(x, dim, devices):
    before, after = (x.shape[:dim], x.shape[dim + 1 :])
    return jnp.moveaxis(x.reshape(*before, devices, -1, *after), dim, 0)


def sum_at_owner(x, axis, dim):
    parts = in_blocks(x, dim, lax.axis_size(axis))
    arrived = lax.all_to_all(parts, axis, split_axis=0, concat_axis=0, tiled=True)
    return arrived.astype(jnp.float32).sum(axis=0)


def rms_scale(values, gain):
    return values * lax.rsqrt(jnp.mean(values * values, axis=-1, keepdims=True) + EPSILON) * gain


def per_device(
    tokens,
    w_query,
    w_forget,
    w_input,
    w_output_gate,
    gate_floor,
    head_gain,
    w_out,
    mix_gain,
    ffn_gain,
    w_up,
    w_down,
    state,
):
    group_kv = lax.axis_size(KV)
    group_tp = lax.axis_size("tp")
    tokens_f = tokens.astype(jnp.float32)
    full_rows = gathered_by_axis(tokens, (("kv_0", "kv_1"), "tp"), 1)
    normed = rms_scale(full_rows.astype(jnp.float32), mix_gain).astype(jnp.bfloat16)

    def project(weight):
        return jnp.dot(normed, weight[:, 0, :], preferred_element_type=jnp.float32).astype(
            jnp.bfloat16
        )

    query_raw, forget_raw, input_raw, gate_raw = (
        lax.all_to_all(project(w_query), KV, split_axis=0, concat_axis=1, tiled=True),
        lax.all_to_all(project(w_forget), KV, split_axis=0, concat_axis=1, tiled=True),
        lax.all_to_all(project(w_input), KV, split_axis=0, concat_axis=1, tiled=True),
        lax.all_to_all(project(w_output_gate), KV, split_axis=0, concat_axis=1, tiled=True),
    )
    seq_local = state.shape[0]
    heads_local = state.shape[1]
    head_size = state.shape[2]
    query_vec = query_raw.astype(jnp.float32).reshape(
        seq_local, heads_local, head_size
    ) * head_size ** (-0.5)
    floor_heads = gate_floor.reshape(heads_local, head_size)
    forget_gate = floor_heads + (1.0 - floor_heads) * jax.nn.sigmoid(
        forget_raw.astype(jnp.float32).reshape(seq_local, heads_local, head_size)
    )
    input_vec = input_raw.astype(jnp.float32).reshape(seq_local, heads_local, head_size)
    gate_vec = gate_raw.astype(jnp.float32).reshape(seq_local, heads_local, head_size)
    new_state = (
        forget_gate[..., None] * state + (1.0 - forget_gate)[..., None] * input_vec[:, :, None, :]
    )
    head_out = jnp.einsum("bhk,bhkv->bhv", query_vec, new_state, precision=lax.Precision.HIGHEST)
    branch = rms_scale(head_out, head_gain) * jax.nn.silu(gate_vec)
    branch = branch.reshape(seq_local, 1, heads_local * head_size).astype(jnp.bfloat16)
    gathered = gathered_by_axis(branch, (("kv_0", "kv_1"), "tp"), 1)
    gathered = gathered.reshape(seq_local, group_kv, group_tp, heads_local * head_size)
    gathered = jnp.transpose(gathered, (1, 0, 2, 3)).reshape(
        group_kv * seq_local, group_tp * heads_local * head_size
    )
    projected = jnp.dot(gathered, w_out, preferred_element_type=jnp.float32)
    residual_one = (tokens_f + projected).astype(jnp.bfloat16)
    pieces = 1
    piece_rows = residual_one.shape[0] // pieces
    whole_rows = gathered_by_axis(residual_one, (("kv_0", "kv_1"), "tp"), 1)
    ffn_in = rms_scale(whole_rows.astype(jnp.float32), ffn_gain).astype(jnp.bfloat16)
    upward = jnp.dot(ffn_in, w_up, preferred_element_type=jnp.float32)
    hidden = jnp.square(jax.nn.relu(upward)).astype(jnp.bfloat16)
    partial_terms = jnp.dot(hidden, w_down, preferred_element_type=jnp.float32)
    share_width = partial_terms.shape[1] // (group_kv * group_tp)
    blocks = partial_terms.reshape(piece_rows, group_kv, group_tp, share_width)
    paired = sum_at_owner(blocks.astype(jnp.bfloat16), "tp", 2)
    summed = sum_at_owner(paired.astype(jnp.bfloat16), KV, 1).reshape(piece_rows, share_width)
    results = (residual_one.astype(jnp.float32) + summed).astype(jnp.bfloat16)
    return (results, new_state)


def solution(mesh):
    torus = Mesh(
        mesh.devices.reshape(mesh.shape["dp"], 8, 8, mesh.shape["tp"]), ("dp", "kv_0", "kv_1", "tp")
    )
    placed = (
        P("dp", KV_TP),
        P(None, "tp", KV),
        P(None, "tp", KV),
        P(None, "tp", KV),
        P(None, "tp", KV),
        P("tp"),
        P(),
        P(None, KV_TP),
        P(),
        P(),
        P(None, KV_TP),
        P(KV_TP, None),
        P(DP_KV, "tp", None, None),
    )
    return jax.shard_map(
        per_device,
        mesh=torus,
        in_specs=placed,
        out_specs=(P("dp", KV_TP), P(DP_KV, "tp", None, None)),
        check_vma=False,
    )
```

profile of v0, /device:TPU:4, one launch (start us, length us, event | category | flops | bytes accessed | tf_op | source)
XLA Modules:
  0.0 201.7 jit_solution(16626151907140990643)
XLA Ops:
  0.6 0.0 copy-start
  0.6 1.6 broadcast_in_dim.14
  2.3 16.6 %all-to-all-start = ((bf16[64,128,32]{1,2,0:T(8,128)(2,1)}), bf16[64,128,32]{1,2,0:T(8,128)(2,1)S(1)}, u32[]{:S(2)}, u32[]{:S(2)}) async-start(bf16[64,128,32]{1,2,0:T(8,128)(2,1)} %broadcast_in_dim.14), calls=%async_computation | async-start | bytes 1048576 | tf_op jit(solution)/shard_map/all_to_all | solution.py:17
  18.9 0.8 mul.132
  19.7 0.7 broadcast_subtract_fusion.1
  20.4 18.2 %all-to-all-done = bf16[64,128,32]{1,2,0:T(8,128)(2,1)S(1)} async-done(((bf16[64,128,32]{1,2,0:T(8,128)(2,1)}), bf16[64,128,32]{1,2,0:T(8,128)(2,1)S(1)}, u32[]{:S(2)}, u32[]{:S(2)}) %all-to-all-start) | async-done | bytes 524320 | tf_op jit(solution)/shard_map/all_to_all | solution.py:17
  38.6 0.1 broadcast_in_dim.15
  38.7 4.6 %all_to_all.92 = bf16[2,64,128,32]{2,3,1,0:T(8,128)(2,1)S(1)} all-to-all(bf16[2,64,128,32]{2,3,1,0:T(8,128)(2,1)S(1)} %broadcast_in_dim.15), channel_id=1, replica_groups=mesh['dp'=4,'kv_0'=8,'kv_1'=8,'tp'=2] {'tp'}, dimensions={0} | all-to-all | bytes 2097152 | tf_op jit(solution)/shard_map/all_to_all | solution.py:17
  43.3 0.6 fusion.2
  43.9 0.7 fusion.4
  44.6 0.0 copy-start.6
  44.6 0.2 convolution_convert_fusion.4
  44.9 0.3 convolution_convert_fusion.3
  45.1 0.0 copy-start.2
  45.2 0.7 copy.86
  45.9 5.0 %all-to-all-start.3 = ((bf16[64,2,16]{2,1,0:T(2,128)(2,1)}), bf16[64,2,16]{2,1,0:T(2,128)(2,1)S(1)}, u32[]{:S(2)}, u32[]{:S(2)}) async-start(bf16[64,2,16]{2,1,0:T(2,128)(2,1)} %bitcast.12), calls=%async_computation.3 | async-start | bytes 65536 | tf_op jit(solution)/shard_map/all_to_all | solution.py:76
  50.9 0.0 copy-done.5
  50.9 0.2 convolution_convert_fusion.2
  51.1 0.7 copy.84
  51.8 11.0 %all-to-all-done.3 = bf16[64,2,16]{2,1,0:T(2,128)(2,1)S(1)} async-done(((bf16[64,2,16]{2,1,0:T(2,128)(2,1)}), bf16[64,2,16]{2,1,0:T(2,128)(2,1)S(1)}, u32[]{:S(2)}, u32[]{:S(2)}) %all-to-all-start.3) | async-done | bytes 4128 | tf_op jit(solution)/shard_map/all_to_all | solution.py:76
  62.8 4.6 %all-to-all-start.2 = ((bf16[64,2,16]{2,1,0:T(2,128)(2,1)}), bf16[64,2,16]{2,1,0:T(2,128)(2,1)S(1)}, u32[]{:S(2)}, u32[]{:S(2)}) async-start(bf16[64,2,16]{2,1,0:T(2,128)(2,1)} %bitcast.6), calls=%async_computation.2 | async-start | bytes 65536 | tf_op jit(solution)/shard_map/all_to_all | solution.py:75
  67.4 0.2 convolution_convert_fusion.1
  67.7 0.7 copy.91
  68.4 0.7 copy.89
  69.1 10.3 %all-to-all-done.2 = bf16[64,2,16]{2,1,0:T(2,128)(2,1)S(1)} async-done(((bf16[64,2,16]{2,1,0:T(2,128)(2,1)}), bf16[64,2,16]{2,1,0:T(2,128)(2,1)S(1)}, u32[]{:S(2)}, u32[]{:S(2)}) %all-to-all-start.2) | async-done | bytes 4128 | tf_op jit(solution)/shard_map/all_to_all | solution.py:75
  79.4 4.6 %all-to-all-start.4 = ((bf16[64,2,16]{2,1,0:T(2,128)(2,1)}), bf16[64,2,16]{2,1,0:T(2,128)(2,1)S(1)}, u32[]{:S(2)}, u32[]{:S(2)}) async-start(bf16[64,2,16]{2,1,0:T(2,128)(2,1)} %bitcast.15), calls=%async_computation.4 | async-start | bytes 65536 | tf_op jit(solution)/shard_map/all_to_all | solution.py:77
  84.0 0.1 copy.87
  84.1 11.9 %all-to-all-done.4 = bf16[64,2,16]{2,1,0:T(2,128)(2,1)S(1)} async-done(((bf16[64,2,16]{2,1,0:T(2,128)(2,1)}), bf16[64,2,16]{2,1,0:T(2,128)(2,1)S(1)}, u32[]{:S(2)}, u32[]{:S(2)}) %all-to-all-start.4) | async-done | bytes 4128 | tf_op jit(solution)/shard_map/all_to_all | solution.py:77
  96.0 4.6 %all-to-all-start.5 = ((bf16[64,2,16]{2,1,0:T(2,128)(2,1)}), bf16[64,2,16]{2,1,0:T(2,128)(2,1)S(1)}, u32[]{:S(2)}, u32[]{:S(2)}) async-start(bf16[64,2,16]{2,1,0:T(2,128)(2,1)} %bitcast.20), calls=%async_computation.5 | async-start | bytes 65536 | tf_op jit(solution)/shard_map/all_to_all | solution.py:78
  100.6 0.0 copy-start.11
  100.6 0.1 reshape.197
  100.7 0.1 reshape.193
  100.8 11.7 %all-to-all-done.5 = bf16[64,2,16]{2,1,0:T(2,128)(2,1)S(1)} async-done(((bf16[64,2,16]{2,1,0:T(2,128)(2,1)}), bf16[64,2,16]{2,1,0:T(2,128)(2,1)S(1)}, u32[]{:S(2)}, u32[]{:S(2)}) %all-to-all-start.5) | async-done | bytes 4128 | tf_op jit(solution)/shard_map/all_to_all | solution.py:78
  112.6 0.1 reshape.194
  112.6 0.1 copy.88
  112.7 0.1 reshape.192
  112.8 0.0 copy-done.10
  112.8 0.6 multiply_add_fusion
  113.4 0.0 copy-start.1
  113.5 1.0 fusion.15
  114.4 0.1 multiply_reduce_fusion.1
  114.5 0.1 fusion.13
  114.6 0.1 broadcast_in_dim.16
  114.8 17.4 %all_to_all.93 = bf16[64,2,1,1024]{3,1,2,0:T(2,128)(2,1)S(1)} all-to-all(bf16[64,2,1,1024]{3,1,2,0:T(2,128)(2,1)S(1)} %broadcast_in_dim.16), channel_id=1, replica_groups=mesh['dp'=4,'kv_0'=8,'kv_1'=8,'tp'=2] {'kv_0','kv_1'}, dimensions={0} | all-to-all | bytes 524288 | tf_op jit(solution)/shard_map/all_to_all | solution.py:17
  132.2 0.3 broadcast_in_dim.18
  132.5 4.2 %all_to_all.94 = bf16[2,64,2,1,1024]{4,2,1,3,0:T(2,128)(2,1)S(1)} all-to-all(bf16[2,64,2,1,1024]{4,2,1,3,0:T(2,128)(2,1)S(1)} %broadcast_in_dim.18), channel_id=1, replica_groups=mesh['dp'=4,'kv_0'=8,'kv_1'=8,'tp'=2] {'tp'}, dimensions={0} | all-to-all | bytes 1048576 | tf_op jit(solution)/shard_map/all_to_all | solution.py:17
  136.6 0.5 copy.96
  137.2 0.1 copy.108
  137.3 0.3 fusion.7
  137.6 0.1 broadcast_in_dim.19
  137.7 23.1 %all_to_all.95 = bf16[64,128,32]{1,2,0:T(8,128)(2,1)S(1)} all-to-all(bf16[64,128,32]{1,2,0:T(8,128)(2,1)S(1)} %broadcast_in_dim.19), channel_id=1, replica_groups=mesh['dp'=4,'kv_0'=8,'kv_1'=8,'tp'=2] {'kv_0','kv_1'}, dimensions={0} | all-to-all | bytes 1048576 | tf_op jit(solution)/shard_map/all_to_all | solution.py:17
  160.8 0.1 broadcast_in_dim.20
  160.9 4.6 %all_to_all.96 = bf16[2,64,128,32]{2,3,1,0:T(8,128)(2,1)S(1)} all-to-all(bf16[2,64,128,32]{2,3,1,0:T(8,128)(2,1)S(1)} %broadcast_in_dim.20), channel_id=1, replica_groups=mesh['dp'=4,'kv_0'=8,'kv_1'=8,'tp'=2] {'tp'}, dimensions={0} | all-to-all | bytes 2097152 | tf_op jit(solution)/shard_map/all_to_all | solution.py:17
  165.5 0.6 multiply_reduce_fusion
  166.1 0.3 copy_convert_fusion
  166.4 0.9 fusion.1
  167.3 2.1 %convolution_convert_fusion = bf16[128,4096]{1,0:T(8,128)(2,1)S(1)} fusion(bf16[128,4096]{1,0:T(8,128)(2,1)S(1)} %copy-done, bf16[128,4096]{0,1:T(8,128)(2,1)S(1)} %fusion.1, bf16[4096,128]{1,0:T(8,128)(2,1)} %param.23), kind=kOutput, calls=%fused_computation | convolution fusion | flops 269008896 | bytes 4194304 | tf_op jit(solution)/shard_map/dot_general | solution.py:111
  169.3 0.7 copy.98
  170.0 0.1 copy.99
  170.1 4.6 %all_to_all.97 = bf16[2,128,64,1,32]{1,4,2,3,0:T(8,128)(2,1)S(1)} all-to-all(bf16[2,128,64,1,32]{1,4,2,3,0:T(8,128)(2,1)S(1)} %copy.99), channel_id=1, replica_groups=mesh['dp'=4,'kv_0'=8,'kv_1'=8,'tp'=2] {'tp'}, dimensions={0} | all-to-all | bytes 2097152 | tf_op jit(solution)/shard_map/all_to_all | solution.py:40
  174.7 0.5 reduce_sum.51
  175.2 25.8 %all_to_all.98 = bf16[64,128,1,1,32]{1,4,3,2,0:T(8,128)(2,1)S(1)} all-to-all(bf16[64,128,1,1,32]{1,4,3,2,0:T(8,128)(2,1)S(1)} %bitcast.95), channel_id=1, replica_groups=mesh['dp'=4,'kv_0'=8,'kv_1'=8,'tp'=2] {'kv_0','kv_1'}, dimensions={0} | all-to-all | bytes 1048576 | tf_op jit(solution)/shard_map/all_to_all | solution.py:40
  201.0 0.1 convert_reduce_fusion
  201.1 0.6 add_convert_fusion
  (29 shorter events, 0.2 us)
Async XLA Ops:
  0.6 166.6 %copy-start = (bf16[128,4096]{1,0:T(8,128)(2,1)S(1)}, bf16[128,4096]{1,0:T(8,128)(2,1)}, u32[]{:S(2)}) copy-start(bf16[128,4096]{1,0:T(8,128)(2,1)} %param.24) | copy-start | bytes 3145732
  2.3 36.3 %all-to-all-start = ((bf16[64,128,32]{1,2,0:T(8,128)(2,1)}), bf16[64,128,32]{1,2,0:T(8,128)(2,1)S(1)}, u32[]{:S(2)}, u32[]{:S(2)}) async-start(bf16[64,128,32]{1,2,0:T(8,128)(2,1)} %broadcast_in_dim.14), calls=%async_computation | async-start | bytes 1048576 | tf_op jit(solution)/shard_map/all_to_all | solution.py:17
  43.3 1.3 copy-start.3
  43.3 1.6 copy-start.4
  43.9 7.0 %copy-start.5 = (bf16[4096,1,16]{0,2,1:T(8,128)(2,1)S(1)}, bf16[4096,1,16]{0,2,1:T(8,128)(2,1)}, u32[]{:S(2)}) copy-start(bf16[4096,1,16]{0,2,1:T(8,128)(2,1)} %param.16) | copy-start | bytes 393220
  44.6 22.8 %copy-start.6 = (bf16[4096,1,16]{0,2,1:T(8,128)(2,1)S(1)}, bf16[4096,1,16]{0,2,1:T(8,128)(2,1)}, u32[]{:S(2)}) copy-start(bf16[4096,1,16]{0,2,1:T(8,128)(2,1)} %param.17) | copy-start | bytes 393220
  45.1 67.7 %copy-start.10 = (f32[1024]{0:T(1024)S(1)}, f32[1024]{0:T(1024)}, u32[]{:S(2)}) copy-start(f32[1024]{0:T(1024)} %param.18) | copy-start | bytes 12292
  45.1 67.7 %copy-start.2 = (f32[2,8,128,128]{3,2,1,0:T(8,128)S(1)}, f32[2,8,128,128]{3,2,1,0:T(8,128)}, u32[]{:S(2)}) copy-start(f32[2,8,128,128]{3,2,1,0:T(8,128)} %param.25) | copy-start | bytes 3145732
  45.9 16.9 %all-to-all-start.3 = ((bf16[64,2,16]{2,1,0:T(2,128)(2,1)}), bf16[64,2,16]{2,1,0:T(2,128)(2,1)S(1)}, u32[]{:S(2)}, u32[]{:S(2)}) async-start(bf16[64,2,16]{2,1,0:T(2,128)(2,1)} %bitcast.12), calls=%async_computation.3 | async-start | bytes 65536 | tf_op jit(solution)/shard_map/all_to_all | solution.py:76
  62.8 16.6 %all-to-all-start.2 = ((bf16[64,2,16]{2,1,0:T(2,128)(2,1)}), bf16[64,2,16]{2,1,0:T(2,128)(2,1)S(1)}, u32[]{:S(2)}, u32[]{:S(2)}) async-start(bf16[64,2,16]{2,1,0:T(2,128)(2,1)} %bitcast.6), calls=%async_computation.2 | async-start | bytes 65536 | tf_op jit(solution)/shard_map/all_to_all | solution.py:75
  79.4 16.6 %all-to-all-start.4 = ((bf16[64,2,16]{2,1,0:T(2,128)(2,1)}), bf16[64,2,16]{2,1,0:T(2,128)(2,1)S(1)}, u32[]{:S(2)}, u32[]{:S(2)}) async-start(bf16[64,2,16]{2,1,0:T(2,128)(2,1)} %bitcast.15), calls=%async_computation.4 | async-start | bytes 65536 | tf_op jit(solution)/shard_map/all_to_all | solution.py:77
  96.0 16.5 %all-to-all-start.5 = ((bf16[64,2,16]{2,1,0:T(2,128)(2,1)}), bf16[64,2,16]{2,1,0:T(2,128)(2,1)S(1)}, u32[]{:S(2)}, u32[]{:S(2)}) async-start(bf16[64,2,16]{2,1,0:T(2,128)(2,1)} %bitcast.20), calls=%async_computation.5 | async-start | bytes 65536 | tf_op jit(solution)/shard_map/all_to_all | solution.py:78
  100.6 14.0 %copy-start.11 = (f32[128]{0:T(128)S(1)}, f32[128]{0:T(128)}, u32[]{:S(2)}) copy-start(f32[128]{0:T(128)} %param.19) | copy-start | bytes 1540
  113.4 23.7 %copy-start.1 = (f32[2,8,128,128]{3,2,1,0:T(8,128)}, f32[2,8,128,128]{3,2,1,0:T(8,128)S(1)}, u32[]{:S(2)}) copy-start(f32[2,8,128,128]{3,2,1,0:T(8,128)S(1)} %multiply_add_fusion) | copy-start | bytes 3145732
  132.2 5.1 %copy-start.7 = (bf16[2048,32]{0,1:T(8,128)(2,1)S(1)}, bf16[2048,32]{0,1:T(8,128)(2,1)}, u32[]{:S(2)}) copy-start(bf16[2048,32]{0,1:T(8,128)(2,1)} %param.20) | copy-start | bytes 393220
  132.2 5.1 %copy-start.8 = (bf16[128,32]{0,1:T(8,128)(2,1)S(1)}, bf16[128,32]{0,1:T(8,128)(2,1)}, u32[]{:S(2)}) copy-start(bf16[128,32]{0,1:T(8,128)(2,1)} %param.13) | copy-start | bytes 24580
  165.5 0.9 copy-start.9
where the time goes:
time: 202 us
  blocking collectives  84.2 us (42%)
  waiting for transfers between devices  63 us (31%)
  starting transfers between devices  35.3 us (17%)
  local copies, waits for them, and re-layouts  8.09 us (4%)
  other arithmetic  5.76 us (3%)
  matrix products  4.32 us (2%)
    all_to_all x5, blocking collectives, sent_to_all(): lax.all_to_all(jnp.broadcast_to(x[None], (devices, *x.shape)), axis, 0, 0...  53.8 us
    all_to_all x2, blocking collectives, sum_at_owner(): lax.all_to_all(parts, axis, split_axis=0, concat_axis=0, tiled=True)  30.4 us
    all_to_all x1, waiting for transfers between devices, sent_to_all(): lax.all_to_all(jnp.broadcast_to(x[None], (devices, *x.shape)), axis, 0, 0...  18.2 us
    all_to_all x1, starting transfers between devices, sent_to_all(): lax.all_to_all(jnp.broadcast_to(x[None], (devices, *x.shape)), axis, 0, 0...  16.6 us
    all_to_all x1, waiting for transfers between devices, per_device(): lax.all_to_all(project(w_input), KV, split_axis=0, concat_axis=1, tiled=T...  11.9 us
    all_to_all x1, waiting for transfers between devices, per_device(): lax.all_to_all(project(w_output_gate), KV, split_axis=0, concat_axis=1, t...  11.7 us
    all_to_all x1, waiting for transfers between devices, per_device(): lax.all_to_all(project(w_forget), KV, split_axis=0, concat_axis=1, tiled=...  11 us
    all_to_all x1, waiting for transfers between devices, per_device(): lax.all_to_all(project(w_query), KV, split_axis=0, concat_axis=1, tiled=T...  10.3 us
  transfers between devices with their start and end apart: 5, of which 5 were waited for; matrix products, arithmetic and copies ran while one was open for 2% of the time, Pallas kernels for 0%

commit v1 on v0

v1 whole, which is shorter than its diff:
```python
import jax
import jax.numpy as jnp
from jax import lax
from jax.experimental import pallas as pl
from jax.experimental.pallas import tpu as pltpu
from jax.sharding import Mesh
from jax.sharding import PartitionSpec as P

KV = ("kv_0", "kv_1")
KV_TP = ("kv_0", "kv_1", "tp")
DP_KV = ("dp", "kv_0", "kv_1")


EPSILON = 1e-06


def rms_scale(values, gain):
    return values * lax.rsqrt(jnp.mean(values * values, axis=-1, keepdims=True) + EPSILON) * gain


def swapped(x):
    return lax.ppermute(x, "tp", [(0, 1), (1, 0)])


def gathered(x):
    chips = lax.axis_size(KV)
    return lax.all_to_all(jnp.broadcast_to(x[None], (chips, *x.shape)), KV, 0, 0, tiled=True)


def contracted(left, right, dims):
    return lax.dot_general(
        left, right, ((dims[:1], dims[1:]), ((), ())), preferred_element_type=jnp.float32
    )


def square_sums(x):
    values = x.astype(jnp.float32)
    return jnp.sum(values * values, axis=0, keepdims=True)


CHUNK = 256


def selection(core, share):
    source = lax.broadcasted_iota(jnp.int32, (CHUNK, CHUNK // 2), 0)
    target = lax.broadcasted_iota(jnp.int32, (CHUNK, CHUNK // 2), 1)
    wanted = (target // share) * (2 * share) + core * share + target % share
    return jnp.where(source == wanted, 1.0, 0.0).astype(jnp.bfloat16)


def split_mix_kernel(share, core_ref, query_ref, forget_ref, input_ref, gate_ref, gain_ref, mine_ref, other_ref):
    core = core_ref[0]
    for ref, index in ((mine_ref, core), (other_ref, 1 - core)):
        chosen = selection(index, share)
        for chunk in range(query_ref.shape[1] // CHUNK):
            span = pl.ds(chunk * CHUNK, CHUNK)
            block = jnp.concatenate(
                [
                    (part[:, span].astype(jnp.float32) * gain_ref[:, span]).astype(jnp.bfloat16)
                    for part in (query_ref, forget_ref, input_ref, gate_ref)
                ],
                axis=0,
            )
            ref[:, pl.ds(chunk * CHUNK // 2, CHUNK // 2)] = jnp.dot(
                block, chosen, preferred_element_type=jnp.float32
            ).astype(jnp.bfloat16)


def split_up_kernel(share, core_ref, weight_ref, gain_ref, mine_ref, other_ref):
    core = core_ref[0]
    for ref, index in ((mine_ref, core), (other_ref, 1 - core)):
        chosen = selection(index, share)
        for chunk in range(weight_ref.shape[0] // CHUNK):
            span = pl.ds(chunk * CHUNK, CHUNK)
            flipped = weight_ref[span, :].astype(jnp.float32).T * gain_ref[:, span]
            ref[:, pl.ds(chunk * CHUNK // 2, CHUNK // 2)] = jnp.dot(
                flipped.astype(jnp.bfloat16), chosen, preferred_element_type=jnp.float32
            ).astype(jnp.bfloat16)


def split_down_kernel(share, core_ref, weight_ref, mine_ref, other_ref):
    core = core_ref[0]
    for ref, index in ((mine_ref, core), (other_ref, 1 - core)):
        chosen = selection(index, share)
        for chunk in range(weight_ref.shape[1] // CHUNK):
            span = pl.ds(chunk * CHUNK, CHUNK)
            picked = jnp.dot(weight_ref[:, span], chosen, preferred_element_type=jnp.float32)
            ref[pl.ds(chunk * CHUNK // 2, CHUNK // 2), :] = picked.T.astype(jnp.bfloat16)


def split_call(kernel, share, shape, *operands):
    core = lax.axis_index("tp").astype(jnp.int32).reshape(1)
    memory = pl.BlockSpec(memory_space=pltpu.VMEM)
    return pl.pallas_call(
        lambda *refs: kernel(share, *refs),
        out_shape=[jax.ShapeDtypeStruct(shape, jnp.bfloat16)] * 2,
        in_specs=[pl.BlockSpec(memory_space=pltpu.SMEM)] + [memory] * len(operands),
        out_specs=[memory] * 2,
    )(core, *operands)


def per_device(
    tokens,
    w_query,
    w_forget,
    w_input,
    w_output_gate,
    gate_floor,
    head_gain,
    w_out,
    mix_gain,
    ffn_gain,
    w_up,
    w_down,
    state,
):
    chips = lax.axis_size(KV)
    cores = lax.axis_size("tp")
    rows, share = tokens.shape
    width = chips * cores * share
    seq_local, heads_local, head_size, _ = state.shape
    tokens_t = tokens.T
    columns = w_query.shape[2]
    hidden_local = w_up.shape[1]

    with jax.named_scope("gather_tokens"):
        token_half = gathered(tokens_t).reshape(chips * share, rows)
    with jax.named_scope("mix_weights"):
        mine, other = split_call(
            split_mix_kernel,
            share,
            (4 * columns, chips * share),
            *[w[:, 0, :].T for w in (w_query, w_forget, w_input, w_output_gate)],
            mix_gain[None, :],
        )
        lent = swapped(other)
    with jax.named_scope("project"):
        sums = square_sums(token_half)
        theirs = contracted(lent, token_half, (1, 0))
        arrived = swapped(jnp.concatenate([theirs, sums], axis=0))
        projected = contracted(mine, token_half, (1, 0)) + arrived[:-1]
        scale = lax.rsqrt((sums + arrived[-1:]) / width + EPSILON)
        raw = (projected * scale).astype(jnp.bfloat16).T
    with jax.named_scope("to_owner"):
        raw = lax.all_to_all(
            raw.reshape(chips, seq_local, 4 * columns), KV, split_axis=0, concat_axis=0, tiled=True
        )
        raw = raw.reshape(chips, seq_local, 4, columns).transpose(2, 1, 0, 3)
        raw = raw.reshape(4, seq_local, heads_local, head_size).astype(jnp.float32)

    query_vec = raw[0] * head_size ** (-0.5)
    floor_heads = gate_floor.reshape(heads_local, head_size)
    forget_gate = floor_heads + (1.0 - floor_heads) * jax.nn.sigmoid(raw[1])
    input_vec = raw[2]
    gate_vec = raw[3]
    new_state = (
        forget_gate[..., None] * state + (1.0 - forget_gate)[..., None] * input_vec[:, :, None, :]
    )
    head_out = jnp.einsum("bhk,bhkv->bhv", query_vec, new_state, precision=lax.Precision.HIGHEST)
    branch = rms_scale(head_out, head_gain) * jax.nn.silu(gate_vec)
    branch = branch.reshape(seq_local, heads_local * head_size).astype(jnp.bfloat16)

    with jax.named_scope("up_weights"):
        own_up, other = split_call(
            split_up_kernel, share, (hidden_local, chips * share), w_up, ffn_gain[None, :]
        )
        branch, own_up, lent_up = lax.optimization_barrier((branch, own_up, swapped(other)))

    with jax.named_scope("gather_branch"):
        branch_half = gathered(branch).reshape(rows, heads_local * head_size)
    with jax.named_scope("out_weights"):
        tp = lax.axis_index("tp")
        span = heads_local * head_size
        own_out = lax.dynamic_slice_in_dim(w_out, tp * span, span, 0)
        lent_out = swapped(lax.dynamic_slice_in_dim(w_out, (1 - tp) * span, span, 0))
    with jax.named_scope("out_product"):
        theirs = swapped(contracted(lent_out, branch_half, (0, 1)))
        projected = contracted(own_out, branch_half, (0, 1)) + theirs
        residual = (tokens_t.astype(jnp.float32) + projected).astype(jnp.bfloat16)

    with jax.named_scope("down_weights"):
        own_down, other = split_call(
            split_down_kernel, share, (chips * share, hidden_local), w_down
        )
        residual, own_down, lent_down = lax.optimization_barrier(
            (residual, own_down, swapped(other))
        )

    with jax.named_scope("gather_residual"):
        residual_half = gathered(residual).reshape(chips * share, rows)
    with jax.named_scope("up_product"):
        up_both = jnp.concatenate([own_up, lent_up], axis=0)
        partial = contracted(up_both, residual_half, (1, 0))
        sums = square_sums(residual_half)
        arrived = swapped(jnp.concatenate([partial, sums], axis=0))
        upward = partial + jnp.concatenate(
            [arrived[hidden_local : 2 * hidden_local], arrived[:hidden_local]], axis=0
        )
        scale = lax.rsqrt((sums + arrived[-1:]) / width + EPSILON)
        hidden = jnp.square(jax.nn.relu(upward * scale)).astype(jnp.bfloat16)

    with jax.named_scope("down_product"):
        down_both = jnp.concatenate([own_down, lent_down], axis=1)
        terms = contracted(down_both, hidden, (1, 0)).astype(jnp.bfloat16)
    with jax.named_scope("sum_terms"):
        terms = lax.all_to_all(
            terms.reshape(chips, share, rows), KV, split_axis=0, concat_axis=0, tiled=True
        )
        summed = terms.astype(jnp.float32).sum(axis=0)
        mixed = (residual.astype(jnp.float32) + summed).astype(jnp.bfloat16).T
    return (mixed, new_state)


def solution(mesh):
    torus = Mesh(
        mesh.devices.reshape(mesh.shape["dp"], 8, 8, mesh.shape["tp"]), ("dp", "kv_0", "kv_1", "tp")
    )
    placed = (
        P("dp", KV_TP),
        P(None, "tp", KV),
        P(None, "tp", KV),
        P(None, "tp", KV),
        P(None, "tp", KV),
        P("tp"),
        P(),
        P(None, KV_TP),
        P(),
        P(),
        P(None, KV_TP),
        P(KV_TP, None),
        P(DP_KV, "tp", None, None),
    )
    return jax.shard_map(
        per_device,
        mesh=torus,
        in_specs=placed,
        out_specs=(P("dp", KV_TP), P(DP_KV, "tp", None, None)),
        check_vma=False,
    )
```

time: 202 us -> 146 us (0.72)
  the two profiles are of different devices: /device:TPU:4 before, /device:TPU:2 now
where the time goes in v1:
time: 146 us
  blocking collectives  50.3 us (34%)
  starting transfers between devices  40.8 us (28%)
  waiting for transfers between devices  36.6 us (25%)
  Pallas kernels  8.05 us (6%)
  local copies, waits for them, and re-layouts  4.17 us (3%)
  matrix products  2.63 us (2%)
  other arithmetic  2.13 us (1%)
    all_to_all x1, blocking collectives, gathered(): lax.all_to_all(jnp.broadcast_to(x[None], (chips, *x.shape)), KV, 0, 0, ti...  25.4 us
    all_to_all x1, blocking collectives, per_device(): lax.all_to_all(terms.reshape(chips, share, rows), KV, split_axis=0, conca...  24.9 us
    all_to_all x2, waiting for transfers between devices, gathered(): lax.all_to_all(jnp.broadcast_to(x[None], (chips, *x.shape)), KV, 0, 0, ti...  22.4 us
    all_to_all x2, starting transfers between devices, gathered(): lax.all_to_all(jnp.broadcast_to(x[None], (chips, *x.shape)), KV, 0, 0, ti...  21.2 us
    ppermute x7, starting transfers between devices, swapped(): return lax.ppermute(x, 'tp', [(0, 1), (1, 0)])  14.7 us
    all_to_all x1, waiting for transfers between devices, per_device(): lax.all_to_all(raw.reshape(chips, seq_local, 4 * columns), KV, split_axis...  11.9 us
    pallas_call x3, Pallas kernels, split_call(): pl.pallas_call(lambda *refs: kernel(share, *refs), out_shape=[jax.ShapeDt...  8.05 us
    all_to_all x1, starting transfers between devices, per_device(): lax.all_to_all(raw.reshape(chips, seq_local, 4 * columns), KV, split_axis...  4.98 us
  transfers between devices with their start and end apart: 10, of which 5 were waited for; matrix products, arithmetic and copies ran while one was open for 3% of the time, Pallas kernels for 6%

profile of v1, /device:TPU:2, one launch (start us, length us, event | category | flops | bytes accessed | tf_op | source)
XLA Modules:
  0.0 145.7 jit_solution(9385030696090165132)
XLA Ops:
  0.6 0.0 copy-start
  0.6 1.6 %broadcast_in_dim.15 = bf16[64,32,128]{2,1,0:T(8,128)(2,1)} broadcast(bf16[32,128]{1,0:T(8,128)(2,1)} %bitcast.76), dimensions={1,2} | broadcast | bytes 532480 | tf_op jit(solution)/shard_map/gather_tokens/broadcast_in_dim | solution.py:27
  2.2 16.6 %all-to-all-start = ((bf16[64,32,128]{2,1,0:T(8,128)(2,1)}), bf16[64,32,128]{2,1,0:T(8,128)(2,1)S(1)}, u32[]{:S(2)}, u32[]{:S(2)}) async-start(bf16[64,32,128]{2,1,0:T(8,128)(2,1)} %broadcast_in_dim.15), calls=%async_computation | async-start | bytes 1048576 | tf_op jit(solution)/shard_map/gather_tokens/all_to_all | solution.py:27
  18.8 2.2 %mix_weights.1 = (bf16[64,2048]{1,0:T(8,128)(2,1)}, bf16[64,2048]{1,0:T(8,128)(2,1)}) custom-call(s32[1]{0:T(128)} %bitcast.1.refs_0_, bf16[16,4096]{1,0:T(8,128)(2,1)} %bitcast.69, bf16[16,4096]{1,0:T(8,128)(2,1)} %bitcast.70, bf16[16,4096]{1,0:T(8,128)(2,1)} %bitcast.71, bf16[16,4096]{1,0:T(8,128)(2,1)} %bitcast.72, f32[1,4096]{1,0:T(1,128)} %bitcast.79), custom_call_target="tpu_custom_call" | custom-call | tf_op jit(solution)/shard_map/mix_weights/pallas_call | solution.py:94
  21.1 1.9 %collective-permute-start = (bf16[64,2048]{1,0:T(8,128)(2,1)}, bf16[64,2048]{1,0:T(8,128)(2,1)S(1)}, u32[]{:S(2)}, u32[]{:S(2)}) collective-permute-start(bf16[64,2048]{1,0:T(8,128)(2,1)} %get-tuple-element.15), channel_id=1, source_target_pairs={{0,1},{1,0},{2,3},{3,2},{4,5},{5,4},{6,7},{7,6},{8,9},{9,8},{10,11... | collective-permute-start | bytes 786440 | tf_op jit(solution)/shard_map/mix_weights/ppermute | solution.py:22
  23.0 15.6 %all-to-all-done = bf16[64,32,128]{2,1,0:T(8,128)(2,1)S(1)} async-done(((bf16[64,32,128]{2,1,0:T(8,128)(2,1)}), bf16[64,32,128]{2,1,0:T(8,128)(2,1)S(1)}, u32[]{:S(2)}, u32[]{:S(2)}) %all-to-all-start) | async-done | bytes 524320 | tf_op jit(solution)/shard_map/gather_tokens/all_to_all | solution.py:27
  38.5 0.3 multiply_reduce_fusion.1
  38.8 0.0 collective-permute-done
  38.8 0.2 fusion.32
  39.1 0.0 copy-start.5
  39.1 1.9 %collective-permute-start.1 = (f32[65,128]{1,0:T(8,128)S(1)}, f32[65,128]{1,0:T(8,128)S(1)}, u32[]{:S(2)}, u32[]{:S(2)}) collective-permute-start(f32[65,128]{1,0:T(8,128)S(1)} %pad_maximum_fusion.1), channel_id=1, source_target_pairs={{0,1},{1,0},{2,3},{3,2},{4,5},{5,4},{6,7},{7,6},{8,9},{9,8},{10,11... | collective-permute-start | bytes 99848 | tf_op jit(solution)/shard_map/project/ppermute | solution.py:22
  41.0 3.0 %up_weights.1 = (bf16[128,2048]{1,0:T(8,128)(2,1)}, bf16[128,2048]{1,0:T(8,128)(2,1)}) custom-call(s32[1]{0:T(128)} %bitcast.1.refs_0_, bf16[4096,128]{1,0:T(8,128)(2,1)} %refs_1_.2, f32[1,4096]{1,0:T(1,128)} %bitcast.77), custom_call_target="tpu_custom_call" | custom-call | tf_op jit(solution)/shard_map/up_weights/pallas_call | solution.py:94
  44.0 2.5 %collective-permute-start.2 = (bf16[128,2048]{1,0:T(8,128)(2,1)}, bf16[128,2048]{1,0:T(8,128)(2,1)S(1)}, u32[]{:S(2)}, u32[]{:S(2)}) collective-permute-start(bf16[128,2048]{1,0:T(8,128)(2,1)} %get-tuple-element.17), channel_id=1, source_target_pairs={{0,1},{1,0},{2,3},{3,2},{4,5},{5,4},{6,7},{7,6},{8,9},{9,8},{10,11... | collective-permute-start | bytes 1572872 | tf_op jit(solution)/shard_map/up_weights/ppermute | solution.py:22
  46.6 0.0 collective-permute-done.1
  46.6 0.0 copy-done.3
  46.6 0.2 fusion.18
  46.8 0.7 copy.39
  47.5 5.0 %all-to-all-start.1 = ((bf16[64,2,64]{2,1,0:T(2,128)(2,1)}), bf16[64,2,64]{2,1,0:T(2,128)(2,1)S(1)}, u32[]{:S(2)}, u32[]{:S(2)}) async-start(bf16[64,2,64]{2,1,0:T(2,128)(2,1)} %bitcast.15), calls=%async_computation.1 | async-start | bytes 65536 | tf_op jit(solution)/shard_map/to_owner/all_to_all | solution.py:145
  52.5 0.0 copy-done.5
  52.6 11.9 %all-to-all-done.1 = bf16[64,2,64]{2,1,0:T(2,128)(2,1)S(1)} async-done(((bf16[64,2,64]{2,1,0:T(2,128)(2,1)}), bf16[64,2,64]{2,1,0:T(2,128)(2,1)S(1)}, u32[]{:S(2)}, u32[]{:S(2)}) %all-to-all-start.1) | async-done | bytes 16416 | tf_op jit(solution)/shard_map/to_owner/all_to_all | solution.py:145
  64.5 0.1 copy.41
  64.6 0.1 copy.43
  64.7 0.1 div.28
  64.8 0.1 copy.45
  64.8 0.1 squeeze.21
  64.9 0.1 copy.44
  65.0 0.1 mul.121
  65.1 0.1 copy.42
  65.2 0.1 reshape.96
  65.3 0.0 copy-done.2
  65.3 0.6 multiply_add_fusion
  65.9 0.0 copy-start.1
  65.9 0.0 copy-start.6
  65.9 1.0 fusion.33
  66.9 0.1 multiply_reduce_fusion.2
  67.0 0.0 copy-done.6
  67.0 0.1 fusion.23
  67.1 0.0 collective-permute-done.2
  67.1 0.8 broadcast_in_dim.18
  68.0 4.6 %all-to-all-start.2 = ((bf16[64,2,1024]{2,1,0:T(2,128)(2,1)}), bf16[64,2,1024]{2,1,0:T(2,128)(2,1)S(1)}, u32[]{:S(2)}, u32[]{:S(2)}) async-start(bf16[64,2,1024]{2,1,0:T(2,128)(2,1)} %broadcast_in_dim.18), calls=%async_computation.2 | async-start | bytes 524288 | tf_op jit(solution)/shard_map/gather_branch/all_to_all | solution.py:27
  72.6 0.0 copy-done
  72.6 0.0 copy-start.4
  72.6 1.9 %collective-permute-start.3 = (bf16[1024,32]{0,1:T(8,128)(2,1)S(1)}, bf16[1024,32]{0,1:T(8,128)(2,1)S(1)}, u32[]{:S(2)}, u32[]{:S(2)}) collective-permute-start(bf16[1024,32]{0,1:T(8,128)(2,1)S(1)} %constant_dynamic-slice_fusion), channel_id=1, source_target_pairs={{0,1},{1,0},{2,3},{3,2},{4,5},{5,4},{6,7},{7,6},{8,9},{9,8},{10,11... | collective-permute-start | bytes 196616 | tf_op jit(solution)/shard_map/out_weights/ppermute | solution.py:22
  74.5 2.8 %down_weights.1 = (bf16[2048,128]{1,0:T(8,128)(2,1)}, bf16[2048,128]{1,0:T(8,128)(2,1)}) custom-call(s32[1]{0:T(128)} %bitcast.1.refs_0_, bf16[128,4096]{1,0:T(8,128)(2,1)} %refs_1_.3), custom_call_target="tpu_custom_call" | custom-call | tf_op jit(solution)/shard_map/down_weights/pallas_call | solution.py:94
  77.4 2.4 %collective-permute-start.5 = (bf16[2048,128]{1,0:T(8,128)(2,1)}, bf16[2048,128]{1,0:T(8,128)(2,1)S(1)}, u32[]{:S(2)}, u32[]{:S(2)}) collective-permute-start(bf16[2048,128]{1,0:T(8,128)(2,1)} %get-tuple-element.20), channel_id=1, source_target_pairs={{0,1},{1,0},{2,3},{3,2},{4,5},{5,4},{6,7},{7,6},{8,9},{9,8},{10,11... | collective-permute-start | bytes 1572872 | tf_op jit(solution)/shard_map/down_weights/ppermute | solution.py:22
  79.8 6.9 %all-to-all-done.2 = bf16[64,2,1024]{2,1,0:T(2,128)(2,1)S(1)} async-done(((bf16[64,2,1024]{2,1,0:T(2,128)(2,1)}), bf16[64,2,1024]{2,1,0:T(2,128)(2,1)S(1)}, u32[]{:S(2)}, u32[]{:S(2)}) %all-to-all-start.2) | async-done | bytes 262176 | tf_op jit(solution)/shard_map/gather_branch/all_to_all | solution.py:27
  86.6 0.1 reshape.89
  86.7 0.0 collective-permute-done.3
  86.8 0.2 fusion.34
  86.9 2.1 %collective-permute-start.4 = (f32[32,128]{1,0:T(8,128)S(1)}, f32[32,128]{1,0:T(8,128)S(1)}, u32[]{:S(2)}, u32[]{:S(2)}) collective-permute-start(f32[32,128]{1,0:T(8,128)S(1)} %fusion.34), channel_id=1, source_target_pairs={{0,1},{1,0},{2,3},{3,2},{4,5},{5,4},{6,7},{7,6},{8,9},{9,8},{10,11... | collective-permute-start | bytes 49160 | tf_op jit(solution)/shard_map/out_product/ppermute | solution.py:22
  89.0 0.2 fusion.14
  89.2 1.0 collective-permute-done.4
  90.2 0.0 collective-permute-done.5
  90.2 0.1 broadcast_in_dim.19
  90.3 25.4 %all_to_all.25 = bf16[64,32,128]{2,1,0:T(8,128)(2,1)S(1)} all-to-all(bf16[64,32,128]{2,1,0:T(8,128)(2,1)S(1)} %broadcast_in_dim.19), channel_id=1, replica_groups=mesh['dp'=4,'kv_0'=8,'kv_1'=8,'tp'=2] {'kv_0','kv_1'}, dimensions={0} | all-to-all | bytes 1048576 | tf_op jit(solution)/shard_map/gather_residual/all_to_all | solution.py:27
  115.6 0.0 copy-done.7
  115.6 0.4 fusion.3
  116.1 0.3 multiply_reduce_fusion
  116.4 1.9 %collective-permute-start.6 = (f32[257,128]{1,0:T(8,128)S(1)}, f32[257,128]{1,0:T(8,128)S(1)}, u32[]{:S(2)}, u32[]{:S(2)}) collective-permute-start(f32[257,128]{1,0:T(8,128)S(1)} %pad_maximum_fusion), channel_id=1, source_target_pairs={{0,1},{1,0},{2,3},{3,2},{4,5},{5,4},{6,7},{7,6},{8,9},{9,8},{10,11... | collective-permute-start | bytes 394760 | tf_op jit(solution)/shard_map/up_product/ppermute | solution.py:22
  118.3 1.3 collective-permute-done.6
  119.7 0.4 convolution_convert_fusion
  120.1 24.9 %all_to_all.26 = bf16[64,32,128]{2,1,0:T(8,128)(2,1)S(1)} all-to-all(bf16[64,32,128]{2,1,0:T(8,128)(2,1)S(1)} %bitcast.67), channel_id=1, replica_groups=mesh['dp'=4,'kv_0'=8,'kv_1'=8,'tp'=2] {'kv_0','kv_1'}, dimensions={0} | all-to-all | bytes 1048576 | tf_op jit(solution)/shard_map/sum_terms/all_to_all | solution.py:206
  145.0 0.1 convert_reduce_fusion
  145.1 0.6 fusion.22
  (20 shorter events, 0.1 us)
Async XLA Ops:
  0.6 72.0 %copy-start = (bf16[2048,32]{0,1:T(8,128)(2,1)S(1)}, bf16[2048,32]{0,1:T(8,128)(2,1)}, u32[]{:S(2)}) copy-start(bf16[2048,32]{0,1:T(8,128)(2,1)} %param.20) | copy-start | bytes 393220
  2.2 36.3 %all-to-all-start = ((bf16[64,32,128]{2,1,0:T(8,128)(2,1)}), bf16[64,32,128]{2,1,0:T(8,128)(2,1)S(1)}, u32[]{:S(2)}, u32[]{:S(2)}) async-start(bf16[64,32,128]{2,1,0:T(8,128)(2,1)} %broadcast_in_dim.15), calls=%async_computation | async-start | bytes 1048576 | tf_op jit(solution)/shard_map/gather_tokens/all_to_all | solution.py:27
  21.1 17.8 %collective-permute-start = (bf16[64,2048]{1,0:T(8,128)(2,1)}, bf16[64,2048]{1,0:T(8,128)(2,1)S(1)}, u32[]{:S(2)}, u32[]{:S(2)}) collective-permute-start(bf16[64,2048]{1,0:T(8,128)(2,1)} %get-tuple-element.15), channel_id=1, source_target_pairs={{0,1},{1,0},{2,3},{3,2},{4,5},{5,4},{6,7},{7,6},{8,9},{9,8},{10,11... | collective-permute-start | bytes 786440 | tf_op jit(solution)/shard_map/mix_weights/ppermute | solution.py:22
  38.8 7.7 %copy-start.3 = (bf16[64,2048]{1,0:T(8,128)(2,1)S(1)}, bf16[64,2048]{1,0:T(8,128)(2,1)}, u32[]{:S(2)}) copy-start(bf16[64,2048]{1,0:T(8,128)(2,1)} %get-tuple-element.14) | copy-start | bytes 786436
  39.1 13.5 %copy-start.5 = (f32[1024]{0:T(1024)S(1)}, f32[1024]{0:T(1024)}, u32[]{:S(2)}) copy-start(f32[1024]{0:T(1024)} %param.18) | copy-start | bytes 12292
  39.1 7.5 %collective-permute-start.1 = (f32[65,128]{1,0:T(8,128)S(1)}, f32[65,128]{1,0:T(8,128)S(1)}, u32[]{:S(2)}, u32[]{:S(2)}) collective-permute-start(f32[65,128]{1,0:T(8,128)S(1)} %pad_maximum_fusion.1), channel_id=1, source_target_pairs={{0,1},{1,0},{2,3},{3,2},{4,5},{5,4},{6,7},{7,6},{8,9},{9,8},{10,11... | collective-permute-start | bytes 99848 | tf_op jit(solution)/shard_map/project/ppermute | solution.py:22
  44.0 21.3 %copy-start.2 = (f32[2,8,128,128]{3,2,1,0:T(8,128)S(1)}, f32[2,8,128,128]{3,2,1,0:T(8,128)}, u32[]{:S(2)}) copy-start(f32[2,8,128,128]{3,2,1,0:T(8,128)} %param.25) | copy-start | bytes 3145732
  44.0 23.1 %collective-permute-start.2 = (bf16[128,2048]{1,0:T(8,128)(2,1)}, bf16[128,2048]{1,0:T(8,128)(2,1)S(1)}, u32[]{:S(2)}, u32[]{:S(2)}) collective-permute-start(bf16[128,2048]{1,0:T(8,128)(2,1)} %get-tuple-element.17), channel_id=1, source_target_pairs={{0,1},{1,0},{2,3},{3,2},{4,5},{5,4},{6,7},{7,6},{8,9},{9,8},{10,11... | collective-permute-start | bytes 1572872 | tf_op jit(solution)/shard_map/up_weights/ppermute | solution.py:22
  47.5 16.9 %all-to-all-start.1 = ((bf16[64,2,64]{2,1,0:T(2,128)(2,1)}), bf16[64,2,64]{2,1,0:T(2,128)(2,1)S(1)}, u32[]{:S(2)}, u32[]{:S(2)}) async-start(bf16[64,2,64]{2,1,0:T(2,128)(2,1)} %bitcast.15), calls=%async_computation.1 | async-start | bytes 65536 | tf_op jit(solution)/shard_map/to_owner/all_to_all | solution.py:145
  65.9 11.5 %copy-start.1 = (f32[2,8,128,128]{3,2,1,0:T(8,128)}, f32[2,8,128,128]{3,2,1,0:T(8,128)S(1)}, u32[]{:S(2)}) copy-start(f32[2,8,128,128]{3,2,1,0:T(8,128)S(1)} %multiply_add_fusion) | copy-start | bytes 3145732
  65.9 1.1 copy-start.6
  68.0 18.7 %all-to-all-start.2 = ((bf16[64,2,1024]{2,1,0:T(2,128)(2,1)}), bf16[64,2,1024]{2,1,0:T(2,128)(2,1)S(1)}, u32[]{:S(2)}, u32[]{:S(2)}) async-start(bf16[64,2,1024]{2,1,0:T(2,128)(2,1)} %broadcast_in_dim.18), calls=%async_computation.2 | async-start | bytes 524288 | tf_op jit(solution)/shard_map/gather_branch/all_to_all | solution.py:27
  72.6 17.5 %copy-start.4 = (bf16[128,32]{0,1:T(8,128)(2,1)S(1)}, bf16[128,32]{0,1:T(8,128)(2,1)}, u32[]{:S(2)}) copy-start(bf16[128,32]{0,1:T(8,128)(2,1)} %param.13) | copy-start | bytes 24580
  72.6 14.1 %collective-permute-start.3 = (bf16[1024,32]{0,1:T(8,128)(2,1)S(1)}, bf16[1024,32]{0,1:T(8,128)(2,1)S(1)}, u32[]{:S(2)}, u32[]{:S(2)}) collective-permute-start(bf16[1024,32]{0,1:T(8,128)(2,1)S(1)} %constant_dynamic-slice_fusion), channel_id=1, source_target_pairs={{0,1},{1,0},{2,3},{3,2},{4,5},{5,4},{6,7},{7,6},{8,9},{9,8},{10,11... | collective-permute-start | bytes 196616 | tf_op jit(solution)/shard_map/out_weights/ppermute | solution.py:22
  77.4 12.8 %collective-permute-start.5 = (bf16[2048,128]{1,0:T(8,128)(2,1)}, bf16[2048,128]{1,0:T(8,128)(2,1)S(1)}, u32[]{:S(2)}, u32[]{:S(2)}) collective-permute-start(bf16[2048,128]{1,0:T(8,128)(2,1)} %get-tuple-element.20), channel_id=1, source_target_pairs={{0,1},{1,0},{2,3},{3,2},{4,5},{5,4},{6,7},{7,6},{8,9},{9,8},{10,11... | collective-permute-start | bytes 1572872 | tf_op jit(solution)/shard_map/down_weights/ppermute | solution.py:22
  86.9 28.7 %copy-start.7 = (bf16[128,2048]{1,0:T(8,128)(2,1)S(1)}, bf16[128,2048]{1,0:T(8,128)(2,1)}, u32[]{:S(2)}) copy-start(bf16[128,2048]{1,0:T(8,128)(2,1)} %get-tuple-element.24) | copy-start | bytes 1572868
  86.9 3.2 %collective-permute-start.4 = (f32[32,128]{1,0:T(8,128)S(1)}, f32[32,128]{1,0:T(8,128)S(1)}, u32[]{:S(2)}, u32[]{:S(2)}) collective-permute-start(f32[32,128]{1,0:T(8,128)S(1)} %fusion.34), channel_id=1, source_target_pairs={{0,1},{1,0},{2,3},{3,2},{4,5},{5,4},{6,7},{7,6},{8,9},{9,8},{10,11... | collective-permute-start | bytes 49160 | tf_op jit(solution)/shard_map/out_product/ppermute | solution.py:22
  116.1 3.6 %copy-start.8 = (bf16[2048,128]{1,0:T(8,128)(2,1)S(1)}, bf16[2048,128]{1,0:T(8,128)(2,1)}, u32[]{:S(2)}) copy-start(bf16[2048,128]{1,0:T(8,128)(2,1)} %get-tuple-element.22) | copy-start | bytes 1572868
  116.4 3.2 %collective-permute-start.6 = (f32[257,128]{1,0:T(8,128)S(1)}, f32[257,128]{1,0:T(8,128)S(1)}, u32[]{:S(2)}, u32[]{:S(2)}) collective-permute-start(f32[257,128]{1,0:T(8,128)S(1)} %pad_maximum_fusion), channel_id=1, source_target_pairs={{0,1},{1,0},{2,3},{3,2},{4,5},{5,4},{6,7},{7,6},{8,9},{9,8},{10,11... | collective-permute-start | bytes 394760 | tf_op jit(solution)/shard_map/up_product/ppermute | solution.py:22

commit v2 on v1

v2 whole, which is shorter than its diff:
```python
import jax
import jax.numpy as jnp
from jax import lax
from jax.experimental import pallas as pl
from jax.experimental.pallas import tpu as pltpu
from jax.sharding import Mesh
from jax.sharding import PartitionSpec as P


FAR = "kv_a"
QUAD = "kv_b"
NEAR = "kv_1"
KV = (FAR, QUAD, NEAR)
KV_TP = (*KV, "tp")
DP_KV = ("dp", *KV)


EPSILON = 1e-06


def rms_scale(values, gain):
    return values * lax.rsqrt(jnp.mean(values * values, axis=-1, keepdims=True) + EPSILON) * gain


def swapped(x):
    return lax.ppermute(x, "tp", [(0, 1), (1, 0)])


def crossed(x, bit):
    return lax.ppermute(x, QUAD, [(b, b ^ bit) for b in range(lax.axis_size(QUAD))])


def gathered(x, axes=KV):
    devices = lax.axis_size(axes)
    return lax.all_to_all(jnp.broadcast_to(x[None], (devices, *x.shape)), axes, 0, 0, tiled=True)


def contracted(left, right, dims):
    return lax.dot_general(
        left, right, ((dims[:1], dims[1:]), ((), ())), preferred_element_type=jnp.float32
    )


def square_sums(x):
    values = x.astype(jnp.float32)
    return jnp.sum(values * values, axis=0, keepdims=True)


CHUNK = 256


def selection(core, share):
    source = lax.broadcasted_iota(jnp.int32, (CHUNK, CHUNK // 2), 0)
    target = lax.broadcasted_iota(jnp.int32, (CHUNK, CHUNK // 2), 1)
    wanted = (target // share) * (2 * share) + core * share + target % share
    return jnp.where(source == wanted, 1.0, 0.0).astype(jnp.bfloat16)


def split_mix_kernel(share, core_ref, query_ref, forget_ref, input_ref, gate_ref, gain_ref, mine_ref, other_ref):
    core = core_ref[0]
    for ref, index in ((mine_ref, core), (other_ref, 1 - core)):
        chosen = selection(index, share)
        for chunk in range(query_ref.shape[1] // CHUNK):
            span = pl.ds(chunk * CHUNK, CHUNK)
            block = jnp.concatenate(
                [
                    (part[:, span].astype(jnp.float32) * gain_ref[:, span]).astype(jnp.bfloat16)
                    for part in (query_ref, forget_ref, input_ref, gate_ref)
                ],
                axis=0,
            )
            ref[:, pl.ds(chunk * CHUNK // 2, CHUNK // 2)] = jnp.dot(
                block, chosen, preferred_element_type=jnp.float32
            ).astype(jnp.bfloat16)


def split_up_kernel(
    share, far, quad, near, core_ref, weight_ref, mine_gain_ref, other_gain_ref, mine_ref, other_ref
):
    core = core_ref[0]
    group = quad * share
    sides = ((mine_ref, mine_gain_ref, core), (other_ref, other_gain_ref, 1 - core))
    for ref, gain_ref, index in sides:
        offset = pl.multiple_of(index * share, share)
        for a in range(far):
            for y in range(near):
                chips = [(a * quad + b) * near + y for b in range(quad)]
                rows = [pl.ds(chip * 2 * share + offset, share) for chip in chips]
                block = jnp.concatenate([weight_ref[span, :] for span in rows], axis=0)
                lanes = pl.ds((a * near + y) * group, group)
                scaled = block.astype(jnp.float32).T * gain_ref[:, lanes]
                ref[:, lanes] = scaled.astype(jnp.bfloat16)


def split_down_kernel(share, core_ref, weight_ref, mine_ref, other_ref):
    core = core_ref[0]
    for ref, index in ((mine_ref, core), (other_ref, 1 - core)):
        chosen = selection(index, share)
        for chunk in range(weight_ref.shape[1] // CHUNK):
            span = pl.ds(chunk * CHUNK, CHUNK)
            picked = jnp.dot(weight_ref[:, span], chosen, preferred_element_type=jnp.float32)
            ref[pl.ds(chunk * CHUNK // 2, CHUNK // 2), :] = picked.T.astype(jnp.bfloat16)


def split_call(kernel, sizes, shape, *operands):
    core = lax.axis_index("tp").astype(jnp.int32).reshape(1)
    memory = pl.BlockSpec(memory_space=pltpu.VMEM)
    return pl.pallas_call(
        lambda *refs: kernel(*sizes, *refs),
        out_shape=[jax.ShapeDtypeStruct(shape, jnp.bfloat16)] * 2,
        in_specs=[pl.BlockSpec(memory_space=pltpu.SMEM)] + [memory] * len(operands),
        out_specs=[memory] * 2,
    )(core, *operands)


def per_device(
    tokens,
    w_query,
    w_forget,
    w_input,
    w_output_gate,
    gate_floor,
    head_gain,
    w_out,
    mix_gain,
    ffn_gain,
    w_up,
    w_down,
    state,
):
    chips = lax.axis_size(KV)
    cores = lax.axis_size("tp")
    far = lax.axis_size(FAR)
    quad = lax.axis_size(QUAD)
    near = lax.axis_size(NEAR)
    rows, share = tokens.shape
    width = chips * cores * share
    seq_local, heads_local, head_size, _ = state.shape
    tokens_t = tokens.T
    columns = w_query.shape[2]
    hidden_local = w_up.shape[1]
    half = chips * share
    a = lax.axis_index(FAR)
    b = lax.axis_index(QUAD)
    y = lax.axis_index(NEAR)
    tp = lax.axis_index("tp")

    token_parts = gathered(tokens_t)
    token_half = token_parts.reshape(half, rows)
    mine, other = split_call(
        split_mix_kernel,
        (share,),
        (4 * columns, half),
        *[w[:, 0, :].T for w in (w_query, w_forget, w_input, w_output_gate)],
        mix_gain[None, :],
    )
    lent = swapped(other)
    pair = jnp.stack([w_out.T, crossed(w_out.T, 2)])
    pair = jnp.where(b & 2 == 2, pair[::-1], pair)
    four = jnp.stack([pair, crossed(pair, 1)], axis=1)
    four = jnp.where(b & 1 == 1, four[:, ::-1], four)
    out_columns = four.reshape(quad * share, cores * heads_local * head_size)
    mine, lent, out_columns = lax.optimization_barrier((mine, lent, out_columns))
    sums = square_sums(token_half)
    theirs = contracted(lent, token_half, (1, 0))
    arrived = swapped(jnp.concatenate([theirs, sums], axis=0))
    projected = contracted(mine, token_half, (1, 0)) + arrived[:-1]
    scale = lax.rsqrt((sums + arrived[-1:]) / width + EPSILON)
    raw = (projected * scale).astype(jnp.bfloat16).T
    raw, w_up, ffn_gain, token_parts = lax.optimization_barrier((raw, w_up, ffn_gain, token_parts))
    raw = lax.all_to_all(
        raw.reshape(chips, seq_local, 4 * columns), KV, split_axis=0, concat_axis=0, tiled=True
    )
    raw = raw.reshape(chips, seq_local, 4, columns).transpose(2, 1, 0, 3)
    raw = raw.reshape(4, seq_local, heads_local, head_size).astype(jnp.float32)
    gains = ffn_gain.reshape(far, quad, near, cores, share).transpose(3, 0, 2, 1, 4)
    gains = gains.reshape(cores, 1, half)
    gains = [lax.dynamic_index_in_dim(gains, core, 0, keepdims=False) for core in (tp, 1 - tp)]
    own_up, other = split_call(
        split_up_kernel, (share, far, quad, near), (hidden_local, half), w_up, *gains
    )
    lent_up = swapped(other)
    parts = token_parts.reshape(far, quad, near, share, far, quad, near * seq_local)
    parts = lax.dynamic_slice(
        parts,
        (a, 0, y, 0, 0, b, 0),
        (1, quad, 1, share, far, 1, near * seq_local),
    )
    block = parts.reshape(quad * share, far * near * seq_local).T.astype(jnp.float32)

    query_vec = raw[0] * head_size ** (-0.5)
    floor_heads = gate_floor.reshape(heads_local, head_size)
    forget_gate = floor_heads + (1.0 - floor_heads) * jax.nn.sigmoid(raw[1])
    input_vec = raw[2]
    gate_vec = raw[3]
    new_state = (
        forget_gate[..., None] * state + (1.0 - forget_gate)[..., None] * input_vec[:, :, None, :]
    )
    head_out = jnp.einsum("bhk,bhkv->bhv", query_vec, new_state, precision=lax.Precision.HIGHEST)
    branch = rms_scale(head_out, head_gain) * jax.nn.silu(gate_vec)
    branch = branch.reshape(seq_local, heads_local * head_size).astype(jnp.bfloat16)
    branch, own_up, lent_up, block, w_down = lax.optimization_barrier(
        (branch, own_up, lent_up, block, w_down)
    )

    branch = gathered(branch, (FAR, NEAR, "tp"))
    branch = branch.reshape(far * near, cores, seq_local, heads_local * head_size)
    branch = branch.transpose(0, 2, 1, 3).reshape(far * near * seq_local, -1)
    own_down, other = split_call(split_down_kernel, (share,), (half, hidden_local), w_down)
    lent_down = swapped(other)
    residual = (block + contracted(branch, out_columns, (1, 1))).astype(jnp.bfloat16)
    residual, own_down, lent_down = lax.optimization_barrier((residual, own_down, lent_down))

    parts = gathered(residual).reshape(
        far, quad, near, far, near * seq_local, quad * share
    )
    residual_half = parts.transpose(3, 1, 4, 0, 2, 5).reshape(rows, half)
    up_both = jnp.concatenate([own_up, lent_up], axis=0)
    partial = contracted(up_both, residual_half, (1, 1))
    values = residual_half.astype(jnp.float32)
    sums = jnp.sum(values * values, axis=1)[None, :]
    arrived = swapped(jnp.concatenate([partial, sums], axis=0))
    upward = partial + jnp.concatenate(
        [arrived[hidden_local : 2 * hidden_local], arrived[:hidden_local]], axis=0
    )
    scale = lax.rsqrt((sums + arrived[-1:]) / width + EPSILON)
    hidden = jnp.square(jax.nn.relu(upward * scale)).astype(jnp.bfloat16)

    down_both = jnp.concatenate([own_down, lent_down], axis=1)
    terms = contracted(down_both, hidden, (1, 0)).astype(jnp.bfloat16)
    terms = lax.all_to_all(
        terms.reshape(chips, share, rows), KV, split_axis=0, concat_axis=0, tiled=True
    )
    own = lax.dynamic_slice(residual_half, (0, ((a * near + y) * quad + b) * share), (rows, share))
    summed = terms.astype(jnp.float32).sum(axis=0)
    mixed = (own.astype(jnp.float32).T + summed).astype(jnp.bfloat16).T
    return (mixed, new_state)


def solution(mesh):
    torus = Mesh(
        mesh.devices.reshape(mesh.shape["dp"], 2, 4, 8, mesh.shape["tp"]), ("dp", *KV_TP)
    )
    placed = (
        P("dp", KV_TP),
        P(None, "tp", KV),
        P(None, "tp", KV),
        P(None, "tp", KV),
        P(None, "tp", KV),
        P("tp"),
        P(),
        P(None, KV_TP),
        P(),
        P(),
        P(None, KV_TP),
        P(KV_TP, None),
        P(DP_KV, "tp", None, None),
    )

    return jax.shard_map(
        per_device,
        mesh=torus,
        in_specs=placed,
        out_specs=(P("dp", KV_TP), P(DP_KV, "tp", None, None)),
        check_vma=False,
    )
```

time: 146 us -> 163 us (1.12)
  the two profiles are of different devices: /device:TPU:2 before, /device:TPU:4 now
where the time goes in v2:
time: 163 us; the launch traced here: 162 us
  waiting for transfers between devices  59.6 us (37%)
  starting transfers between devices  54.2 us (33%)
  blocking collectives  24.6 us (15%)
  Pallas kernels  7.57 us (5%)
  local copies, waits for them, and re-layouts  6.75 us (4%)
  matrix products  4.42 us (3%)
  other arithmetic  3.56 us (2%)
    all_to_all x1, blocking collectives, gathered(): lax.all_to_all(jnp.broadcast_to(x[None], (devices, *x.shape)), axes, 0, 0...  24.6 us
    all_to_all x1, waiting for transfers between devices, per_device(): lax.all_to_all(terms.reshape(chips, share, rows), KV, split_axis=0, conca...  19.6 us
    all_to_all x2, starting transfers between devices, gathered(): lax.all_to_all(jnp.broadcast_to(x[None], (devices, *x.shape)), axes, 0, 0...  18.6 us
    ppermute x2, waiting for transfers between devices, crossed(): lax.ppermute(x, QUAD, [(b, b ^ bit) for b in range(lax.axis_size(QUAD))])  16.4 us
    all_to_all x1, waiting for transfers between devices, per_device(): lax.all_to_all(raw.reshape(chips, seq_local, 4 * columns), KV, split_axis...  11.8 us
    all_to_all x1, starting transfers between devices, per_device(): lax.all_to_all(raw.reshape(chips, seq_local, 4 * columns), KV, split_axis...  10.6 us
    ppermute x5, starting transfers between devices, swapped(): return lax.ppermute(x, 'tp', [(0, 1), (1, 0)])  9.93 us
    ppermute x2, starting transfers between devices, crossed(): lax.ppermute(x, QUAD, [(b, b ^ bit) for b in range(lax.axis_size(QUAD))])  9.83 us
  transfers between devices with their start and end apart: 11, of which 6 were waited for; matrix products, arithmetic and copies ran while one was open for 5% of the time, Pallas kernels for 3%

profile of v2, /device:TPU:4, one launch (start us, length us, event | category | flops | bytes accessed | tf_op | source)
XLA Modules:
  0.0 161.8 jit_solution(1387129631362658740)
XLA Ops:
  0.6 6.2 %collective-permute-start.1 = (bf16[32,2048]{1,0:T(8,128)(2,1)}, bf16[32,2048]{1,0:T(8,128)(2,1)S(1)}, u32[]{:S(2)}, u32[]{:S(2)}) collective-permute-start(bf16[32,2048]{1,0:T(8,128)(2,1)} %bitcast.106), channel_id=1, source_target_pairs={{0,32},{16,48},{32,0},{48,16},{1,33},{17,49},{33,1},{49,17},{2,34}... | collective-permute-start | bytes 393224 | tf_op jit(solution)/shard_map/ppermute | solution.py:30
  6.9 2.2 %shard_map.140 = (bf16[64,2048]{1,0:T(8,128)(2,1)}, bf16[64,2048]{1,0:T(8,128)(2,1)}) custom-call(s32[1]{0:T(128)} %bitcast.refs_0_, bf16[16,4096]{1,0:T(8,128)(2,1)} %bitcast.102, bf16[16,4096]{1,0:T(8,128)(2,1)} %bitcast.103, bf16[16,4096]{1,0:T(8,128)(2,1)} %bitcast.104, bf16[16,4096]{1,0:T(8,128)(2,1)} %bitcast.105, f32[1,4096]{1,0:T(1,128)} %bitcast.113), custom_call_target="tpu_custom_call" | custom-call | tf_op jit(solution)/shard_map/pallas_call | solution.py:108
  9.1 1.9 %collective-permute-start = (bf16[64,2048]{1,0:T(8,128)(2,1)}, bf16[64,2048]{1,0:T(8,128)(2,1)S(1)}, u32[]{:S(2)}, u32[]{:S(2)}) collective-permute-start(bf16[64,2048]{1,0:T(8,128)(2,1)} %get-tuple-element.24), channel_id=1, source_target_pairs={{0,1},{1,0},{2,3},{3,2},{4,5},{5,4},{6,7},{7,6},{8,9},{9,8},{10,11... | collective-permute-start | bytes 786440 | tf_op jit(solution)/shard_map/ppermute | solution.py:26
  11.0 1.6 broadcast_in_dim.13
  12.6 14.8 %all-to-all-start = ((bf16[64,32,128]{2,1,0:T(8,128)(2,1)}), bf16[64,32,128]{2,1,0:T(8,128)(2,1)S(1)}, u32[]{:S(2)}, u32[]{:S(2)}) async-start(bf16[64,32,128]{2,1,0:T(8,128)(2,1)} %broadcast_in_dim.13), calls=%async_computation | async-start | bytes 1048576 | tf_op jit(solution)/shard_map/all_to_all | solution.py:35
  27.4 0.0 collective-permute-done.1
  27.5 0.0 copy-start.4
  27.5 3.6 %collective-permute-start.2 = (bf16[2,32,2048]{2,1,0:T(8,128)(2,1)S(1)}, bf16[2,32,2048]{2,1,0:T(8,128)(2,1)S(1)}, u32[]{:S(2)}, u32[]{:S(2)}) collective-permute-start(bf16[2,32,2048]{2,1,0:T(8,128)(2,1)S(1)} %reverse_select_fusion.1), channel_id=1, source_target_pairs={{0,16},{16,0},{32,48},{48,32},{1,17},{17,1},{33,49},{49,33},{2,18}... | collective-permute-start | bytes 786440 | tf_op jit(solution)/shard_map/ppermute | solution.py:30
  31.2 16.4 %collective-permute-done.2 = bf16[2,32,2048]{2,1,0:T(8,128)(2,1)S(1)} collective-permute-done((bf16[2,32,2048]{2,1,0:T(8,128)(2,1)S(1)}, bf16[2,32,2048]{2,1,0:T(8,128)(2,1)S(1)}, u32[]{:S(2)}, u32[]{:S(2)}) %collective-permute-start.2) | collective-permute-done | bytes 262176 | tf_op jit(solution)/shard_map/ppermute | solution.py:30
  47.6 0.1 pad_maximum_fusion
  47.7 0.1 reverse_select_fusion
  47.8 0.2 fusion.29
  48.0 0.3 multiply_reduce_fusion.1
  48.3 2.0 %collective-permute-start.3 = (f32[65,128]{1,0:T(8,128)S(1)}, f32[65,128]{1,0:T(8,128)S(1)}, u32[]{:S(2)}, u32[]{:S(2)}) collective-permute-start(f32[65,128]{1,0:T(8,128)S(1)} %pad_maximum_fusion.3), channel_id=1, source_target_pairs={{0,1},{1,0},{2,3},{3,2},{4,5},{5,4},{6,7},{7,6},{8,9},{9,8},{10,11... | collective-permute-start | bytes 99848 | tf_op jit(solution)/shard_map/ppermute | solution.py:26
  50.3 1.1 collective-permute-done.3
  51.4 0.2 fusion.2
  51.7 0.1 reshape.113
  51.8 0.1 reshape.114
  51.9 0.6 dynamic-slice_bitcast_fusion
  52.6 2.5 %shard_map.141 = (bf16[128,2048]{1,0:T(8,128)(2,1)}, bf16[128,2048]{1,0:T(8,128)(2,1)}) custom-call(s32[1]{0:T(128)} %bitcast.refs_0_, bf16[4096,128]{1,0:T(8,128)(2,1)} %refs_1_, f32[1,2048]{1,0:T(1,128)} %get-tuple-element.57.refs_2_, f32[1,2048]{1,0:T(1,128)} %get-tuple-element.56.refs_3_), custom_call_target="tpu_custom_call" | custom-call | tf_op jit(solution)/shard_map/pallas_call | solution.py:108
  55.1 2.1 %collective-permute-start.4 = (bf16[128,2048]{1,0:T(8,128)(2,1)}, bf16[128,2048]{1,0:T(8,128)(2,1)}, u32[]{:S(2)}, u32[]{:S(2)}) collective-permute-start(bf16[128,2048]{1,0:T(8,128)(2,1)} %get-tuple-element.31), channel_id=1, source_target_pairs={{0,1},{1,0},{2,3},{3,2},{4,5},{5,4},{6,7},{7,6},{8,9},{9,8},{10,11... | collective-permute-start | bytes 1572872 | tf_op jit(solution)/shard_map/ppermute | solution.py:26
  57.1 1.0 copy.76
  58.2 0.7 copy.68
  58.9 10.6 %all-to-all-start.1 = ((bf16[64,2,64]{2,1,0:T(2,128)(2,1)}), bf16[64,2,64]{2,1,0:T(2,128)(2,1)S(1)}, u32[]{:S(2)}, u32[]{:S(2)}) async-start(bf16[64,2,64]{2,1,0:T(2,128)(2,1)} %bitcast.22), calls=%async_computation.1 | async-start | bytes 65536 | tf_op jit(solution)/shard_map/all_to_all | solution.py:171
  69.6 0.1 reshape.125
  69.7 0.0 copy-start.5
  69.7 11.8 %all-to-all-done.1 = bf16[64,2,64]{2,1,0:T(2,128)(2,1)S(1)} async-done(((bf16[64,2,64]{2,1,0:T(2,128)(2,1)}), bf16[64,2,64]{2,1,0:T(2,128)(2,1)S(1)}, u32[]{:S(2)}, u32[]{:S(2)}) %all-to-all-start.1) | async-done | bytes 16416 | tf_op jit(solution)/shard_map/all_to_all | solution.py:171
  81.4 0.1 copy.70
  81.5 0.1 copy.72
  81.6 0.1 div.28
  81.7 0.1 copy.73
  81.8 0.1 mul.123
  81.9 0.1 copy.71
  82.0 0.1 reshape.126
  82.1 0.1 copy.74
  82.1 0.1 squeeze.28
  82.2 1.8 %multiply_add_fusion = f32[2,8,128,128]{3,2,1,0:T(8,128)S(1)} fusion(f32[2,8,128,128]{3,2,1,0:T(8,128)} %param.25, f32[2,8,128]{2,1,0:T(8,128)S(1)} %mul.123, f32[2,8,128]{2,1,0:T(8,128)S(1)} %get-tuple-element.48, f32[2,8,128]{2,1,0:T(8,128)S(1)} %get-tuple-element.49), kind=kLoop, calls=%fused_computation.14 | loop fusion | flops 786432 | bytes 2121728 | tf_op jit(solution)/shard_map/add | solution.py:197
  84.1 0.0 copy-start
  84.1 1.0 fusion.30
  85.1 0.1 multiply_reduce_fusion.2
  85.2 0.1 fusion.21
  85.3 0.7 broadcast_in_dim.15
  86.0 3.8 %all-to-all-start.2 = ((bf16[32,2,1024]{2,1,0:T(2,128)(2,1)}), bf16[32,2,1024]{2,1,0:T(2,128)(2,1)S(1)}, u32[]{:S(2)}, u32[]{:S(2)}) async-start(bf16[32,2,1024]{2,1,0:T(2,128)(2,1)} %broadcast_in_dim.15), calls=%async_computation.2 | async-start | bytes 262144 | tf_op jit(solution)/shard_map/all_to_all | solution.py:35
  89.8 2.8 %shard_map.142 = (bf16[2048,128]{1,0:T(8,128)(2,1)}, bf16[2048,128]{1,0:T(8,128)(2,1)}) custom-call(s32[1]{0:T(128)} %bitcast.refs_0_, bf16[128,4096]{1,0:T(8,128)(2,1)} %refs_1_.1), custom_call_target="tpu_custom_call" | custom-call | tf_op jit(solution)/shard_map/pallas_call | solution.py:108
  92.7 2.1 %collective-permute-start.5 = (bf16[2048,128]{1,0:T(8,128)(2,1)}, bf16[2048,128]{1,0:T(8,128)(2,1)S(1)}, u32[]{:S(2)}, u32[]{:S(2)}) collective-permute-start(bf16[2048,128]{1,0:T(8,128)(2,1)} %get-tuple-element.38), channel_id=1, source_target_pairs={{0,1},{1,0},{2,3},{3,2},{4,5},{5,4},{6,7},{7,6},{8,9},{9,8},{10,11... | collective-permute-start | bytes 1572872 | tf_op jit(solution)/shard_map/ppermute | solution.py:26
  94.7 9.4 %all-to-all-done.2 = bf16[32,2,1024]{2,1,0:T(2,128)(2,1)S(1)} async-done(((bf16[32,2,1024]{2,1,0:T(2,128)(2,1)}), bf16[32,2,1024]{2,1,0:T(2,128)(2,1)S(1)}, u32[]{:S(2)}, u32[]{:S(2)}) %all-to-all-start.2) | async-done | bytes 131104 | tf_op jit(solution)/shard_map/all_to_all | solution.py:35
  104.2 0.1 copy.78
  104.3 0.3 fusion.31
  104.6 0.1 broadcast_in_dim.16
  104.7 24.6 %all_to_all.25 = bf16[64,32,128]{2,1,0:T(8,128)(2,1)S(1)} all-to-all(bf16[64,32,128]{2,1,0:T(8,128)(2,1)S(1)} %broadcast_in_dim.16), channel_id=1, replica_groups=mesh['dp'=4,'kv_a'=2,'kv_b'=4,'kv_1'=8,'tp'=2] {'kv_a','kv_b','kv_1'}, dimensions={0} | all-to-all | bytes 1048576 | tf_op jit(solution)/shard_map/all_to_all | solution.py:35
  129.3 0.2 copy.79
  129.5 0.2 multiply_reduce_fusion
  129.7 0.2 reshape.119
  129.9 0.1 broadcast_in_dim.17
  130.0 1.5 fusion.6
  131.5 1.9 %collective-permute-start.6 = (f32[257,128]{1,0:T(8,128)S(1)}, f32[257,128]{1,0:T(8,128)S(1)}, u32[]{:S(2)}, u32[]{:S(2)}) collective-permute-start(f32[257,128]{1,0:T(8,128)S(1)} %pad_maximum_fusion.2), channel_id=1, source_target_pairs={{0,1},{1,0},{2,3},{3,2},{4,5},{5,4},{6,7},{7,6},{8,9},{9,8},{10,11... | collective-permute-start | bytes 394760 | tf_op jit(solution)/shard_map/ppermute | solution.py:26
  133.5 1.3 collective-permute-done.6
  134.8 1.2 convolution_convert_fusion
  136.1 5.3 %all-to-all-start.4 = ((bf16[64,32,128]{2,1,0:T(8,128)(2,1)}), bf16[64,32,128]{2,1,0:T(8,128)(2,1)S(1)}, u32[]{:S(2)}, u32[]{:S(2)}) async-start(bf16[64,32,128]{2,1,0:T(8,128)(2,1)} %bitcast.41), calls=%async_computation.4 | async-start | bytes 1048576 | tf_op jit(solution)/shard_map/all_to_all | solution.py:231
  141.3 0.1 constant_dynamic-slice_fusion
  141.4 0.1 copy.84
  141.5 19.6 %all-to-all-done.4 = bf16[64,32,128]{2,1,0:T(8,128)(2,1)S(1)} async-done(((bf16[64,32,128]{2,1,0:T(8,128)(2,1)}), bf16[64,32,128]{2,1,0:T(8,128)(2,1)S(1)}, u32[]{:S(2)}, u32[]{:S(2)}) %all-to-all-start.4) | async-done | bytes 524320 | tf_op jit(solution)/shard_map/all_to_all | solution.py:231
  161.1 0.1 convert_reduce_fusion
  161.2 0.6 fusion.20
  (37 shorter events, 0.4 us)
Async XLA Ops:
  0.6 26.8 %copy-start.2 = (bf16[2048,32]{0,1:T(8,128)(2,1)S(1)}, bf16[2048,32]{0,1:T(8,128)(2,1)}, u32[]{:S(2)}) copy-start(bf16[2048,32]{0,1:T(8,128)(2,1)} %param.20) | copy-start | bytes 393220
  0.6 26.7 %collective-permute-start.1 = (bf16[32,2048]{1,0:T(8,128)(2,1)}, bf16[32,2048]{1,0:T(8,128)(2,1)S(1)}, u32[]{:S(2)}, u32[]{:S(2)}) collective-permute-start(bf16[32,2048]{1,0:T(8,128)(2,1)} %bitcast.106), channel_id=1, source_target_pairs={{0,32},{16,48},{32,0},{48,16},{1,33},{17,49},{33,1},{49,17},{2,34}... | collective-permute-start | bytes 393224 | tf_op jit(solution)/shard_map/ppermute | solution.py:30
  9.1 38.7 %collective-permute-start = (bf16[64,2048]{1,0:T(8,128)(2,1)}, bf16[64,2048]{1,0:T(8,128)(2,1)S(1)}, u32[]{:S(2)}, u32[]{:S(2)}) collective-permute-start(bf16[64,2048]{1,0:T(8,128)(2,1)} %get-tuple-element.24), channel_id=1, source_target_pairs={{0,1},{1,0},{2,3},{3,2},{4,5},{5,4},{6,7},{7,6},{8,9},{9,8},{10,11... | collective-permute-start | bytes 786440 | tf_op jit(solution)/shard_map/ppermute | solution.py:26
  12.6 35.2 %all-to-all-start = ((bf16[64,32,128]{2,1,0:T(8,128)(2,1)}), bf16[64,32,128]{2,1,0:T(8,128)(2,1)S(1)}, u32[]{:S(2)}, u32[]{:S(2)}) async-start(bf16[64,32,128]{2,1,0:T(8,128)(2,1)} %broadcast_in_dim.13), calls=%async_computation | async-start | bytes 1048576 | tf_op jit(solution)/shard_map/all_to_all | solution.py:35
  27.5 22.8 %copy-start.4 = (f32[1024]{0:T(1024)S(1)}, f32[1024]{0:T(1024)}, u32[]{:S(2)}) copy-start(f32[1024]{0:T(1024)} %param.18) | copy-start | bytes 12292
  27.5 23.9 %copy-start.1 = (bf16[64,2048]{1,0:T(8,128)(2,1)S(1)}, bf16[64,2048]{1,0:T(8,128)(2,1)}, u32[]{:S(2)}) copy-start(bf16[64,2048]{1,0:T(8,128)(2,1)} %get-tuple-element.25) | copy-start | bytes 786436
  27.5 20.1 %collective-permute-start.2 = (bf16[2,32,2048]{2,1,0:T(8,128)(2,1)S(1)}, bf16[2,32,2048]{2,1,0:T(8,128)(2,1)S(1)}, u32[]{:S(2)}, u32[]{:S(2)}) collective-permute-start(bf16[2,32,2048]{2,1,0:T(8,128)(2,1)S(1)} %reverse_select_fusion.1), channel_id=1, source_target_pairs={{0,16},{16,0},{32,48},{48,32},{1,17},{17,1},{33,49},{49,33},{2,18}... | collective-permute-start | bytes 786440 | tf_op jit(solution)/shard_map/ppermute | solution.py:30
  47.6 4.1 %copy-start.3 = (f32[4096]{0:T(1024)S(1)}, f32[4096]{0:T(1024)}, u32[]{:S(2)}) copy-start(f32[4096]{0:T(1024)} %param.22) | copy-start | bytes 49156
  48.3 3.1 %collective-permute-start.3 = (f32[65,128]{1,0:T(8,128)S(1)}, f32[65,128]{1,0:T(8,128)S(1)}, u32[]{:S(2)}, u32[]{:S(2)}) collective-permute-start(f32[65,128]{1,0:T(8,128)S(1)} %pad_maximum_fusion.3), channel_id=1, source_target_pairs={{0,1},{1,0},{2,3},{3,2},{4,5},{5,4},{6,7},{7,6},{8,9},{9,8},{10,11... | collective-permute-start | bytes 99848 | tf_op jit(solution)/shard_map/ppermute | solution.py:26
  55.1 30.2 %collective-permute-start.4 = (bf16[128,2048]{1,0:T(8,128)(2,1)}, bf16[128,2048]{1,0:T(8,128)(2,1)}, u32[]{:S(2)}, u32[]{:S(2)}) collective-permute-start(bf16[128,2048]{1,0:T(8,128)(2,1)} %get-tuple-element.31), channel_id=1, source_target_pairs={{0,1},{1,0},{2,3},{3,2},{4,5},{5,4},{6,7},{7,6},{8,9},{9,8},{10,11... | collective-permute-start | bytes 1572872 | tf_op jit(solution)/shard_map/ppermute | solution.py:26
  58.9 22.5 %all-to-all-start.1 = ((bf16[64,2,64]{2,1,0:T(2,128)(2,1)}), bf16[64,2,64]{2,1,0:T(2,128)(2,1)S(1)}, u32[]{:S(2)}, u32[]{:S(2)}) async-start(bf16[64,2,64]{2,1,0:T(2,128)(2,1)} %bitcast.22), calls=%async_computation.1 | async-start | bytes 65536 | tf_op jit(solution)/shard_map/all_to_all | solution.py:171
  69.7 15.5 %copy-start.5 = (f32[128]{0:T(128)S(1)}, f32[128]{0:T(128)}, u32[]{:S(2)}) copy-start(f32[128]{0:T(128)} %param.19) | copy-start | bytes 1540
  84.1 20.6 %copy-start = (f32[2,8,128,128]{3,2,1,0:T(8,128)}, f32[2,8,128,128]{3,2,1,0:T(8,128)S(1)}, u32[]{:S(2)}) copy-start(f32[2,8,128,128]{3,2,1,0:T(8,128)S(1)} %multiply_add_fusion) | copy-start | bytes 3145732
  86.0 18.2 %all-to-all-start.2 = ((bf16[32,2,1024]{2,1,0:T(2,128)(2,1)}), bf16[32,2,1024]{2,1,0:T(2,128)(2,1)S(1)}, u32[]{:S(2)}, u32[]{:S(2)}) async-start(bf16[32,2,1024]{2,1,0:T(2,128)(2,1)} %broadcast_in_dim.15), calls=%async_computation.2 | async-start | bytes 262144 | tf_op jit(solution)/shard_map/all_to_all | solution.py:35
  92.7 12.0 %collective-permute-start.5 = (bf16[2048,128]{1,0:T(8,128)(2,1)}, bf16[2048,128]{1,0:T(8,128)(2,1)S(1)}, u32[]{:S(2)}, u32[]{:S(2)}) collective-permute-start(bf16[2048,128]{1,0:T(8,128)(2,1)} %get-tuple-element.38), channel_id=1, source_target_pairs={{0,1},{1,0},{2,3},{3,2},{4,5},{5,4},{6,7},{7,6},{8,9},{9,8},{10,11... | collective-permute-start | bytes 1572872 | tf_op jit(solution)/shard_map/ppermute | solution.py:26
  104.6 25.4 %copy-start.6 = (bf16[128,2048]{1,0:T(8,128)(2,1)S(1)}, bf16[128,2048]{1,0:T(8,128)(2,1)}, u32[]{:S(2)}) copy-start(bf16[128,2048]{1,0:T(8,128)(2,1)} %get-tuple-element.42) | copy-start | bytes 1572868
  129.7 5.1 %copy-start.7 = (bf16[2048,128]{1,0:T(8,128)(2,1)S(1)}, bf16[2048,128]{1,0:T(8,128)(2,1)}, u32[]{:S(2)}) copy-start(bf16[2048,128]{1,0:T(8,128)(2,1)} %get-tuple-element.40) | copy-start | bytes 1572868
  131.5 3.2 %collective-permute-start.6 = (f32[257,128]{1,0:T(8,128)S(1)}, f32[257,128]{1,0:T(8,128)S(1)}, u32[]{:S(2)}, u32[]{:S(2)}) collective-permute-start(f32[257,128]{1,0:T(8,128)S(1)} %pad_maximum_fusion.2), channel_id=1, source_target_pairs={{0,1},{1,0},{2,3},{3,2},{4,5},{5,4},{6,7},{7,6},{8,9},{9,8},{10,11... | collective-permute-start | bytes 394760 | tf_op jit(solution)/shard_map/ppermute | solution.py:26
  136.1 25.0 %all-to-all-start.4 = ((bf16[64,32,128]{2,1,0:T(8,128)(2,1)}), bf16[64,32,128]{2,1,0:T(8,128)(2,1)S(1)}, u32[]{:S(2)}, u32[]{:S(2)}) async-start(bf16[64,32,128]{2,1,0:T(8,128)(2,1)} %bitcast.41), calls=%async_computation.4 | async-start | bytes 1048576 | tf_op jit(solution)/shard_map/all_to_all | solution.py:231

commit v3 on v2

v3 whole, which is shorter than its diff:
```python
import jax
import jax.numpy as jnp
from jax import lax
from jax.experimental import pallas as pl
from jax.experimental.pallas import tpu as pltpu
from jax.sharding import Mesh
from jax.sharding import PartitionSpec as P


KV = ("kv_0", "kv_1")
KV_TP = ("kv_0", "kv_1", "tp")
DP_KV = ("dp", "kv_0", "kv_1")


EPSILON = 1e-06


def rms_scale(values, gain):
    return values * lax.rsqrt(jnp.mean(values * values, axis=-1, keepdims=True) + EPSILON) * gain


def swapped(x):
    return lax.ppermute(x, "tp", [(0, 1), (1, 0)])


def gathered(x):
    chips = lax.axis_size(KV)
    return lax.all_to_all(jnp.broadcast_to(x[None], (chips, *x.shape)), KV, 0, 0, tiled=True)


def contracted(left, right, dims):
    return lax.dot_general(
        left, right, ((dims[:1], dims[1:]), ((), ())), preferred_element_type=jnp.float32
    )


def square_sums(x):
    values = x.astype(jnp.float32)
    return jnp.sum(values * values, axis=0, keepdims=True)


CHUNK = 256


def selection(core, share):
    source = lax.broadcasted_iota(jnp.int32, (CHUNK, CHUNK // 2), 0)
    target = lax.broadcasted_iota(jnp.int32, (CHUNK, CHUNK // 2), 1)
    wanted = (target // share) * (2 * share) + core * share + target % share
    return jnp.where(source == wanted, 1.0, 0.0).astype(jnp.bfloat16)


def split_mix_kernel(share, core_ref, query_ref, forget_ref, input_ref, gate_ref, gain_ref, mine_ref, other_ref):
    core = core_ref[0]
    for ref, index in ((mine_ref, core), (other_ref, 1 - core)):
        chosen = selection(index, share)
        for chunk in range(query_ref.shape[1] // CHUNK):
            span = pl.ds(chunk * CHUNK, CHUNK)
            block = jnp.concatenate(
                [
                    (part[:, span].astype(jnp.float32) * gain_ref[:, span]).astype(jnp.bfloat16)
                    for part in (query_ref, forget_ref, input_ref, gate_ref)
                ],
                axis=0,
            )
            ref[:, pl.ds(chunk * CHUNK // 2, CHUNK // 2)] = jnp.dot(
                block, chosen, preferred_element_type=jnp.float32
            ).astype(jnp.bfloat16)


def split_up_kernel(share, core_ref, weight_ref, gain_ref, mine_ref, other_ref):
    core = core_ref[0]
    for ref, index in ((mine_ref, core), (other_ref, 1 - core)):
        chosen = selection(index, share)
        for chunk in range(weight_ref.shape[0] // CHUNK):
            span = pl.ds(chunk * CHUNK, CHUNK)
            flipped = weight_ref[span, :].astype(jnp.float32).T * gain_ref[:, span]
            ref[:, pl.ds(chunk * CHUNK // 2, CHUNK // 2)] = jnp.dot(
                flipped.astype(jnp.bfloat16), chosen, preferred_element_type=jnp.float32
            ).astype(jnp.bfloat16)


def split_down_kernel(share, core_ref, weight_ref, mine_ref, other_ref):
    core = core_ref[0]
    for ref, index in ((mine_ref, core), (other_ref, 1 - core)):
        chosen = selection(index, share)
        for chunk in range(weight_ref.shape[1] // CHUNK):
            span = pl.ds(chunk * CHUNK, CHUNK)
            picked = jnp.dot(weight_ref[:, span], chosen, preferred_element_type=jnp.float32)
            ref[pl.ds(chunk * CHUNK // 2, CHUNK // 2), :] = picked.T.astype(jnp.bfloat16)


def split_call(kernel, share, shape, *operands):
    core = lax.axis_index("tp").astype(jnp.int32).reshape(1)
    memory = pl.BlockSpec(memory_space=pltpu.VMEM)
    return pl.pallas_call(
        lambda *refs: kernel(share, *refs),
        out_shape=[jax.ShapeDtypeStruct(shape, jnp.bfloat16)] * 2,
        in_specs=[pl.BlockSpec(memory_space=pltpu.SMEM)] + [memory] * len(operands),
        out_specs=[memory] * 2,
    )(core, *operands)


def per_device(
    tokens,
    w_query,
    w_forget,
    w_input,
    w_output_gate,
    gate_floor,
    head_gain,
    w_out,
    mix_gain,
    ffn_gain,
    w_up,
    w_down,
    state,
):
    chips = lax.axis_size(KV)
    cores = lax.axis_size("tp")
    rows, share = tokens.shape
    width = chips * cores * share
    seq_local, heads_local, head_size, _ = state.shape
    tokens_t = tokens.T
    columns = w_query.shape[2]
    hidden_local = w_up.shape[1]

    token_half = gathered(tokens_t).reshape(chips * share, rows)
    mine, other = split_call(
        split_mix_kernel,
        share,
        (4 * columns, chips * share),
        *[w[:, 0, :].T for w in (w_query, w_forget, w_input, w_output_gate)],
        mix_gain[None, :],
    )
    lent = swapped(other)
    sums = square_sums(token_half)
    theirs = contracted(lent, token_half, (1, 0))
    arrived = swapped(jnp.concatenate([theirs, sums], axis=0))
    projected = contracted(mine, token_half, (1, 0)) + arrived[:-1]
    scale = lax.rsqrt((sums + arrived[-1:]) / width + EPSILON)
    raw = (projected * scale).astype(jnp.bfloat16).T
    raw = lax.all_to_all(
        raw.reshape(chips, seq_local, 4 * columns), KV, split_axis=0, concat_axis=0, tiled=True
    )
    raw = raw.reshape(chips, seq_local, 4, columns).transpose(2, 1, 0, 3)
    raw = raw.reshape(4, seq_local, heads_local, head_size).astype(jnp.float32)

    query_vec = raw[0] * head_size ** (-0.5)
    floor_heads = gate_floor.reshape(heads_local, head_size)
    forget_gate = floor_heads + (1.0 - floor_heads) * jax.nn.sigmoid(raw[1])
    input_vec = raw[2]
    gate_vec = raw[3]
    new_state = (
        forget_gate[..., None] * state + (1.0 - forget_gate)[..., None] * input_vec[:, :, None, :]
    )
    head_out = jnp.einsum("bhk,bhkv->bhv", query_vec, new_state, precision=lax.Precision.HIGHEST)
    branch = rms_scale(head_out, head_gain) * jax.nn.silu(gate_vec)
    branch = branch.reshape(seq_local, heads_local * head_size).astype(jnp.bfloat16)

    own_up, other = split_call(
        split_up_kernel, share, (hidden_local, chips * share), w_up, ffn_gain[None, :]
    )
    branch, own_up, lent_up = lax.optimization_barrier((branch, own_up, swapped(other)))

    branch_half = gathered(branch).reshape(rows, heads_local * head_size)
    tp = lax.axis_index("tp")
    span = heads_local * head_size
    own_out = lax.dynamic_slice_in_dim(w_out, tp * span, span, 0)
    lent_out = swapped(lax.dynamic_slice_in_dim(w_out, (1 - tp) * span, span, 0))
    theirs = swapped(contracted(lent_out, branch_half, (0, 1)))
    projected = contracted(own_out, branch_half, (0, 1)) + theirs
    residual = (tokens_t.astype(jnp.float32) + projected).astype(jnp.bfloat16)

    own_down, other = split_call(split_down_kernel, share, (chips * share, hidden_local), w_down)
    residual, own_down, lent_down = lax.optimization_barrier((residual, own_down, swapped(other)))

    residual_half = gathered(residual).reshape(chips * share, rows)
    up_both = jnp.concatenate([own_up, lent_up], axis=0)
    partial = contracted(up_both, residual_half, (1, 0))
    sums = square_sums(residual_half)
    arrived = swapped(jnp.concatenate([partial, sums], axis=0))
    upward = partial + jnp.concatenate(
        [arrived[hidden_local : 2 * hidden_local], arrived[:hidden_local]], axis=0
    )
    scale = lax.rsqrt((sums + arrived[-1:]) / width + EPSILON)
    hidden = jnp.square(jax.nn.relu(upward * scale)).astype(jnp.bfloat16)

    down_both = jnp.concatenate([own_down, lent_down], axis=1)
    terms = contracted(down_both, hidden, (1, 0)).astype(jnp.bfloat16)
    terms = lax.all_to_all(
        terms.reshape(chips, share, rows), KV, split_axis=0, concat_axis=0, tiled=True
    )
    summed = terms.astype(jnp.float32).sum(axis=0)
    mixed = (residual.astype(jnp.float32) + summed).astype(jnp.bfloat16).T
    return (mixed, new_state)


def solution(mesh):
    torus = Mesh(
        mesh.devices.reshape(mesh.shape["dp"], 8, 8, mesh.shape["tp"]), ("dp", "kv_0", "kv_1", "tp")
    )
    placed = (
        P("dp", KV_TP),
        P(None, "tp", KV),
        P(None, "tp", KV),
        P(None, "tp", KV),
        P(None, "tp", KV),
        P("tp"),
        P(),
        P(None, KV_TP),
        P(),
        P(),
        P(None, KV_TP),
        P(KV_TP, None),
        P(DP_KV, "tp", None, None),
    )

    return jax.shard_map(
        per_device,
        mesh=torus,
        in_specs=placed,
        out_specs=(P("dp", KV_TP), P(DP_KV, "tp", None, None)),
        check_vma=False,
    )
```

time: 163 us -> 146 us (0.90)
  the two profiles are of different devices: /device:TPU:4 before, /device:TPU:2 now
where the time goes in v3:
time: 146 us
  blocking collectives  50.3 us (34%)
  starting transfers between devices  40.8 us (28%)
  waiting for transfers between devices  36.6 us (25%)
  Pallas kernels  8.05 us (6%)
  local copies, waits for them, and re-layouts  4.17 us (3%)
  matrix products  2.63 us (2%)
  other arithmetic  2.13 us (1%)
    all_to_all x1, blocking collectives, gathered(): lax.all_to_all(jnp.broadcast_to(x[None], (chips, *x.shape)), KV, 0, 0, ti...  25.4 us
    all_to_all x1, blocking collectives, per_device(): lax.all_to_all(terms.reshape(chips, share, rows), KV, split_axis=0, conca...  24.9 us
    all_to_all x2, waiting for transfers between devices, gathered(): lax.all_to_all(jnp.broadcast_to(x[None], (chips, *x.shape)), KV, 0, 0, ti...  22.4 us
    all_to_all x2, starting transfers between devices, gathered(): lax.all_to_all(jnp.broadcast_to(x[None], (chips, *x.shape)), KV, 0, 0, ti...  21.2 us
    ppermute x7, starting transfers between devices, swapped(): return lax.ppermute(x, 'tp', [(0, 1), (1, 0)])  14.7 us
    all_to_all x1, waiting for transfers between devices, per_device(): lax.all_to_all(raw.reshape(chips, seq_local, 4 * columns), KV, split_axis...  11.9 us
    pallas_call x3, Pallas kernels, split_call(): pl.pallas_call(lambda *refs: kernel(share, *refs), out_shape=[jax.ShapeDt...  8.05 us
    all_to_all x1, starting transfers between devices, per_device(): lax.all_to_all(raw.reshape(chips, seq_local, 4 * columns), KV, split_axis...  4.98 us
  transfers between devices with their start and end apart: 10, of which 5 were waited for; matrix products, arithmetic and copies ran while one was open for 3% of the time, Pallas kernels for 6%

profile of v3, /device:TPU:2, one launch (start us, length us, event | category | flops | bytes accessed | tf_op | source)
XLA Modules:
  0.0 145.7 jit_solution(9385030696090165132)
XLA Ops:
  0.6 0.0 copy-start
  0.6 1.6 %broadcast_in_dim.15 = bf16[64,32,128]{2,1,0:T(8,128)(2,1)} broadcast(bf16[32,128]{1,0:T(8,128)(2,1)} %bitcast.76), dimensions={1,2} | broadcast | bytes 532480 | tf_op jit(solution)/shard_map/broadcast_in_dim | solution.py:28
  2.2 16.6 %all-to-all-start = ((bf16[64,32,128]{2,1,0:T(8,128)(2,1)}), bf16[64,32,128]{2,1,0:T(8,128)(2,1)S(1)}, u32[]{:S(2)}, u32[]{:S(2)}) async-start(bf16[64,32,128]{2,1,0:T(8,128)(2,1)} %broadcast_in_dim.15), calls=%async_computation | async-start | bytes 1048576 | tf_op jit(solution)/shard_map/all_to_all | solution.py:28
  18.8 2.2 %shard_map.140 = (bf16[64,2048]{1,0:T(8,128)(2,1)}, bf16[64,2048]{1,0:T(8,128)(2,1)}) custom-call(s32[1]{0:T(128)} %bitcast.1.refs_0_, bf16[16,4096]{1,0:T(8,128)(2,1)} %bitcast.69, bf16[16,4096]{1,0:T(8,128)(2,1)} %bitcast.70, bf16[16,4096]{1,0:T(8,128)(2,1)} %bitcast.71, bf16[16,4096]{1,0:T(8,128)(2,1)} %bitcast.72, f32[1,4096]{1,0:T(1,128)} %bitcast.79), custom_call_target="tpu_custom_call" | custom-call | tf_op jit(solution)/shard_map/pallas_call | solution.py:95
  21.1 1.9 %collective-permute-start = (bf16[64,2048]{1,0:T(8,128)(2,1)}, bf16[64,2048]{1,0:T(8,128)(2,1)S(1)}, u32[]{:S(2)}, u32[]{:S(2)}) collective-permute-start(bf16[64,2048]{1,0:T(8,128)(2,1)} %get-tuple-element.15), channel_id=1, source_target_pairs={{0,1},{1,0},{2,3},{3,2},{4,5},{5,4},{6,7},{7,6},{8,9},{9,8},{10,11... | collective-permute-start | bytes 786440 | tf_op jit(solution)/shard_map/ppermute | solution.py:23
  23.0 15.6 %all-to-all-done = bf16[64,32,128]{2,1,0:T(8,128)(2,1)S(1)} async-done(((bf16[64,32,128]{2,1,0:T(8,128)(2,1)}), bf16[64,32,128]{2,1,0:T(8,128)(2,1)S(1)}, u32[]{:S(2)}, u32[]{:S(2)}) %all-to-all-start) | async-done | bytes 524320 | tf_op jit(solution)/shard_map/all_to_all | solution.py:28
  38.5 0.3 multiply_reduce_fusion.1
  38.8 0.0 collective-permute-done
  38.8 0.2 fusion.32
  39.1 0.0 copy-start.5
  39.1 1.9 %collective-permute-start.1 = (f32[65,128]{1,0:T(8,128)S(1)}, f32[65,128]{1,0:T(8,128)S(1)}, u32[]{:S(2)}, u32[]{:S(2)}) collective-permute-start(f32[65,128]{1,0:T(8,128)S(1)} %pad_maximum_fusion.1), channel_id=1, source_target_pairs={{0,1},{1,0},{2,3},{3,2},{4,5},{5,4},{6,7},{7,6},{8,9},{9,8},{10,11... | collective-permute-start | bytes 99848 | tf_op jit(solution)/shard_map/ppermute | solution.py:23
  41.0 3.0 %shard_map.141 = (bf16[128,2048]{1,0:T(8,128)(2,1)}, bf16[128,2048]{1,0:T(8,128)(2,1)}) custom-call(s32[1]{0:T(128)} %bitcast.1.refs_0_, bf16[4096,128]{1,0:T(8,128)(2,1)} %refs_1_.2, f32[1,4096]{1,0:T(1,128)} %bitcast.77), custom_call_target="tpu_custom_call" | custom-call | tf_op jit(solution)/shard_map/pallas_call | solution.py:95
  44.0 2.5 %collective-permute-start.2 = (bf16[128,2048]{1,0:T(8,128)(2,1)}, bf16[128,2048]{1,0:T(8,128)(2,1)S(1)}, u32[]{:S(2)}, u32[]{:S(2)}) collective-permute-start(bf16[128,2048]{1,0:T(8,128)(2,1)} %get-tuple-element.17), channel_id=1, source_target_pairs={{0,1},{1,0},{2,3},{3,2},{4,5},{5,4},{6,7},{7,6},{8,9},{9,8},{10,11... | collective-permute-start | bytes 1572872 | tf_op jit(solution)/shard_map/ppermute | solution.py:23
  46.6 0.0 collective-permute-done.1
  46.6 0.0 copy-done.3
  46.6 0.2 fusion.18
  46.8 0.7 copy.39
  47.5 5.0 %all-to-all-start.1 = ((bf16[64,2,64]{2,1,0:T(2,128)(2,1)}), bf16[64,2,64]{2,1,0:T(2,128)(2,1)S(1)}, u32[]{:S(2)}, u32[]{:S(2)}) async-start(bf16[64,2,64]{2,1,0:T(2,128)(2,1)} %bitcast.15), calls=%async_computation.1 | async-start | bytes 65536 | tf_op jit(solution)/shard_map/all_to_all | solution.py:142
  52.5 0.0 copy-done.5
  52.6 11.9 %all-to-all-done.1 = bf16[64,2,64]{2,1,0:T(2,128)(2,1)S(1)} async-done(((bf16[64,2,64]{2,1,0:T(2,128)(2,1)}), bf16[64,2,64]{2,1,0:T(2,128)(2,1)S(1)}, u32[]{:S(2)}, u32[]{:S(2)}) %all-to-all-start.1) | async-done | bytes 16416 | tf_op jit(solution)/shard_map/all_to_all | solution.py:142
  64.5 0.1 copy.41
  64.6 0.1 copy.43
  64.7 0.1 div.28
  64.8 0.1 copy.45
  64.8 0.1 squeeze.21
  64.9 0.1 copy.44
  65.0 0.1 mul.121
  65.1 0.1 copy.42
  65.2 0.1 reshape.96
  65.3 0.0 copy-done.2
  65.3 0.6 multiply_add_fusion
  65.9 0.0 copy-start.1
  65.9 0.0 copy-start.6
  65.9 1.0 fusion.33
  66.9 0.1 multiply_reduce_fusion.2
  67.0 0.1 fusion.23
  67.1 0.0 collective-permute-done.2
  67.1 0.8 broadcast_in_dim.18
  68.0 4.6 %all-to-all-start.2 = ((bf16[64,2,1024]{2,1,0:T(2,128)(2,1)}), bf16[64,2,1024]{2,1,0:T(2,128)(2,1)S(1)}, u32[]{:S(2)}, u32[]{:S(2)}) async-start(bf16[64,2,1024]{2,1,0:T(2,128)(2,1)} %broadcast_in_dim.18), calls=%async_computation.2 | async-start | bytes 524288 | tf_op jit(solution)/shard_map/all_to_all | solution.py:28
  72.6 0.0 copy-done
  72.6 0.0 copy-start.4
  72.6 1.9 %collective-permute-start.3 = (bf16[1024,32]{0,1:T(8,128)(2,1)S(1)}, bf16[1024,32]{0,1:T(8,128)(2,1)S(1)}, u32[]{:S(2)}, u32[]{:S(2)}) collective-permute-start(bf16[1024,32]{0,1:T(8,128)(2,1)S(1)} %constant_dynamic-slice_fusion), channel_id=1, source_target_pairs={{0,1},{1,0},{2,3},{3,2},{4,5},{5,4},{6,7},{7,6},{8,9},{9,8},{10,11... | collective-permute-start | bytes 196616 | tf_op jit(solution)/shard_map/ppermute | solution.py:23
  74.5 2.8 %shard_map.142 = (bf16[2048,128]{1,0:T(8,128)(2,1)}, bf16[2048,128]{1,0:T(8,128)(2,1)}) custom-call(s32[1]{0:T(128)} %bitcast.1.refs_0_, bf16[128,4096]{1,0:T(8,128)(2,1)} %refs_1_.3), custom_call_target="tpu_custom_call" | custom-call | tf_op jit(solution)/shard_map/pallas_call | solution.py:95
  77.4 0.0 copy-done.1
  77.4 2.4 %collective-permute-start.5 = (bf16[2048,128]{1,0:T(8,128)(2,1)}, bf16[2048,128]{1,0:T(8,128)(2,1)S(1)}, u32[]{:S(2)}, u32[]{:S(2)}) collective-permute-start(bf16[2048,128]{1,0:T(8,128)(2,1)} %get-tuple-element.20), channel_id=1, source_target_pairs={{0,1},{1,0},{2,3},{3,2},{4,5},{5,4},{6,7},{7,6},{8,9},{9,8},{10,11... | collective-permute-start | bytes 1572872 | tf_op jit(solution)/shard_map/ppermute | solution.py:23
  79.8 6.9 %all-to-all-done.2 = bf16[64,2,1024]{2,1,0:T(2,128)(2,1)S(1)} async-done(((bf16[64,2,1024]{2,1,0:T(2,128)(2,1)}), bf16[64,2,1024]{2,1,0:T(2,128)(2,1)S(1)}, u32[]{:S(2)}, u32[]{:S(2)}) %all-to-all-start.2) | async-done | bytes 262176 | tf_op jit(solution)/shard_map/all_to_all | solution.py:28
  86.6 0.1 reshape.89
  86.7 0.0 collective-permute-done.3
  86.8 0.2 fusion.34
  86.9 2.1 %collective-permute-start.4 = (f32[32,128]{1,0:T(8,128)S(1)}, f32[32,128]{1,0:T(8,128)S(1)}, u32[]{:S(2)}, u32[]{:S(2)}) collective-permute-start(f32[32,128]{1,0:T(8,128)S(1)} %fusion.34), channel_id=1, source_target_pairs={{0,1},{1,0},{2,3},{3,2},{4,5},{5,4},{6,7},{7,6},{8,9},{9,8},{10,11... | collective-permute-start | bytes 49160 | tf_op jit(solution)/shard_map/ppermute | solution.py:23
  89.0 0.2 fusion.14
  89.2 1.0 collective-permute-done.4
  90.2 0.0 collective-permute-done.5
  90.2 0.1 broadcast_in_dim.19
  90.3 25.4 %all_to_all.25 = bf16[64,32,128]{2,1,0:T(8,128)(2,1)S(1)} all-to-all(bf16[64,32,128]{2,1,0:T(8,128)(2,1)S(1)} %broadcast_in_dim.19), channel_id=1, replica_groups=mesh['dp'=4,'kv_0'=8,'kv_1'=8,'tp'=2] {'kv_0','kv_1'}, dimensions={0} | all-to-all | bytes 1048576 | tf_op jit(solution)/shard_map/all_to_all | solution.py:28
  115.6 0.4 fusion.3
  116.1 0.0 copy-start.8
  116.1 0.3 multiply_reduce_fusion
  116.4 1.9 %collective-permute-start.6 = (f32[257,128]{1,0:T(8,128)S(1)}, f32[257,128]{1,0:T(8,128)S(1)}, u32[]{:S(2)}, u32[]{:S(2)}) collective-permute-start(f32[257,128]{1,0:T(8,128)S(1)} %pad_maximum_fusion), channel_id=1, source_target_pairs={{0,1},{1,0},{2,3},{3,2},{4,5},{5,4},{6,7},{7,6},{8,9},{9,8},{10,11... | collective-permute-start | bytes 394760 | tf_op jit(solution)/shard_map/ppermute | solution.py:23
  118.3 1.3 collective-permute-done.6
  119.7 0.4 convolution_convert_fusion
  120.1 24.9 %all_to_all.26 = bf16[64,32,128]{2,1,0:T(8,128)(2,1)S(1)} all-to-all(bf16[64,32,128]{2,1,0:T(8,128)(2,1)S(1)} %bitcast.67), channel_id=1, replica_groups=mesh['dp'=4,'kv_0'=8,'kv_1'=8,'tp'=2] {'kv_0','kv_1'}, dimensions={0} | all-to-all | bytes 1048576 | tf_op jit(solution)/shard_map/all_to_all | solution.py:190
  145.0 0.1 convert_reduce_fusion
  145.1 0.6 fusion.22
  (20 shorter events, 0.1 us)
Async XLA Ops:
  0.6 72.0 %copy-start = (bf16[2048,32]{0,1:T(8,128)(2,1)S(1)}, bf16[2048,32]{0,1:T(8,128)(2,1)}, u32[]{:S(2)}) copy-start(bf16[2048,32]{0,1:T(8,128)(2,1)} %param.20) | copy-start | bytes 393220
  2.2 36.3 %all-to-all-start = ((bf16[64,32,128]{2,1,0:T(8,128)(2,1)}), bf16[64,32,128]{2,1,0:T(8,128)(2,1)S(1)}, u32[]{:S(2)}, u32[]{:S(2)}) async-start(bf16[64,32,128]{2,1,0:T(8,128)(2,1)} %broadcast_in_dim.15), calls=%async_computation | async-start | bytes 1048576 | tf_op jit(solution)/shard_map/all_to_all | solution.py:28
  21.1 17.8 %collective-permute-start = (bf16[64,2048]{1,0:T(8,128)(2,1)}, bf16[64,2048]{1,0:T(8,128)(2,1)S(1)}, u32[]{:S(2)}, u32[]{:S(2)}) collective-permute-start(bf16[64,2048]{1,0:T(8,128)(2,1)} %get-tuple-element.15), channel_id=1, source_target_pairs={{0,1},{1,0},{2,3},{3,2},{4,5},{5,4},{6,7},{7,6},{8,9},{9,8},{10,11... | collective-permute-start | bytes 786440 | tf_op jit(solution)/shard_map/ppermute | solution.py:23
  38.8 7.7 %copy-start.3 = (bf16[64,2048]{1,0:T(8,128)(2,1)S(1)}, bf16[64,2048]{1,0:T(8,128)(2,1)}, u32[]{:S(2)}) copy-start(bf16[64,2048]{1,0:T(8,128)(2,1)} %get-tuple-element.14) | copy-start | bytes 786436
  39.1 13.5 %copy-start.5 = (f32[1024]{0:T(1024)S(1)}, f32[1024]{0:T(1024)}, u32[]{:S(2)}) copy-start(f32[1024]{0:T(1024)} %param.18) | copy-start | bytes 12292
  39.1 7.5 %collective-permute-start.1 = (f32[65,128]{1,0:T(8,128)S(1)}, f32[65,128]{1,0:T(8,128)S(1)}, u32[]{:S(2)}, u32[]{:S(2)}) collective-permute-start(f32[65,128]{1,0:T(8,128)S(1)} %pad_maximum_fusion.1), channel_id=1, source_target_pairs={{0,1},{1,0},{2,3},{3,2},{4,5},{5,4},{6,7},{7,6},{8,9},{9,8},{10,11... | collective-permute-start | bytes 99848 | tf_op jit(solution)/shard_map/ppermute | solution.py:23
  44.0 21.3 %copy-start.2 = (f32[2,8,128,128]{3,2,1,0:T(8,128)S(1)}, f32[2,8,128,128]{3,2,1,0:T(8,128)}, u32[]{:S(2)}) copy-start(f32[2,8,128,128]{3,2,1,0:T(8,128)} %param.25) | copy-start | bytes 3145732
  44.0 23.1 %collective-permute-start.2 = (bf16[128,2048]{1,0:T(8,128)(2,1)}, bf16[128,2048]{1,0:T(8,128)(2,1)S(1)}, u32[]{:S(2)}, u32[]{:S(2)}) collective-permute-start(bf16[128,2048]{1,0:T(8,128)(2,1)} %get-tuple-element.17), channel_id=1, source_target_pairs={{0,1},{1,0},{2,3},{3,2},{4,5},{5,4},{6,7},{7,6},{8,9},{9,8},{10,11... | collective-permute-start | bytes 1572872 | tf_op jit(solution)/shard_map/ppermute | solution.py:23
  47.5 16.9 %all-to-all-start.1 = ((bf16[64,2,64]{2,1,0:T(2,128)(2,1)}), bf16[64,2,64]{2,1,0:T(2,128)(2,1)S(1)}, u32[]{:S(2)}, u32[]{:S(2)}) async-start(bf16[64,2,64]{2,1,0:T(2,128)(2,1)} %bitcast.15), calls=%async_computation.1 | async-start | bytes 65536 | tf_op jit(solution)/shard_map/all_to_all | solution.py:142
  65.9 11.5 %copy-start.1 = (f32[2,8,128,128]{3,2,1,0:T(8,128)}, f32[2,8,128,128]{3,2,1,0:T(8,128)S(1)}, u32[]{:S(2)}) copy-start(f32[2,8,128,128]{3,2,1,0:T(8,128)S(1)} %multiply_add_fusion) | copy-start | bytes 3145732
  65.9 1.1 copy-start.6
  68.0 18.7 %all-to-all-start.2 = ((bf16[64,2,1024]{2,1,0:T(2,128)(2,1)}), bf16[64,2,1024]{2,1,0:T(2,128)(2,1)S(1)}, u32[]{:S(2)}, u32[]{:S(2)}) async-start(bf16[64,2,1024]{2,1,0:T(2,128)(2,1)} %broadcast_in_dim.18), calls=%async_computation.2 | async-start | bytes 524288 | tf_op jit(solution)/shard_map/all_to_all | solution.py:28
  72.6 17.5 %copy-start.4 = (bf16[128,32]{0,1:T(8,128)(2,1)S(1)}, bf16[128,32]{0,1:T(8,128)(2,1)}, u32[]{:S(2)}) copy-start(bf16[128,32]{0,1:T(8,128)(2,1)} %param.13) | copy-start | bytes 24580
  72.6 14.1 %collective-permute-start.3 = (bf16[1024,32]{0,1:T(8,128)(2,1)S(1)}, bf16[1024,32]{0,1:T(8,128)(2,1)S(1)}, u32[]{:S(2)}, u32[]{:S(2)}) collective-permute-start(bf16[1024,32]{0,1:T(8,128)(2,1)S(1)} %constant_dynamic-slice_fusion), channel_id=1, source_target_pairs={{0,1},{1,0},{2,3},{3,2},{4,5},{5,4},{6,7},{7,6},{8,9},{9,8},{10,11... | collective-permute-start | bytes 196616 | tf_op jit(solution)/shard_map/ppermute | solution.py:23
  77.4 12.8 %collective-permute-start.5 = (bf16[2048,128]{1,0:T(8,128)(2,1)}, bf16[2048,128]{1,0:T(8,128)(2,1)S(1)}, u32[]{:S(2)}, u32[]{:S(2)}) collective-permute-start(bf16[2048,128]{1,0:T(8,128)(2,1)} %get-tuple-element.20), channel_id=1, source_target_pairs={{0,1},{1,0},{2,3},{3,2},{4,5},{5,4},{6,7},{7,6},{8,9},{9,8},{10,11... | collective-permute-start | bytes 1572872 | tf_op jit(solution)/shard_map/ppermute | solution.py:23
  86.9 28.7 %copy-start.7 = (bf16[128,2048]{1,0:T(8,128)(2,1)S(1)}, bf16[128,2048]{1,0:T(8,128)(2,1)}, u32[]{:S(2)}) copy-start(bf16[128,2048]{1,0:T(8,128)(2,1)} %get-tuple-element.24) | copy-start | bytes 1572868
  86.9 3.2 %collective-permute-start.4 = (f32[32,128]{1,0:T(8,128)S(1)}, f32[32,128]{1,0:T(8,128)S(1)}, u32[]{:S(2)}, u32[]{:S(2)}) collective-permute-start(f32[32,128]{1,0:T(8,128)S(1)} %fusion.34), channel_id=1, source_target_pairs={{0,1},{1,0},{2,3},{3,2},{4,5},{5,4},{6,7},{7,6},{8,9},{9,8},{10,11... | collective-permute-start | bytes 49160 | tf_op jit(solution)/shard_map/ppermute | solution.py:23
  116.1 3.6 %copy-start.8 = (bf16[2048,128]{1,0:T(8,128)(2,1)S(1)}, bf16[2048,128]{1,0:T(8,128)(2,1)}, u32[]{:S(2)}) copy-start(bf16[2048,128]{1,0:T(8,128)(2,1)} %get-tuple-element.22) | copy-start | bytes 1572868
  116.4 3.2 %collective-permute-start.6 = (f32[257,128]{1,0:T(8,128)S(1)}, f32[257,128]{1,0:T(8,128)S(1)}, u32[]{:S(2)}, u32[]{:S(2)}) collective-permute-start(f32[257,128]{1,0:T(8,128)S(1)} %pad_maximum_fusion), channel_id=1, source_target_pairs={{0,1},{1,0},{2,3},{3,2},{4,5},{5,4},{6,7},{7,6},{8,9},{9,8},{10,11... | collective-permute-start | bytes 394760 | tf_op jit(solution)/shard_map/ppermute | solution.py:23

commit v4 on v3

--- a/solution.py
+++ b/solution.py
@@ -87,6 +87,20 @@
             span = pl.ds(chunk * CHUNK, CHUNK)
             picked = jnp.dot(weight_ref[:, span], chosen, preferred_element_type=jnp.float32)
             ref[pl.ds(chunk * CHUNK // 2, CHUNK // 2), :] = picked.T.astype(jnp.bfloat16)
+
+
+def project_kernel(mix_ref, tokens_ref, packed_ref):
+    partial = jnp.dot(mix_ref[...], tokens_ref[...], preferred_element_type=jnp.float32)
+    values = tokens_ref[...].astype(jnp.float32)
+    sums = jnp.sum(values * values, axis=0, keepdims=True)
+    high = sums.astype(jnp.bfloat16).astype(jnp.float32)
+    cores, rows, lanes = packed_ref.shape
+    columns = partial.shape[0] // cores
+    place = lax.broadcasted_iota(jnp.int32, (lanes - columns, rows), 0)
+    extra = jnp.where(place == 0, high, jnp.where(place == 1, sums - high, 0.0))
+    for core in range(cores):
+        block = jnp.concatenate([partial[core * columns : (core + 1) * columns], extra], axis=0)
+        packed_ref[core] = block.T.astype(jnp.bfloat16)
 
 
 def split_call(kernel, share, shape, *operands):
@@ -124,6 +138,8 @@
     columns = w_query.shape[2]
     hidden_local = w_up.shape[1]
 
+    tp = lax.axis_index("tp")
+
     token_half = gathered(tokens_t).reshape(chips * share, rows)
     mine, other = split_call(
         split_mix_kernel,
@@ -133,17 +149,34 @@
         mix_gain[None, :],
     )
     lent = swapped(other)
-    sums = square_sums(token_half)
-    theirs = contracted(lent, token_half, (1, 0))
-    arrived = swapped(jnp.concatenate([theirs, sums], axis=0))
-    projected = contracted(mine, token_half, (1, 0)) + arrived[:-1]
-    scale = lax.rsqrt((sums + arrived[-1:]) / width + EPSILON)
-    raw = (projected * scale).astype(jnp.bfloat16).T
-    raw = lax.all_to_all(
-        raw.reshape(chips, seq_local, 4 * columns), KV, split_axis=0, concat_axis=0, tiled=True
-    )
+    mix = jnp.concatenate([jnp.where(tp == 0, mine, lent), jnp.where(tp == 0, lent, mine)], axis=0)
+    own_up, other = split_call(
+        split_up_kernel, share, (hidden_local, chips * share), w_up, ffn_gain[None, :]
+    )
+    lent_up = swapped(other)
+    mix, own_up, lent_up = lax.optimization_barrier((mix, own_up, lent_up))
+    memory = pl.BlockSpec(memory_space=pltpu.VMEM)
+    raw = pl.pallas_call(
+        project_kernel,
+        out_shape=jax.ShapeDtypeStruct((cores, rows, 128), jnp.bfloat16),
+        in_specs=[memory] * 2,
+        out_specs=memory,
+    )(mix, token_half)
+    raw = raw.reshape(cores, chips, seq_local, 128).transpose(1, 0, 2, 3)
+    raw = raw.reshape(chips * cores, seq_local, 128)
+    raw, w_out, w_down = lax.optimization_barrier((raw, w_out, w_down))
+    raw = lax.all_to_all(raw, KV_TP, split_axis=0, concat_axis=0, tiled=True)
+    raw = raw.reshape(chips, cores, seq_local, 128).astype(jnp.float32).sum(axis=1)
+    sums = raw[0, :, 4 * columns : 4 * columns + 2].sum(axis=1)
+    scale = lax.rsqrt(sums / width + EPSILON)
+    raw = raw[:, :, : 4 * columns] * scale[None, :, None]
     raw = raw.reshape(chips, seq_local, 4, columns).transpose(2, 1, 0, 3)
-    raw = raw.reshape(4, seq_local, heads_local, head_size).astype(jnp.float32)
+    raw = raw.reshape(4, seq_local, heads_local, head_size)
+    span = heads_local * head_size
+    own_out = lax.dynamic_slice_in_dim(w_out, tp * span, span, 0)
+    lent_out = swapped(lax.dynamic_slice_in_dim(w_out, (1 - tp) * span, span, 0))
+    own_down, other = split_call(split_down_kernel, share, (chips * share, hidden_local), w_down)
+    lent_down = swapped(other)
 
     query_vec = raw[0] * head_size ** (-0.5)
     floor_heads = gate_floor.reshape(heads_local, head_size)
@@ -157,22 +190,14 @@
     branch = rms_scale(head_out, head_gain) * jax.nn.silu(gate_vec)
     branch = branch.reshape(seq_local, heads_local * head_size).astype(jnp.bfloat16)
 
-    own_up, other = split_call(
-        split_up_kernel, share, (hidden_local, chips * share), w_up, ffn_gain[None, :]
-    )
-    branch, own_up, lent_up = lax.optimization_barrier((branch, own_up, swapped(other)))
+    branch, own_out, lent_out, own_down, lent_down = lax.optimization_barrier(
+        (branch, own_out, lent_out, own_down, lent_down)
+    )
 
     branch_half = gathered(branch).reshape(rows, heads_local * head_size)
-    tp = lax.axis_index("tp")
-    span = heads_local * head_size
-    own_out = lax.dynamic_slice_in_dim(w_out, tp * span, span, 0)
-    lent_out = swapped(lax.dynamic_slice_in_dim(w_out, (1 - tp) * span, span, 0))
     theirs = swapped(contracted(lent_out, branch_half, (0, 1)))
     projected = contracted(own_out, branch_half, (0, 1)) + theirs
     residual = (tokens_t.astype(jnp.float32) + projected).astype(jnp.bfloat16)
-
-    own_down, other = split_call(split_down_kernel, share, (chips * share, hidden_local), w_down)
-    residual, own_down, lent_down = lax.optimization_barrier((residual, own_down, swapped(other)))
 
     residual_half = gathered(residual).reshape(chips * share, rows)
     up_both = jnp.concatenate([own_up, lent_up], axis=0)

time: 146 us -> 146 us (level)
  blocking collectives: 50.3 us -> 72.5 us
  waiting for transfers between devices: 36.6 us -> 15.2 us
  starting transfers between devices: 40.8 us -> 35.7 us
  Pallas kernels: 8.05 us -> 10.3 us
    all_to_all x1 -> x2, blocking collectives: 25.4 us -> 47.1 us  [gathered(): lax.all_to_all(jnp.broadcast_to(x[None], (chips, *x.shape)), KV, 0, 0, ti...]
    all_to_all x2 -> x1, waiting for transfers between devices: 22.4 us -> 8.26 us  [gathered(): lax.all_to_all(jnp.broadcast_to(x[None], (chips, *x.shape)), KV, 0, 0, ti...]
    all_to_all x1, waiting for transfers between devices: 11.9 us -> 3.72 us  [per_device(): raw = lax.all_to_all(raw, KV_TP, split_axis=0, concat_axis=0, tiled=True)]
    all_to_all x2 -> x1, starting transfers between devices: 21.2 us -> 16.6 us  [gathered(): lax.all_to_all(jnp.broadcast_to(x[None], (chips, *x.shape)), KV, 0, 0, ti...]
    pallas_call x0 -> x1, Pallas kernels: none -> 2.23 us  [per_device(): pl.pallas_call(project_kernel, out_shape=jax.ShapeDtypeStruct((cores, row...]
    ppermute x7 -> x6, starting transfers between devices: 14.7 us -> 12.9 us  [swapped(): return lax.ppermute(x, 'tp', [(0, 1), (1, 0)])]
    ppermute x7 -> x6, waiting for transfers between devices: 2.31 us -> 3.26 us  [swapped(): return lax.ppermute(x, 'tp', [(0, 1), (1, 0)])]
  transfers between devices with their start and end apart: 10 -> 8, of which waited for: 5 -> 5; matrix products, arithmetic and copies ran while one was open for 3% -> 3% of each run, Pallas kernels for 6% -> 6%
where the time goes in v4:
time: 146 us; the launch traced here: 145 us
  blocking collectives  72.5 us (50%)
  starting transfers between devices  35.7 us (24%)
  waiting for transfers between devices  15.2 us (10%)
  Pallas kernels  10.3 us (7%)
  local copies, waits for them, and re-layouts  5.2 us (4%)
  other arithmetic  2.96 us (2%)
  matrix products  2.18 us (1%)
    all_to_all x2, blocking collectives, gathered(): lax.all_to_all(jnp.broadcast_to(x[None], (chips, *x.shape)), KV, 0, 0, ti...  47.1 us
    all_to_all x1, blocking collectives, per_device(): lax.all_to_all(terms.reshape(chips, share, rows), KV, split_axis=0, conca...  25.4 us
    all_to_all x1, starting transfers between devices, gathered(): lax.all_to_all(jnp.broadcast_to(x[None], (chips, *x.shape)), KV, 0, 0, ti...  16.6 us
    ppermute x6, starting transfers between devices, swapped(): return lax.ppermute(x, 'tp', [(0, 1), (1, 0)])  12.9 us
    all_to_all x1, waiting for transfers between devices, gathered(): lax.all_to_all(jnp.broadcast_to(x[None], (chips, *x.shape)), KV, 0, 0, ti...  8.26 us
    pallas_call x3, Pallas kernels, split_call(): pl.pallas_call(lambda *refs: kernel(share, *refs), out_shape=[jax.ShapeDt...  8.11 us
    all_to_all x1, starting transfers between devices, per_device(): raw = lax.all_to_all(raw, KV_TP, split_axis=0, concat_axis=0, tiled=True)  6.2 us
    all_to_all x1, waiting for transfers between devices, per_device(): raw = lax.all_to_all(raw, KV_TP, split_axis=0, concat_axis=0, tiled=True)  3.72 us
  transfers between devices with their start and end apart: 8, of which 5 were waited for; matrix products, arithmetic and copies ran while one was open for 3% of the time, Pallas kernels for 6%

profile of v4, /device:TPU:2, one launch (start us, length us, event | category | flops | bytes accessed | tf_op | source)
XLA Modules:
  0.0 145.0 jit_solution(15272407120412571398)
XLA Ops:
  0.6 1.6 %broadcast_in_dim.14 = bf16[64,32,128]{2,1,0:T(8,128)(2,1)} broadcast(bf16[32,128]{1,0:T(8,128)(2,1)} %bitcast.76), dimensions={1,2} | broadcast | bytes 532480 | tf_op jit(solution)/shard_map/broadcast_in_dim | solution.py:28
  2.2 16.6 %all-to-all-start = ((bf16[64,32,128]{2,1,0:T(8,128)(2,1)}), bf16[64,32,128]{2,1,0:T(8,128)(2,1)S(1)}, u32[]{:S(2)}, u32[]{:S(2)}) async-start(bf16[64,32,128]{2,1,0:T(8,128)(2,1)} %broadcast_in_dim.14), calls=%async_computation | async-start | bytes 1048576 | tf_op jit(solution)/shard_map/all_to_all | solution.py:28
  18.8 2.3 %shard_map.140 = (bf16[64,2048]{1,0:T(8,128)(2,1)}, bf16[64,2048]{1,0:T(8,128)(2,1)}) custom-call(s32[1]{0:T(128)} %bitcast.1.refs_0_, bf16[16,4096]{1,0:T(8,128)(2,1)} %bitcast.70, bf16[16,4096]{1,0:T(8,128)(2,1)} %bitcast.71, bf16[16,4096]{1,0:T(8,128)(2,1)} %bitcast.72, bf16[16,4096]{1,0:T(8,128)(2,1)} %bitcast.73, f32[1,4096]{1,0:T(1,128)} %bitcast.80), custom_call_target="tpu_custom_call" | custom-call | tf_op jit(solution)/shard_map/pallas_call | solution.py:109
  21.0 2.0 %collective-permute-start = (bf16[64,2048]{1,0:T(8,128)(2,1)}, bf16[64,2048]{1,0:T(8,128)(2,1)S(1)}, u32[]{:S(2)}, u32[]{:S(2)}) collective-permute-start(bf16[64,2048]{1,0:T(8,128)(2,1)} %get-tuple-element.20), channel_id=1, source_target_pairs={{0,1},{1,0},{2,3},{3,2},{4,5},{5,4},{6,7},{7,6},{8,9},{9,8},{10,11... | collective-permute-start | bytes 786440 | tf_op jit(solution)/shard_map/ppermute | solution.py:23
  23.1 3.0 %shard_map.141 = (bf16[128,2048]{1,0:T(8,128)(2,1)}, bf16[128,2048]{1,0:T(8,128)(2,1)}) custom-call(s32[1]{0:T(128)} %bitcast.1.refs_0_, bf16[4096,128]{1,0:T(8,128)(2,1)} %refs_1_.1, f32[1,4096]{1,0:T(1,128)} %bitcast.78), custom_call_target="tpu_custom_call" | custom-call | tf_op jit(solution)/shard_map/pallas_call | solution.py:109
  26.1 2.4 %collective-permute-start.1 = (bf16[128,2048]{1,0:T(8,128)(2,1)}, bf16[128,2048]{1,0:T(8,128)(2,1)S(1)}, u32[]{:S(2)}, u32[]{:S(2)}) collective-permute-start(bf16[128,2048]{1,0:T(8,128)(2,1)} %get-tuple-element.22), channel_id=1, source_target_pairs={{0,1},{1,0},{2,3},{3,2},{4,5},{5,4},{6,7},{7,6},{8,9},{9,8},{10,11... | collective-permute-start | bytes 1572872 | tf_op jit(solution)/shard_map/ppermute | solution.py:23
  28.5 0.0 collective-permute-done
  28.5 0.0 copy-done.3
  28.6 0.0 copy-start.6
  28.6 0.0 copy-start.4
  28.6 0.8 pad_maximum_fusion.mix_ref
  29.4 0.8 collective-permute-done.1
  30.2 8.3 %all-to-all-done = bf16[64,32,128]{2,1,0:T(8,128)(2,1)S(1)} async-done(((bf16[64,32,128]{2,1,0:T(8,128)(2,1)}), bf16[64,32,128]{2,1,0:T(8,128)(2,1)S(1)}, u32[]{:S(2)}, u32[]{:S(2)}) %all-to-all-start) | async-done | bytes 524320 | tf_op jit(solution)/shard_map/all_to_all | solution.py:28
  38.5 0.8 copy-done.1
  39.3 2.2 %shard_map.142 = bf16[2,128,128]{2,1,0:T(8,128)(2,1)} custom-call(bf16[128,2048]{1,0:T(8,128)(2,1)} %pad_maximum_fusion.mix_ref, bf16[2048,128]{1,0:T(8,128)(2,1)} %bitcast.63), custom_call_target="tpu_custom_call" | custom-call | tf_op jit(solution)/shard_map/pallas_call | solution.py:159
  41.5 0.9 copy.28
  42.4 0.7 copy.29
  43.1 6.2 %all-to-all-start.1 = ((bf16[128,2,128]{2,1,0:T(2,128)(2,1)}), bf16[128,2,128]{2,1,0:T(2,128)(2,1)S(1)}, u32[]{:S(2)}, u32[]{:S(2)}) async-start(bf16[128,2,128]{2,1,0:T(2,128)(2,1)} %copy.29), calls=%async_computation.1 | async-start | bytes 131072 | tf_op jit(solution)/shard_map/all_to_all | solution.py:168
  49.3 0.0 copy-done.6
  49.4 0.0 copy-done.4
  49.4 0.0 copy-start.2
  49.4 2.1 %collective-permute-start.2 = (bf16[1024,32]{0,1:T(8,128)(2,1)S(1)}, bf16[1024,32]{0,1:T(8,128)(2,1)S(1)}, u32[]{:S(2)}, u32[]{:S(2)}) collective-permute-start(bf16[1024,32]{0,1:T(8,128)(2,1)S(1)} %get-tuple-element.42), channel_id=1, source_target_pairs={{0,1},{1,0},{2,3},{3,2},{4,5},{5,4},{6,7},{7,6},{8,9},{9,8},{10,11... | collective-permute-start | bytes 196616 | tf_op jit(solution)/shard_map/ppermute | solution.py:23
  51.5 2.8 %shard_map.143 = (bf16[2048,128]{1,0:T(8,128)(2,1)}, bf16[2048,128]{1,0:T(8,128)(2,1)}) custom-call(s32[1]{0:T(128)} %bitcast.1.refs_0_, bf16[128,4096]{1,0:T(8,128)(2,1)} %refs_1_.2), custom_call_target="tpu_custom_call" | custom-call | tf_op jit(solution)/shard_map/pallas_call | solution.py:109
  54.3 2.4 %collective-permute-start.3 = (bf16[2048,128]{1,0:T(8,128)(2,1)}, bf16[2048,128]{1,0:T(8,128)(2,1)S(1)}, u32[]{:S(2)}, u32[]{:S(2)}) collective-permute-start(bf16[2048,128]{1,0:T(8,128)(2,1)} %get-tuple-element.28), channel_id=1, source_target_pairs={{0,1},{1,0},{2,3},{3,2},{4,5},{5,4},{6,7},{7,6},{8,9},{9,8},{10,11... | collective-permute-start | bytes 1572872 | tf_op jit(solution)/shard_map/ppermute | solution.py:23
  56.7 3.7 %all-to-all-done.1 = bf16[128,2,128]{2,1,0:T(2,128)(2,1)S(1)} async-done(((bf16[128,2,128]{2,1,0:T(2,128)(2,1)}), bf16[128,2,128]{2,1,0:T(2,128)(2,1)S(1)}, u32[]{:S(2)}, u32[]{:S(2)}) %all-to-all-start.1) | async-done | bytes 65568 | tf_op jit(solution)/shard_map/all_to_all | solution.py:168
  60.4 0.1 convert_reduce_fusion.1
  60.5 0.1 slice.41
  60.6 0.1 reduce_sum.46
  60.7 0.1 copy_multiply_fusion
  60.8 0.1 copy.31
  60.9 0.1 copy.33
  61.0 0.1 div.31
  61.0 0.1 copy.35
  61.1 0.1 squeeze.22
  61.2 0.1 copy.34
  61.3 0.1 mul.111
  61.4 0.1 copy.32
  61.5 0.1 reshape.100
  61.6 0.6 multiply_add_fusion
  62.2 0.0 copy-start
  62.2 0.0 copy-start.7
  62.2 1.0 fusion.27
  63.2 0.1 multiply_reduce_fusion.1
  63.3 0.1 fusion.20
  63.4 0.0 collective-permute-done.2
  63.4 0.0 collective-permute-done.3
  63.4 0.1 broadcast_in_dim.15
  63.6 23.8 %all_to_all.25 = bf16[64,2,1024]{2,1,0:T(2,128)(2,1)S(1)} all-to-all(bf16[64,2,1024]{2,1,0:T(2,128)(2,1)S(1)} %broadcast_in_dim.15), channel_id=1, replica_groups=mesh['dp'=4,'kv_0'=8,'kv_1'=8,'tp'=2] {'kv_0','kv_1'}, dimensions={0} | all-to-all | bytes 524288 | tf_op jit(solution)/shard_map/all_to_all | solution.py:28
  87.4 0.1 reshape.96
  87.5 0.0 copy-done
  87.5 0.2 fusion.28
  87.6 2.1 %collective-permute-start.4 = (f32[32,128]{1,0:T(8,128)S(1)}, f32[32,128]{1,0:T(8,128)S(1)}, u32[]{:S(2)}, u32[]{:S(2)}) collective-permute-start(f32[32,128]{1,0:T(8,128)S(1)} %fusion.28), channel_id=1, source_target_pairs={{0,1},{1,0},{2,3},{3,2},{4,5},{5,4},{6,7},{7,6},{8,9},{9,8},{10,11... | collective-permute-start | bytes 49160 | tf_op jit(solution)/shard_map/ppermute | solution.py:23
  89.7 1.1 collective-permute-done.4
  90.9 0.2 fusion.1
  91.1 0.1 broadcast_in_dim.16
  91.2 23.3 %all_to_all.26 = bf16[64,32,128]{2,1,0:T(8,128)(2,1)S(1)} all-to-all(bf16[64,32,128]{2,1,0:T(8,128)(2,1)S(1)} %broadcast_in_dim.16), channel_id=1, replica_groups=mesh['dp'=4,'kv_0'=8,'kv_1'=8,'tp'=2] {'kv_0','kv_1'}, dimensions={0} | all-to-all | bytes 1048576 | tf_op jit(solution)/shard_map/all_to_all | solution.py:28
  114.5 0.4 fusion.5
  114.9 0.3 multiply_reduce_fusion
  115.2 1.9 %collective-permute-start.5 = (f32[257,128]{1,0:T(8,128)S(1)}, f32[257,128]{1,0:T(8,128)S(1)}, u32[]{:S(2)}, u32[]{:S(2)}) collective-permute-start(f32[257,128]{1,0:T(8,128)S(1)} %pad_maximum_fusion.1), channel_id=1, source_target_pairs={{0,1},{1,0},{2,3},{3,2},{4,5},{5,4},{6,7},{7,6},{8,9},{9,8},{10,11... | collective-permute-start | bytes 394760 | tf_op jit(solution)/shard_map/ppermute | solution.py:23
  117.1 1.3 collective-permute-done.5
  118.5 0.4 convolution_convert_fusion
  118.9 25.4 %all_to_all.27 = bf16[64,32,128]{2,1,0:T(8,128)(2,1)S(1)} all-to-all(bf16[64,32,128]{2,1,0:T(8,128)(2,1)S(1)} %bitcast.65), channel_id=1, replica_groups=mesh['dp'=4,'kv_0'=8,'kv_1'=8,'tp'=2] {'kv_0','kv_1'}, dimensions={0} | all-to-all | bytes 1048576 | tf_op jit(solution)/shard_map/all_to_all | solution.py:215
  144.3 0.1 convert_reduce_fusion
  144.4 0.6 fusion.19
  (21 shorter events, 0.2 us)
Async XLA Ops:
  2.2 36.3 %all-to-all-start = ((bf16[64,32,128]{2,1,0:T(8,128)(2,1)}), bf16[64,32,128]{2,1,0:T(8,128)(2,1)S(1)}, u32[]{:S(2)}, u32[]{:S(2)}) async-start(bf16[64,32,128]{2,1,0:T(8,128)(2,1)} %broadcast_in_dim.14), calls=%async_computation | async-start | bytes 1048576 | tf_op jit(solution)/shard_map/all_to_all | solution.py:28
  21.0 7.5 %copy-start.3 = (bf16[64,2048]{1,0:T(8,128)(2,1)S(1)}, bf16[64,2048]{1,0:T(8,128)(2,1)}, u32[]{:S(2)}) copy-start(bf16[64,2048]{1,0:T(8,128)(2,1)} %get-tuple-element.19) | copy-start | bytes 786436
  21.0 7.5 %collective-permute-start = (bf16[64,2048]{1,0:T(8,128)(2,1)}, bf16[64,2048]{1,0:T(8,128)(2,1)S(1)}, u32[]{:S(2)}, u32[]{:S(2)}) collective-permute-start(bf16[64,2048]{1,0:T(8,128)(2,1)} %get-tuple-element.20), channel_id=1, source_target_pairs={{0,1},{1,0},{2,3},{3,2},{4,5},{5,4},{6,7},{7,6},{8,9},{9,8},{10,11... | collective-permute-start | bytes 786440 | tf_op jit(solution)/shard_map/ppermute | solution.py:23
  26.1 4.1 %collective-permute-start.1 = (bf16[128,2048]{1,0:T(8,128)(2,1)}, bf16[128,2048]{1,0:T(8,128)(2,1)S(1)}, u32[]{:S(2)}, u32[]{:S(2)}) collective-permute-start(bf16[128,2048]{1,0:T(8,128)(2,1)} %get-tuple-element.22), channel_id=1, source_target_pairs={{0,1},{1,0},{2,3},{3,2},{4,5},{5,4},{6,7},{7,6},{8,9},{9,8},{10,11... | collective-permute-start | bytes 1572872 | tf_op jit(solution)/shard_map/ppermute | solution.py:23
  28.6 20.8 %copy-start.6 = (f32[1024]{0:T(1024)S(1)}, f32[1024]{0:T(1024)}, u32[]{:S(2)}) copy-start(f32[1024]{0:T(1024)} %param.18) | copy-start | bytes 12292
  28.6 20.8 %copy-start.4 = (bf16[2048,32]{0,1:T(8,128)(2,1)S(1)}, bf16[2048,32]{0,1:T(8,128)(2,1)}, u32[]{:S(2)}) copy-start(bf16[2048,32]{0,1:T(8,128)(2,1)} %param.20) | copy-start | bytes 393220
  38.5 0.8 copy-start.1
  43.1 17.3 %all-to-all-start.1 = ((bf16[128,2,128]{2,1,0:T(2,128)(2,1)}), bf16[128,2,128]{2,1,0:T(2,128)(2,1)S(1)}, u32[]{:S(2)}, u32[]{:S(2)}) async-start(bf16[128,2,128]{2,1,0:T(2,128)(2,1)} %copy.29), calls=%async_computation.1 | async-start | bytes 131072 | tf_op jit(solution)/shard_map/all_to_all | solution.py:168
  49.4 12.2 %copy-start.2 = (f32[2,8,128,128]{3,2,1,0:T(8,128)S(1)}, f32[2,8,128,128]{3,2,1,0:T(8,128)}, u32[]{:S(2)}) copy-start(f32[2,8,128,128]{3,2,1,0:T(8,128)} %param.25) | copy-start | bytes 3145732
  49.4 14.0 %collective-permute-start.2 = (bf16[1024,32]{0,1:T(8,128)(2,1)S(1)}, bf16[1024,32]{0,1:T(8,128)(2,1)S(1)}, u32[]{:S(2)}, u32[]{:S(2)}) collective-permute-start(bf16[1024,32]{0,1:T(8,128)(2,1)S(1)} %get-tuple-element.42), channel_id=1, source_target_pairs={{0,1},{1,0},{2,3},{3,2},{4,5},{5,4},{6,7},{7,6},{8,9},{9,8},{10,11... | collective-permute-start | bytes 196616 | tf_op jit(solution)/shard_map/ppermute | solution.py:23
  54.3 9.1 %collective-permute-start.3 = (bf16[2048,128]{1,0:T(8,128)(2,1)}, bf16[2048,128]{1,0:T(8,128)(2,1)S(1)}, u32[]{:S(2)}, u32[]{:S(2)}) collective-permute-start(bf16[2048,128]{1,0:T(8,128)(2,1)} %get-tuple-element.28), channel_id=1, source_target_pairs={{0,1},{1,0},{2,3},{3,2},{4,5},{5,4},{6,7},{7,6},{8,9},{9,8},{10,11... | collective-permute-start | bytes 1572872 | tf_op jit(solution)/shard_map/ppermute | solution.py:23
  62.2 25.3 %copy-start = (f32[2,8,128,128]{3,2,1,0:T(8,128)}, f32[2,8,128,128]{3,2,1,0:T(8,128)S(1)}, u32[]{:S(2)}) copy-start(f32[2,8,128,128]{3,2,1,0:T(8,128)S(1)} %multiply_add_fusion) | copy-start | bytes 3145732
  62.2 1.1 copy-start.7
  63.2 27.7 %copy-start.5 = (bf16[128,32]{0,1:T(8,128)(2,1)S(1)}, bf16[128,32]{0,1:T(8,128)(2,1)}, u32[]{:S(2)}) copy-start(bf16[128,32]{0,1:T(8,128)(2,1)} %param.13) | copy-start | bytes 24580
  87.6 26.8 %copy-start.8 = (bf16[128,2048]{1,0:T(8,128)(2,1)S(1)}, bf16[128,2048]{1,0:T(8,128)(2,1)}, u32[]{:S(2)}) copy-start(bf16[128,2048]{1,0:T(8,128)(2,1)} %get-tuple-element.34) | copy-start | bytes 1572868
  87.6 3.2 %collective-permute-start.4 = (f32[32,128]{1,0:T(8,128)S(1)}, f32[32,128]{1,0:T(8,128)S(1)}, u32[]{:S(2)}, u32[]{:S(2)}) collective-permute-start(f32[32,128]{1,0:T(8,128)S(1)} %fusion.28), channel_id=1, source_target_pairs={{0,1},{1,0},{2,3},{3,2},{4,5},{5,4},{6,7},{7,6},{8,9},{9,8},{10,11... | collective-permute-start | bytes 49160 | tf_op jit(solution)/shard_map/ppermute | solution.py:23
  114.9 3.6 %copy-start.9 = (bf16[2048,128]{1,0:T(8,128)(2,1)S(1)}, bf16[2048,128]{1,0:T(8,128)(2,1)}, u32[]{:S(2)}) copy-start(bf16[2048,128]{1,0:T(8,128)(2,1)} %get-tuple-element.32) | copy-start | bytes 1572868
  115.2 3.2 %collective-permute-start.5 = (f32[257,128]{1,0:T(8,128)S(1)}, f32[257,128]{1,0:T(8,128)S(1)}, u32[]{:S(2)}, u32[]{:S(2)}) collective-permute-start(f32[257,128]{1,0:T(8,128)S(1)} %pad_maximum_fusion.1), channel_id=1, source_target_pairs={{0,1},{1,0},{2,3},{3,2},{4,5},{5,4},{6,7},{7,6},{8,9},{9,8},{10,11... | collective-permute-start | bytes 394760 | tf_op jit(solution)/shard_map/ppermute | solution.py:23

commit v5 on v3

v5 whole, which is shorter than its diff:
```python
import jax
import jax.numpy as jnp
from jax import lax
from jax.experimental import pallas as pl
from jax.experimental.pallas import tpu as pltpu
from jax.sharding import Mesh
from jax.sharding import PartitionSpec as P


KV = ("kv_0", "kv_1")
KV_TP = ("kv_0", "kv_1", "tp")
DP_KV = ("dp", "kv_0", "kv_1")


EPSILON = 1e-06


def rms_scale(values, gain):
    return values * lax.rsqrt(jnp.mean(values * values, axis=-1, keepdims=True) + EPSILON) * gain


def swapped(x):
    return lax.ppermute(x, "tp", [(0, 1), (1, 0)])


def gathered(x):
    chips = lax.axis_size(KV)
    return lax.all_to_all(jnp.broadcast_to(x[None], (chips, *x.shape)), KV, 0, 0, tiled=True)


def contracted(left, right, dims):
    return lax.dot_general(
        left, right, ((dims[:1], dims[1:]), ((), ())), preferred_element_type=jnp.float32
    )


def square_sums(x):
    values = x.astype(jnp.float32)
    return jnp.sum(values * values, axis=0, keepdims=True)


CHUNK = 256


def selection(core, share):
    source = lax.broadcasted_iota(jnp.int32, (CHUNK, CHUNK // 2), 0)
    target = lax.broadcasted_iota(jnp.int32, (CHUNK, CHUNK // 2), 1)
    wanted = (target // share) * (2 * share) + core * share + target % share
    return jnp.where(source == wanted, 1.0, 0.0).astype(jnp.bfloat16)


def split_kernel(
    share,
    core_ref,
    query_ref,
    forget_ref,
    input_ref,
    gate_ref,
    out_ref,
    up_ref,
    down_ref,
    mix_gain_ref,
    ffn_gain_ref,
    mine_ref,
    other_ref,
):
    core = core_ref[0]
    half = CHUNK // 2
    columns = query_ref.shape[0]
    hidden = down_ref.shape[0]
    span = out_ref.shape[1] // 2
    lines = out_ref.shape[0] // 2
    for ref, index in ((mine_ref, core), (other_ref, 1 - core)):
        chosen = selection(index, share)
        for chunk in range(up_ref.shape[0] // CHUNK):
            source = pl.ds(chunk * CHUNK, CHUNK)
            parts = [
                part[:, source].astype(jnp.float32) * mix_gain_ref[:, source]
                for part in (query_ref, forget_ref, input_ref, gate_ref)
            ]
            parts.append(up_ref[source, :].astype(jnp.float32).T * ffn_gain_ref[:, source])
            rows = jnp.concatenate([part.astype(jnp.bfloat16) for part in parts], axis=0)
            rows = jnp.concatenate([rows, down_ref[:, source]], axis=0)
            ref[: 4 * columns + 2 * hidden, pl.ds(chunk * half, half)] = jnp.dot(
                rows, chosen, preferred_element_type=jnp.float32
            ).astype(jnp.bfloat16)
        start = pl.multiple_of(index * span, span)
        for piece in range(2):
            ref[4 * columns + 2 * hidden :, pl.ds(piece * span, span)] = out_ref[
                pl.ds(piece * lines, lines), pl.ds(start, span)
            ]


def split_weights(share, *operands):
    columns, hidden = operands[0].shape[0], operands[6].shape[0]
    lines, width = operands[4].shape[0] // 2, operands[0].shape[1] // 2
    core = lax.axis_index("tp").astype(jnp.int32).reshape(1)
    memory = pl.BlockSpec(memory_space=pltpu.VMEM)
    shape = jax.ShapeDtypeStruct((4 * columns + 2 * hidden + lines, width), jnp.bfloat16)
    return pl.pallas_call(
        lambda *refs: split_kernel(share, *refs),
        out_shape=[shape] * 2,
        in_specs=[pl.BlockSpec(memory_space=pltpu.SMEM)] + [memory] * len(operands),
        out_specs=[memory] * 2,
    )(core, *operands)


def per_device(
    tokens,
    w_query,
    w_forget,
    w_input,
    w_output_gate,
    gate_floor,
    head_gain,
    w_out,
    mix_gain,
    ffn_gain,
    w_up,
    w_down,
    state,
):
    chips = lax.axis_size(KV)
    cores = lax.axis_size("tp")
    rows, share = tokens.shape
    width = chips * cores * share
    seq_local, heads_local, head_size, _ = state.shape
    tokens_t = tokens.T
    columns = w_query.shape[2]
    hidden_local = w_up.shape[1]

    tp = lax.axis_index("tp")

    token_half = gathered(tokens_t).reshape(chips * share, rows)
    mine, other = split_weights(
        share,
        *[w[:, 0, :].T for w in (w_query, w_forget, w_input, w_output_gate)],
        w_out.T,
        w_up,
        w_down,
        mix_gain[None, :],
        ffn_gain[None, :],
    )
    mine, lent = lax.optimization_barrier((mine, swapped(other)))
    cuts = (0, 4 * columns, 4 * columns + hidden_local, 4 * columns + 2 * hidden_local)
    (own_down, lent_down), (own_out, lent_out) = [
        [both[start:end] for both in (mine, lent)]
        for start, end in zip(cuts[2:], (cuts[3], mine.shape[0]))
    ]
    own_out, lent_out = [
        jnp.concatenate([both[:, : both.shape[1] // 2], both[:, both.shape[1] // 2 :]], axis=0)
        for both in (own_out, lent_out)
    ]
    down_both = jnp.concatenate([own_down, lent_down], axis=0)
    mine, lent, own_out, lent_out, down_both = lax.optimization_barrier(
        (mine, lent, own_out, lent_out, down_both)
    )
    (own_mix, lent_mix), (own_up, lent_up) = [
        [both[start:end] for both in (mine, lent)] for start, end in zip(cuts[:2], cuts[1:3])
    ]
    sums = square_sums(token_half)
    high = sums.astype(jnp.bfloat16).astype(jnp.float32)
    place = lax.broadcasted_iota(jnp.int32, (128 - 4 * columns, rows), 0)
    extra = jnp.where(place == 0, high, jnp.where(place == 1, sums - high, 0.0))
    own = contracted(own_mix, token_half, (1, 0))
    theirs = contracted(lent_mix, token_half, (1, 0))
    first, second = jnp.where(tp == 0, own, theirs), jnp.where(tp == 0, theirs, own)
    raw = jnp.stack(
        [jnp.concatenate([part, extra], axis=0).T for part in (first, second)]
    ).astype(jnp.bfloat16)
    raw = raw.reshape(cores * chips, seq_local, 128)
    raw = lax.all_to_all(raw, ("tp", *KV), split_axis=0, concat_axis=0, tiled=True)
    raw = raw.reshape(cores, chips, seq_local, 128).astype(jnp.float32).sum(axis=0)
    sums = raw[0, :, 4 * columns : 4 * columns + 2].sum(axis=1)
    scale = lax.rsqrt(sums / width + EPSILON)
    raw = raw[:, :, : 4 * columns] * scale[None, :, None]
    raw = raw.reshape(chips, seq_local, 4, columns).transpose(2, 1, 0, 3)
    raw = raw.reshape(4, seq_local, heads_local, head_size)
    query_vec = raw[0] * head_size ** (-0.5)
    floor_heads = gate_floor.reshape(heads_local, head_size)
    forget_gate = floor_heads + (1.0 - floor_heads) * jax.nn.sigmoid(raw[1])
    input_vec = raw[2]
    gate_vec = raw[3]
    new_state = (
        forget_gate[..., None] * state + (1.0 - forget_gate)[..., None] * input_vec[:, :, None, :]
    )
    head_out = jnp.einsum("bhk,bhkv->bhv", query_vec, new_state, precision=lax.Precision.HIGHEST)
    branch = rms_scale(head_out, head_gain) * jax.nn.silu(gate_vec)
    branch = branch.reshape(seq_local, heads_local * head_size).astype(jnp.bfloat16)

    branch_half = gathered(branch).reshape(rows, heads_local * head_size)
    theirs = swapped(contracted(lent_out, branch_half, (1, 1)))
    projected = contracted(own_out, branch_half, (1, 1)) + theirs
    residual = (tokens_t.astype(jnp.float32) + projected).astype(jnp.bfloat16)

    residual_half = gathered(residual).reshape(chips * share, rows)
    partial = jnp.concatenate(
        [contracted(up, residual_half, (1, 0)) for up in (own_up, lent_up)], axis=0
    )
    sums = square_sums(residual_half)
    arrived = swapped(jnp.concatenate([partial, sums], axis=0))
    upward = partial + jnp.concatenate(
        [arrived[hidden_local : 2 * hidden_local], arrived[:hidden_local]], axis=0
    )
    scale = lax.rsqrt((sums + arrived[-1:]) / width + EPSILON)
    hidden = jnp.square(jax.nn.relu(upward * scale)).astype(jnp.bfloat16)

    terms = contracted(down_both, hidden, (0, 0)).astype(jnp.bfloat16)
    terms = lax.all_to_all(
        terms.reshape(chips, share, rows), KV, split_axis=0, concat_axis=0, tiled=True
    )
    summed = terms.astype(jnp.float32).sum(axis=0)
    mixed = (residual.astype(jnp.float32) + summed).astype(jnp.bfloat16).T
    return (mixed, new_state)


def solution(mesh):
    torus = Mesh(
        mesh.devices.reshape(mesh.shape["dp"], 8, 8, mesh.shape["tp"]), ("dp", "kv_0", "kv_1", "tp")
    )
    placed = (
        P("dp", KV_TP),
        P(None, "tp", KV),
        P(None, "tp", KV),
        P(None, "tp", KV),
        P(None, "tp", KV),
        P("tp"),
        P(),
        P(None, KV_TP),
        P(),
        P(),
        P(None, KV_TP),
        P(KV_TP, None),
        P(DP_KV, "tp", None, None),
    )

    return jax.shard_map(
        per_device,
        mesh=torus,
        in_specs=placed,
        out_specs=(P("dp", KV_TP), P(DP_KV, "tp", None, None)),
        check_vma=False,
    )
```

time: 146 us -> 144 us (0.986)
  blocking collectives: 50.3 us -> 67.6 us
  starting transfers between devices: 40.8 us -> 28.6 us
  waiting for transfers between devices: 36.6 us -> 27.3 us
  matrix products: 2.63 us -> 5.96 us
  Pallas kernels: 8.05 us -> 4.9 us
  local copies, waits for them, and re-layouts: 4.17 us -> 5.74 us
    all_to_all x1 -> x2, blocking collectives: 25.4 us -> 42.3 us  [gathered(): lax.all_to_all(jnp.broadcast_to(x[None], (chips, *x.shape)), KV, 0, 0, ti...]
    all_to_all x2 -> x1, waiting for transfers between devices: 22.4 us -> 12.9 us  [gathered(): lax.all_to_all(jnp.broadcast_to(x[None], (chips, *x.shape)), KV, 0, 0, ti...]
    ppermute x7 -> x3, starting transfers between devices: 14.7 us -> 5.77 us  [swapped(): return lax.ppermute(x, 'tp', [(0, 1), (1, 0)])]
    all_to_all x2 -> x1, starting transfers between devices: 21.2 us -> 16.6 us  [gathered(): lax.all_to_all(jnp.broadcast_to(x[None], (chips, *x.shape)), KV, 0, 0, ti...]
    dot_general x6 -> x7, matrix products: 1.65 us -> 4.98 us  [contracted(): lax.dot_general(left, right, ((dims[:1], dims[1:]), ((), ())), preferred_...]
    pallas_call x3 -> x1, Pallas kernels: 8.05 us -> 4.9 us  [split_weights(): pl.pallas_call(lambda *refs: split_kernel(share, *refs), out_shape=[shape...]
    slice x0 -> x3, local copies, waits for them, and re-layouts: none -> 2.28 us  [the longest x2 1.5 us: per_device(): both[start:end]]
  transfers between devices with their start and end apart: 10 -> 5, of which waited for: 5 -> 4; matrix products, arithmetic and copies ran while one was open for 3% -> 0% of each run, Pallas kernels for 6% -> 3%
where the time goes in v5:
time: 144 us
  blocking collectives  67.6 us (47%)
  starting transfers between devices  28.6 us (20%)
  waiting for transfers between devices  27.3 us (19%)
  matrix products  5.96 us (4%)
  local copies, waits for them, and re-layouts  5.74 us (4%)
  Pallas kernels  4.9 us (3%)
  other arithmetic  2.67 us (2%)
    all_to_all x2, blocking collectives, gathered(): lax.all_to_all(jnp.broadcast_to(x[None], (chips, *x.shape)), KV, 0, 0, ti...  42.3 us
    all_to_all x1, blocking collectives, per_device(): lax.all_to_all(terms.reshape(chips, share, rows), KV, split_axis=0, conca...  25.4 us
    all_to_all x1, starting transfers between devices, gathered(): lax.all_to_all(jnp.broadcast_to(x[None], (chips, *x.shape)), KV, 0, 0, ti...  16.6 us
    all_to_all x1, waiting for transfers between devices, gathered(): lax.all_to_all(jnp.broadcast_to(x[None], (chips, *x.shape)), KV, 0, 0, ti...  12.9 us
    all_to_all x1, waiting for transfers between devices, per_device(): lax.all_to_all(raw, ('tp', *KV), split_axis=0, concat_axis=0, tiled=True)  12 us
    all_to_all x1, starting transfers between devices, per_device(): lax.all_to_all(raw, ('tp', *KV), split_axis=0, concat_axis=0, tiled=True)  6.2 us
    ppermute x3, starting transfers between devices, swapped(): return lax.ppermute(x, 'tp', [(0, 1), (1, 0)])  5.77 us
    dot_general x7, matrix products, contracted(): lax.dot_general(left, right, ((dims[:1], dims[1:]), ((), ())), preferred_...  4.98 us
  transfers between devices with their start and end apart: 5, of which 4 were waited for; matrix products, arithmetic and copies ran while one was open for 0% of the time, Pallas kernels for 3%

profile of v5, /device:TPU:2, one launch (start us, length us, event | category | flops | bytes accessed | tf_op | source)
XLA Modules:
  0.0 143.7 jit_solution(12674607452101336706)
XLA Ops:
  0.6 1.6 %broadcast_in_dim.34 = bf16[64,32,128]{2,1,0:T(8,128)(2,1)} broadcast(bf16[32,128]{1,0:T(8,128)(2,1)} %bitcast.86), dimensions={1,2} | broadcast | bytes 532480 | tf_op jit(solution)/shard_map/broadcast_in_dim | solution.py:28
  2.2 16.6 %all-to-all-start = ((bf16[64,32,128]{2,1,0:T(8,128)(2,1)}), bf16[64,32,128]{2,1,0:T(8,128)(2,1)S(1)}, u32[]{:S(2)}, u32[]{:S(2)}) async-start(bf16[64,32,128]{2,1,0:T(8,128)(2,1)} %broadcast_in_dim.34), calls=%async_computation | async-start | bytes 1048576 | tf_op jit(solution)/shard_map/all_to_all | solution.py:28
  18.8 4.9 %shard_map.140 = (bf16[336,2048]{1,0:T(8,128)(2,1)}, bf16[336,2048]{1,0:T(8,128)(2,1)}) custom-call(s32[1]{0:T(128)} %bitcast.1.refs_0_, bf16[16,4096]{1,0:T(8,128)(2,1)} %bitcast.79, bf16[16,4096]{1,0:T(8,128)(2,1)} %bitcast.80, bf16[16,4096]{1,0:T(8,128)(2,1)} %bitcast.81, bf16[16,4096]{1,0:T(8,128)(2,1)} %bitcast.82, bf16[32,2048]{1,0:T(8,128)(2,1)} %bitcast.83, ...), custom_call_target="tpu_custom_call" | custom-call | tf_op jit(solution)/shard_map/pallas_call | solution.py:100
  23.7 1.9 %collective-permute-start = (bf16[336,2048]{1,0:T(8,128)(2,1)}, bf16[336,2048]{1,0:T(8,128)(2,1)S(1)}, u32[]{:S(2)}, u32[]{:S(2)}) collective-permute-start(bf16[336,2048]{1,0:T(8,128)(2,1)} %get-tuple-element.12), channel_id=1, source_target_pairs={{0,1},{1,0},{2,3},{3,2},{4,5},{5,4},{6,7},{7,6},{8,9},{9,8},{10,11... | collective-permute-start | bytes 4128776 | tf_op jit(solution)/shard_map/ppermute | solution.py:23
  25.6 12.9 %all-to-all-done = bf16[64,32,128]{2,1,0:T(8,128)(2,1)S(1)} async-done(((bf16[64,32,128]{2,1,0:T(8,128)(2,1)}), bf16[64,32,128]{2,1,0:T(8,128)(2,1)S(1)}, u32[]{:S(2)}, u32[]{:S(2)}) %all-to-all-start) | async-done | bytes 524320 | tf_op jit(solution)/shard_map/all_to_all | solution.py:28
  38.5 0.3 multiply_reduce_fusion.1
  38.8 0.1 select_convert_fusion.1
  38.9 0.0 collective-permute-done
  38.9 0.0 copy-start.1
  38.9 1.5 %slice.71 = bf16[128,2048]{1,0:T(8,128)(2,1)S(1)} slice(bf16[336,2048]{1,0:T(8,128)(2,1)} %get-tuple-element.16), slice={[192:320], [0:2048]} | slice | bytes 1048576 | tf_op jit(solution)/shard_map/slice | solution.py:147
  40.4 0.8 fusion.28
  41.2 0.1 pad_maximum_fusion
  41.4 0.0 copy-start.4
  41.4 0.0 copy-done.1
  41.4 0.2 fusion.6
  41.6 0.0 copy-start.2
  41.6 1.3 select_convert_fusion.2
  42.9 0.7 copy.32
  43.7 6.2 %all-to-all-start.1 = ((bf16[128,2,128]{2,1,0:T(2,128)(2,1)}), bf16[128,2,128]{2,1,0:T(2,128)(2,1)S(1)}, u32[]{:S(2)}, u32[]{:S(2)}) async-start(bf16[128,2,128]{2,1,0:T(2,128)(2,1)} %bitcast.18), calls=%async_computation.1 | async-start | bytes 131072 | tf_op jit(solution)/shard_map/all_to_all | solution.py:172
  49.9 0.0 copy-done.4
  49.9 12.0 %all-to-all-done.1 = bf16[128,2,128]{2,1,0:T(2,128)(2,1)S(1)} async-done(((bf16[128,2,128]{2,1,0:T(2,128)(2,1)}), bf16[128,2,128]{2,1,0:T(2,128)(2,1)S(1)}, u32[]{:S(2)}, u32[]{:S(2)}) %all-to-all-start.1) | async-done | bytes 65568 | tf_op jit(solution)/shard_map/all_to_all | solution.py:172
  61.8 0.1 convert_reduce_fusion.1
  61.9 0.2 slice_reduce_fusion
  62.1 0.1 copy_multiply_fusion
  62.2 0.1 copy.34
  62.3 0.1 copy.36
  62.4 0.1 div.31
  62.5 0.1 copy.38
  62.5 0.1 squeeze.22
  62.6 0.1 copy.37
  62.7 0.1 mul.110
  62.8 0.1 copy.35
  62.9 0.1 reshape.107
  63.0 0.0 copy-done.2
  63.0 0.0 copy-start.5
  63.0 0.6 multiply_add_fusion
  63.6 0.0 copy-start
  63.6 0.0 copy-start.3
  63.6 1.0 fusion.31
  64.6 0.1 multiply_reduce_fusion.2
  64.7 0.0 copy-done.5
  64.7 0.1 fusion.23
  64.8 0.1 broadcast_in_dim.60
  65.0 18.9 %all_to_all.25 = bf16[64,2,1024]{2,1,0:T(2,128)(2,1)S(1)} all-to-all(bf16[64,2,1024]{2,1,0:T(2,128)(2,1)S(1)} %broadcast_in_dim.60), channel_id=1, replica_groups=mesh['dp'=4,'kv_0'=8,'kv_1'=8,'tp'=2] {'kv_0','kv_1'}, dimensions={0} | all-to-all | bytes 524288 | tf_op jit(solution)/shard_map/all_to_all | solution.py:28
  83.9 0.1 reshape.103
  84.0 0.2 fusion.32
  84.2 0.0 copy-done
  84.2 1.9 %collective-permute-start.1 = (f32[32,128]{1,0:T(8,128)S(1)}, f32[32,128]{1,0:T(8,128)S(1)}, u32[]{:S(2)}, u32[]{:S(2)}) collective-permute-start(f32[32,128]{1,0:T(8,128)S(1)} %fusion.32), channel_id=1, source_target_pairs={{0,1},{1,0},{2,3},{3,2},{4,5},{5,4},{6,7},{7,6},{8,9},{9,8},{10,11... | collective-permute-start | bytes 49160 | tf_op jit(solution)/shard_map/ppermute | solution.py:23
  86.1 1.1 collective-permute-done.1
  87.3 0.0 copy-done.3
  87.3 0.2 fusion.1
  87.5 0.1 broadcast_in_dim.61
  87.6 23.3 %all_to_all.26 = bf16[64,32,128]{2,1,0:T(8,128)(2,1)S(1)} all-to-all(bf16[64,32,128]{2,1,0:T(8,128)(2,1)S(1)} %broadcast_in_dim.61), channel_id=1, replica_groups=mesh['dp'=4,'kv_0'=8,'kv_1'=8,'tp'=2] {'kv_0','kv_1'}, dimensions={0} | all-to-all | bytes 1048576 | tf_op jit(solution)/shard_map/all_to_all | solution.py:28
  110.9 1.3 fusion.2
  112.2 1.3 fusion.4
  113.6 0.3 multiply_reduce_fusion
  113.9 1.9 %collective-permute-start.2 = (f32[257,128]{1,0:T(8,128)S(1)}, f32[257,128]{1,0:T(8,128)S(1)}, u32[]{:S(2)}, u32[]{:S(2)}) collective-permute-start(f32[257,128]{1,0:T(8,128)S(1)} %pad_maximum_fusion.1), channel_id=1, source_target_pairs={{0,1},{1,0},{2,3},{3,2},{4,5},{5,4},{6,7},{7,6},{8,9},{9,8},{10,11... | collective-permute-start | bytes 394760 | tf_op jit(solution)/shard_map/ppermute | solution.py:23
  115.8 1.3 collective-permute-done.2
  117.1 0.5 convolution_convert_fusion
  117.6 25.4 %all_to_all.27 = bf16[64,32,128]{2,1,0:T(8,128)(2,1)S(1)} all-to-all(bf16[64,32,128]{2,1,0:T(8,128)(2,1)S(1)} %bitcast.75), channel_id=1, replica_groups=mesh['dp'=4,'kv_0'=8,'kv_1'=8,'tp'=2] {'kv_0','kv_1'}, dimensions={0} | all-to-all | bytes 1048576 | tf_op jit(solution)/shard_map/all_to_all | solution.py:209
  143.0 0.1 convert_reduce_fusion
  143.1 0.6 fusion.22
  (17 shorter events, 0.2 us)
Async XLA Ops:
  2.2 36.3 %all-to-all-start = ((bf16[64,32,128]{2,1,0:T(8,128)(2,1)}), bf16[64,32,128]{2,1,0:T(8,128)(2,1)S(1)}, u32[]{:S(2)}, u32[]{:S(2)}) async-start(bf16[64,32,128]{2,1,0:T(8,128)(2,1)} %broadcast_in_dim.34), calls=%async_computation | async-start | bytes 1048576 | tf_op jit(solution)/shard_map/all_to_all | solution.py:28
  23.7 15.2 %collective-permute-start = (bf16[336,2048]{1,0:T(8,128)(2,1)}, bf16[336,2048]{1,0:T(8,128)(2,1)S(1)}, u32[]{:S(2)}, u32[]{:S(2)}) collective-permute-start(bf16[336,2048]{1,0:T(8,128)(2,1)} %get-tuple-element.12), channel_id=1, source_target_pairs={{0,1},{1,0},{2,3},{3,2},{4,5},{5,4},{6,7},{7,6},{8,9},{9,8},{10,11... | collective-permute-start | bytes 4128776 | tf_op jit(solution)/shard_map/ppermute | solution.py:23
  38.9 2.5 %copy-start.1 = (bf16[336,2048]{1,0:T(8,128)(2,1)}, bf16[336,2048]{1,0:T(8,128)(2,1)S(1)}, u32[]{:S(2)}) copy-start(bf16[336,2048]{1,0:T(8,128)(2,1)S(1)} %collective-permute-done) | copy-start | bytes 4128772
  41.4 8.5 %copy-start.4 = (f32[1024]{0:T(1024)S(1)}, f32[1024]{0:T(1024)}, u32[]{:S(2)}) copy-start(f32[1024]{0:T(1024)} %param.18) | copy-start | bytes 12292
  41.6 21.4 %copy-start.2 = (f32[2,8,128,128]{3,2,1,0:T(8,128)S(1)}, f32[2,8,128,128]{3,2,1,0:T(8,128)}, u32[]{:S(2)}) copy-start(f32[2,8,128,128]{3,2,1,0:T(8,128)} %param.25) | copy-start | bytes 3145732
  43.7 18.2 %all-to-all-start.1 = ((bf16[128,2,128]{2,1,0:T(2,128)(2,1)}), bf16[128,2,128]{2,1,0:T(2,128)(2,1)S(1)}, u32[]{:S(2)}, u32[]{:S(2)}) async-start(bf16[128,2,128]{2,1,0:T(2,128)(2,1)} %bitcast.18), calls=%async_computation.1 | async-start | bytes 131072 | tf_op jit(solution)/shard_map/all_to_all | solution.py:172
  63.0 1.7 %copy-start.5 = (f32[128]{0:T(128)S(1)}, f32[128]{0:T(128)}, u32[]{:S(2)}) copy-start(f32[128]{0:T(128)} %param.19) | copy-start | bytes 1540
  63.6 20.6 %copy-start = (f32[2,8,128,128]{3,2,1,0:T(8,128)}, f32[2,8,128,128]{3,2,1,0:T(8,128)S(1)}, u32[]{:S(2)}) copy-start(f32[2,8,128,128]{3,2,1,0:T(8,128)S(1)} %multiply_add_fusion) | copy-start | bytes 3145732
  63.6 23.6 %copy-start.3 = (bf16[128,32]{0,1:T(8,128)(2,1)S(1)}, bf16[128,32]{0,1:T(8,128)(2,1)}, u32[]{:S(2)}) copy-start(bf16[128,32]{0,1:T(8,128)(2,1)} %param.13) | copy-start | bytes 24580
  84.2 3.1 %collective-permute-start.1 = (f32[32,128]{1,0:T(8,128)S(1)}, f32[32,128]{1,0:T(8,128)S(1)}, u32[]{:S(2)}, u32[]{:S(2)}) collective-permute-start(f32[32,128]{1,0:T(8,128)S(1)} %fusion.32), channel_id=1, source_target_pairs={{0,1},{1,0},{2,3},{3,2},{4,5},{5,4},{6,7},{7,6},{8,9},{9,8},{10,11... | collective-permute-start | bytes 49160 | tf_op jit(solution)/shard_map/ppermute | solution.py:23
  113.9 3.2 %collective-permute-start.2 = (f32[257,128]{1,0:T(8,128)S(1)}, f32[257,128]{1,0:T(8,128)S(1)}, u32[]{:S(2)}, u32[]{:S(2)}) collective-permute-start(f32[257,128]{1,0:T(8,128)S(1)} %pad_maximum_fusion.1), channel_id=1, source_target_pairs={{0,1},{1,0},{2,3},{3,2},{4,5},{5,4},{6,7},{7,6},{8,9},{9,8},{10,11... | collective-permute-start | bytes 394760 | tf_op jit(solution)/shard_map/ppermute | solution.py:23

commit v6 on v5

--- a/solution.py
+++ b/solution.py
@@ -61,7 +61,10 @@
     down_ref,
     mix_gain_ref,
     ffn_gain_ref,
-    mine_ref,
+    mix_ref,
+    own_up_ref,
+    own_down_ref,
+    own_out_ref,
     other_ref,
 ):
     core = core_ref[0]
@@ -70,10 +73,12 @@
     hidden = down_ref.shape[0]
     span = out_ref.shape[1] // 2
     lines = out_ref.shape[0] // 2
-    for ref, index in ((mine_ref, core), (other_ref, 1 - core)):
+    first, second = 4 * columns, 4 * columns + hidden
+    for own, index in ((True, core), (False, 1 - core)):
         chosen = selection(index, share)
         for chunk in range(up_ref.shape[0] // CHUNK):
             source = pl.ds(chunk * CHUNK, CHUNK)
+            target = pl.ds(chunk * half, half)
             parts = [
                 part[:, source].astype(jnp.float32) * mix_gain_ref[:, source]
                 for part in (query_ref, forget_ref, input_ref, gate_ref)
@@ -81,27 +86,41 @@
             parts.append(up_ref[source, :].astype(jnp.float32).T * ffn_gain_ref[:, source])
             rows = jnp.concatenate([part.astype(jnp.bfloat16) for part in parts], axis=0)
             rows = jnp.concatenate([rows, down_ref[:, source]], axis=0)
-            ref[: 4 * columns + 2 * hidden, pl.ds(chunk * half, half)] = jnp.dot(
-                rows, chosen, preferred_element_type=jnp.float32
-            ).astype(jnp.bfloat16)
+            picked = jnp.dot(rows, chosen, preferred_element_type=jnp.float32)
+            picked = picked.astype(jnp.bfloat16)
+            if own:
+                mix_ref[:, target] = picked[:first]
+                own_up_ref[:, target] = picked[first:second]
+                own_down_ref[:, target] = picked[second:]
+            else:
+                other_ref[: second + hidden, target] = picked
         start = pl.multiple_of(index * span, span)
-        for piece in range(2):
-            ref[4 * columns + 2 * hidden :, pl.ds(piece * span, span)] = out_ref[
-                pl.ds(piece * lines, lines), pl.ds(start, span)
-            ]
+        if own:
+            own_out_ref[...] = out_ref[:, pl.ds(start, span)]
+        else:
+            for piece in range(2):
+                other_ref[second + hidden :, pl.ds(piece * span, span)] = out_ref[
+                    pl.ds(piece * lines, lines), pl.ds(start, span)
+                ]
 
 
 def split_weights(share, *operands):
     columns, hidden = operands[0].shape[0], operands[6].shape[0]
-    lines, width = operands[4].shape[0] // 2, operands[0].shape[1] // 2
+    lines, width = operands[4].shape[0], operands[0].shape[1] // 2
     core = lax.axis_index("tp").astype(jnp.int32).reshape(1)
     memory = pl.BlockSpec(memory_space=pltpu.VMEM)
-    shape = jax.ShapeDtypeStruct((4 * columns + 2 * hidden + lines, width), jnp.bfloat16)
+    shapes = (
+        (4 * columns, width),
+        (hidden, width),
+        (hidden, width),
+        (lines, operands[4].shape[1] // 2),
+        (4 * columns + 2 * hidden + lines // 2, width),
+    )
     return pl.pallas_call(
         lambda *refs: split_kernel(share, *refs),
-        out_shape=[shape] * 2,
+        out_shape=[jax.ShapeDtypeStruct(shape, jnp.bfloat16) for shape in shapes],
         in_specs=[pl.BlockSpec(memory_space=pltpu.SMEM)] + [memory] * len(operands),
-        out_specs=[memory] * 2,
+        out_specs=[memory] * len(shapes),
     )(core, *operands)
 
 
@@ -132,7 +151,7 @@
     tp = lax.axis_index("tp")
 
     token_half = gathered(tokens_t).reshape(chips * share, rows)
-    mine, other = split_weights(
+    own_mix, own_up, own_down, own_out, other = split_weights(
         share,
         *[w[:, 0, :].T for w in (w_query, w_forget, w_input, w_output_gate)],
         w_out.T,
@@ -141,23 +160,16 @@
         mix_gain[None, :],
         ffn_gain[None, :],
     )
-    mine, lent = lax.optimization_barrier((mine, swapped(other)))
-    cuts = (0, 4 * columns, 4 * columns + hidden_local, 4 * columns + 2 * hidden_local)
-    (own_down, lent_down), (own_out, lent_out) = [
-        [both[start:end] for both in (mine, lent)]
-        for start, end in zip(cuts[2:], (cuts[3], mine.shape[0]))
-    ]
-    own_out, lent_out = [
-        jnp.concatenate([both[:, : both.shape[1] // 2], both[:, both.shape[1] // 2 :]], axis=0)
-        for both in (own_out, lent_out)
-    ]
-    down_both = jnp.concatenate([own_down, lent_down], axis=0)
-    mine, lent, own_out, lent_out, down_both = lax.optimization_barrier(
-        (mine, lent, own_out, lent_out, down_both)
-    )
-    (own_mix, lent_mix), (own_up, lent_up) = [
-        [both[start:end] for both in (mine, lent)] for start, end in zip(cuts[:2], cuts[1:3])
-    ]
+    lent = swapped(other)
+    first = 4 * columns
+    second, third = first + hidden_local, first + 2 * hidden_local
+    span = lent.shape[1] // 2
+    lent_out = jnp.concatenate([lent[third:, :span], lent[third:, span:]], axis=0)
+    up_both = jnp.concatenate([own_up, lent[first:second]], axis=0)
+    down_both = jnp.concatenate([own_down, lent[second:third]], axis=0)
+    lent_mix, own_mix, own_out, lent_out, up_both, down_both = lax.optimization_barrier(
+        (lent[:first], own_mix, own_out, lent_out, up_both, down_both)
+    )
     sums = square_sums(token_half)
     high = sums.astype(jnp.bfloat16).astype(jnp.float32)
     place = lax.broadcasted_iota(jnp.int32, (128 - 4 * columns, rows), 0)
@@ -170,6 +182,7 @@
     ).astype(jnp.bfloat16)
     raw = raw.reshape(cores * chips, seq_local, 128)
     raw = lax.all_to_all(raw, ("tp", *KV), split_axis=0, concat_axis=0, tiled=True)
+    raw, gate_floor, head_gain = lax.optimization_barrier((raw, gate_floor, head_gain))
     raw = raw.reshape(cores, chips, seq_local, 128).astype(jnp.float32).sum(axis=0)
     sums = raw[0, :, 4 * columns : 4 * columns + 2].sum(axis=1)
     scale = lax.rsqrt(sums / width + EPSILON)
@@ -184,7 +197,7 @@
     new_state = (
         forget_gate[..., None] * state + (1.0 - forget_gate)[..., None] * input_vec[:, :, None, :]
     )
-    head_out = jnp.einsum("bhk,bhkv->bhv", query_vec, new_state, precision=lax.Precision.HIGHEST)
+    head_out = jnp.sum(query_vec[..., None] * new_state, axis=2)
     branch = rms_scale(head_out, head_gain) * jax.nn.silu(gate_vec)
     branch = branch.reshape(seq_local, heads_local * head_size).astype(jnp.bfloat16)
 
@@ -194,9 +207,7 @@
     residual = (tokens_t.astype(jnp.float32) + projected).astype(jnp.bfloat16)
 
     residual_half = gathered(residual).reshape(chips * share, rows)
-    partial = jnp.concatenate(
-        [contracted(up, residual_half, (1, 0)) for up in (own_up, lent_up)], axis=0
-    )
+    partial = contracted(up_both, residual_half, (1, 0))
     sums = square_sums(residual_half)
     arrived = swapped(jnp.concatenate([partial, sums], axis=0))
     upward = partial + jnp.concatenate(

time: 144 us -> 140 us (0.972)
  the two profiles are of different devices: /device:TPU:2 before, /device:TPU:6 now
where the time goes in v6:
time: 140 us
  blocking collectives  85.8 us (61%)
  starting transfers between devices  22.4 us (16%)
  waiting for transfers between devices  15.7 us (11%)
  local copies, waits for them, and re-layouts  4.7 us (3%)
  Pallas kernels  4.54 us (3%)
  other arithmetic  3.9 us (3%)
  matrix products  1.73 us (1%)
    all_to_all x2, blocking collectives, gathered(): lax.all_to_all(jnp.broadcast_to(x[None], (chips, *x.shape)), KV, 0, 0, ti...  42.3 us
    all_to_all x1, blocking collectives, per_device(): lax.all_to_all(terms.reshape(chips, share, rows), KV, split_axis=0, conca...  25.4 us
    all_to_all x1, blocking collectives, per_device(): lax.all_to_all(raw, ('tp', *KV), split_axis=0, concat_axis=0, tiled=True)  18.2 us
    all_to_all x1, starting transfers between devices, gathered(): lax.all_to_all(jnp.broadcast_to(x[None], (chips, *x.shape)), KV, 0, 0, ti...  16.6 us
    all_to_all x1, waiting for transfers between devices, gathered(): lax.all_to_all(jnp.broadcast_to(x[None], (chips, *x.shape)), KV, 0, 0, ti...  13.2 us
    ppermute x3, starting transfers between devices, swapped(): return lax.ppermute(x, 'tp', [(0, 1), (1, 0)])  5.77 us
    pallas_call x1, Pallas kernels, split_weights(): pl.pallas_call(lambda *refs: split_kernel(share, *refs), out_shape=[jax.S...  4.54 us
  transfers between devices with their start and end apart: 4, of which 3 were waited for; matrix products, arithmetic and copies ran while one was open for 0% of the time, Pallas kernels for 3%

profile of v6, /device:TPU:6, one launch (start us, length us, event | category | flops | bytes accessed | tf_op | source)
XLA Modules:
  0.0 139.7 jit_solution(10488508925227454686)
XLA Ops:
  0.6 0.0 copy-start
  0.6 1.6 %broadcast_in_dim.34 = bf16[64,32,128]{2,1,0:T(8,128)(2,1)} broadcast(bf16[32,128]{1,0:T(8,128)(2,1)} %bitcast.86), dimensions={1,2} | broadcast | bytes 532480 | tf_op jit(solution)/shard_map/broadcast_in_dim | solution.py:28
  2.2 16.6 %all-to-all-start = ((bf16[64,32,128]{2,1,0:T(8,128)(2,1)}), bf16[64,32,128]{2,1,0:T(8,128)(2,1)S(1)}, u32[]{:S(2)}, u32[]{:S(2)}) async-start(bf16[64,32,128]{2,1,0:T(8,128)(2,1)} %broadcast_in_dim.34), calls=%async_computation | async-start | bytes 1048576 | tf_op jit(solution)/shard_map/all_to_all | solution.py:28
  18.8 4.5 %shard_map.140 = (bf16[64,2048]{1,0:T(8,128)(2,1)}, bf16[128,2048]{1,0:T(8,128)(2,1)}, bf16[128,2048]{1,0:T(8,128)(2,1)}, bf16[32,1024]{1,0:T(8,128)(2,1)}, bf16[336,2048]{1,0:T(8,128)(2,1)}) custom-call(s32[1]{0:T(128)} %bitcast.1.refs_0_, bf16[16,4096]{1,0:T(8,128)(2,1)} %bitcast.81, bf16[16,4096]{1,0:T(8,128)(2,1)} %bitcast.82, ...), custom_call_target="tpu_custom_call" | custom-call | tf_op jit(solution)/shard_map/pallas_call | solution.py:119
  23.3 1.9 %collective-permute-start = (bf16[336,2048]{1,0:T(8,128)(2,1)}, bf16[336,2048]{1,0:T(8,128)(2,1)S(1)}, u32[]{:S(2)}, u32[]{:S(2)}) collective-permute-start(bf16[336,2048]{1,0:T(8,128)(2,1)} %get-tuple-element.16), channel_id=1, source_target_pairs={{0,1},{1,0},{2,3},{3,2},{4,5},{5,4},{6,7},{7,6},{8,9},{9,8},{10,11... | collective-permute-start | bytes 4128776 | tf_op jit(solution)/shard_map/ppermute | solution.py:23
  25.3 0.0 copy-start.3
  25.3 13.2 %all-to-all-done = bf16[64,32,128]{2,1,0:T(8,128)(2,1)S(1)} async-done(((bf16[64,32,128]{2,1,0:T(8,128)(2,1)}), bf16[64,32,128]{2,1,0:T(8,128)(2,1)S(1)}, u32[]{:S(2)}, u32[]{:S(2)}) %all-to-all-start) | async-done | bytes 524320 | tf_op jit(solution)/shard_map/all_to_all | solution.py:28
  38.5 0.0 copy-start.4
  38.5 0.3 multiply_reduce_fusion.2
  38.8 0.1 select_convert_fusion.1
  38.9 0.0 collective-permute-done
  38.9 0.0 copy-start.1
  39.0 0.1 fusion.21
  39.0 1.0 copy-done.1
  40.0 0.0 copy-done.3
  40.0 0.0 copy-done.4
  40.0 0.0 slice-start
  40.0 0.2 pad_maximum_fusion
  40.2 0.0 copy-start.5
  40.2 0.8 slice-done
  41.0 0.2 fusion.24
  41.2 0.0 copy-done.5
  41.2 0.0 copy-start.8
  41.3 0.2 select_convert_fusion.2
  41.5 0.0 copy-start.2
  41.5 0.1 copy.32
  41.7 18.2 %all_to_all.25 = bf16[128,2,128]{2,1,0:T(2,128)(2,1)S(1)} all-to-all(bf16[128,2,128]{2,1,0:T(2,128)(2,1)S(1)} %bitcast.79), channel_id=1, replica_groups=mesh['dp'=4,'kv_0'=8,'kv_1'=8,'tp'=2] {'tp','kv_0','kv_1'}, dimensions={0} | all-to-all | bytes 131072 | tf_op jit(solution)/shard_map/all_to_all | solution.py:184
  59.8 0.1 convert_reduce_fusion.1
  59.9 0.2 slice_reduce_fusion
  60.1 0.1 copy_multiply_fusion
  60.2 0.1 copy.34
  60.3 0.1 copy.38
  60.4 0.1 squeeze.22
  60.5 0.1 copy.35
  60.6 0.1 mul.143
  60.7 0.1 copy.37
  60.7 0.1 mul.150
  60.8 0.1 copy.36
  60.9 0.1 div.36
  61.0 0.0 copy-done.8
  61.0 0.0 copy-done.2
  61.0 1.8 %multiply_reduce_fusion.1 = (f32[2,8,128]{2,1,0:T(8,128)S(1)}, f32[2,8,128,128]{3,2,1,0:T(8,128)}) fusion(f32[2,8,128]{2,1,0:T(8,128)S(1)} %mul.143, f32[2,8,128]{2,1,0:T(8,128)S(1)} %mul.150, f32[2,8,128]{2,1,0:T(8,128)S(1)} %get-tuple-element.32, f32[2,8,128,128]{3,2,1,0:T(8,128)S(1)} %copy-done.2, f32[2,8,128]{2,1,0:T(8,128)S(1)} %get-tuple-element.33), kind=kLoop, calls=%fused_computation.8 | loop fusion | flops 1308672 | bytes 2138112 | tf_op jit(solution)/shard_map/reduce_sum | solution.py:200
  62.8 0.1 multiply_reduce_fusion.3
  62.9 0.1 multiply_bitcast_fusion
  63.0 0.0 copy-done
  63.0 0.1 broadcast_in_dim.61
  63.2 18.9 %all_to_all.26 = bf16[64,2,1024]{2,1,0:T(2,128)(2,1)S(1)} all-to-all(bf16[64,2,1024]{2,1,0:T(2,128)(2,1)S(1)} %broadcast_in_dim.61), channel_id=1, replica_groups=mesh['dp'=4,'kv_0'=8,'kv_1'=8,'tp'=2] {'kv_0','kv_1'}, dimensions={0} | all-to-all | bytes 524288 | tf_op jit(solution)/shard_map/all_to_all | solution.py:28
  82.1 0.1 reshape.148
  82.2 0.2 fusion.25
  82.4 1.9 %collective-permute-start.1 = (f32[32,128]{1,0:T(8,128)S(1)}, f32[32,128]{1,0:T(8,128)S(1)}, u32[]{:S(2)}, u32[]{:S(2)}) collective-permute-start(f32[32,128]{1,0:T(8,128)S(1)} %fusion.25), channel_id=1, source_target_pairs={{0,1},{1,0},{2,3},{3,2},{4,5},{5,4},{6,7},{7,6},{8,9},{9,8},{10,11... | collective-permute-start | bytes 49160 | tf_op jit(solution)/shard_map/ppermute | solution.py:23
  84.3 1.1 collective-permute-done.1
  85.5 0.0 copy-done.6
  85.5 0.0 copy-done.7
  85.5 0.2 fusion.1
  85.7 0.1 broadcast_in_dim.62
  85.8 23.3 %all_to_all.27 = bf16[64,32,128]{2,1,0:T(8,128)(2,1)S(1)} all-to-all(bf16[64,32,128]{2,1,0:T(8,128)(2,1)S(1)} %broadcast_in_dim.62), channel_id=1, replica_groups=mesh['dp'=4,'kv_0'=8,'kv_1'=8,'tp'=2] {'kv_0','kv_1'}, dimensions={0} | all-to-all | bytes 1048576 | tf_op jit(solution)/shard_map/all_to_all | solution.py:28
  109.1 0.4 fusion.26
  109.5 0.3 multiply_reduce_fusion
  109.8 1.9 %collective-permute-start.2 = (f32[257,128]{1,0:T(8,128)S(1)}, f32[257,128]{1,0:T(8,128)S(1)}, u32[]{:S(2)}, u32[]{:S(2)}) collective-permute-start(f32[257,128]{1,0:T(8,128)S(1)} %pad_maximum_fusion.2), channel_id=1, source_target_pairs={{0,1},{1,0},{2,3},{3,2},{4,5},{5,4},{6,7},{7,6},{8,9},{9,8},{10,11... | collective-permute-start | bytes 394760 | tf_op jit(solution)/shard_map/ppermute | solution.py:23
  111.7 1.3 collective-permute-done.2
  113.1 0.5 convolution_convert_fusion
  113.6 25.4 %all_to_all.28 = bf16[64,32,128]{2,1,0:T(8,128)(2,1)S(1)} all-to-all(bf16[64,32,128]{2,1,0:T(8,128)(2,1)S(1)} %bitcast.76), channel_id=1, replica_groups=mesh['dp'=4,'kv_0'=8,'kv_1'=8,'tp'=2] {'kv_0','kv_1'}, dimensions={0} | all-to-all | bytes 1048576 | tf_op jit(solution)/shard_map/all_to_all | solution.py:220
  139.0 0.1 convert_reduce_fusion
  139.1 0.6 fusion.15
  (19 shorter events, 0.2 us)
Async XLA Ops:
  0.6 62.3 %copy-start = (f32[128]{0:T(128)S(1)}, f32[128]{0:T(128)}, u32[]{:S(2)}) copy-start(f32[128]{0:T(128)} %param.19) | copy-start | bytes 1540
  2.2 36.3 %all-to-all-start = ((bf16[64,32,128]{2,1,0:T(8,128)(2,1)}), bf16[64,32,128]{2,1,0:T(8,128)(2,1)S(1)}, u32[]{:S(2)}, u32[]{:S(2)}) async-start(bf16[64,32,128]{2,1,0:T(8,128)(2,1)} %broadcast_in_dim.34), calls=%async_computation | async-start | bytes 1048576 | tf_op jit(solution)/shard_map/all_to_all | solution.py:28
  23.3 15.6 %collective-permute-start = (bf16[336,2048]{1,0:T(8,128)(2,1)}, bf16[336,2048]{1,0:T(8,128)(2,1)S(1)}, u32[]{:S(2)}, u32[]{:S(2)}) collective-permute-start(bf16[336,2048]{1,0:T(8,128)(2,1)} %get-tuple-element.16), channel_id=1, source_target_pairs={{0,1},{1,0},{2,3},{3,2},{4,5},{5,4},{6,7},{7,6},{8,9},{9,8},{10,11... | collective-permute-start | bytes 4128776 | tf_op jit(solution)/shard_map/ppermute | solution.py:23
  25.3 14.8 %copy-start.3 = (bf16[128,2048]{1,0:T(8,128)(2,1)S(1)}, bf16[128,2048]{1,0:T(8,128)(2,1)}, u32[]{:S(2)}) copy-start(bf16[128,2048]{1,0:T(8,128)(2,1)} %get-tuple-element.19) | copy-start | bytes 1572868
  38.5 1.5 %copy-start.4 = (bf16[128,2048]{1,0:T(8,128)(2,1)S(1)}, bf16[128,2048]{1,0:T(8,128)(2,1)}, u32[]{:S(2)}) copy-start(bf16[128,2048]{1,0:T(8,128)(2,1)} %get-tuple-element.20) | copy-start | bytes 1572868
  38.9 1.1 copy-start.1
  40.0 1.0 slice-start
  40.2 1.0 copy-start.5
  41.2 19.7 %copy-start.8 = (f32[1024]{0:T(1024)S(1)}, f32[1024]{0:T(1024)}, u32[]{:S(2)}) copy-start(f32[1024]{0:T(1024)} %param.18) | copy-start | bytes 12292
  41.5 19.5 %copy-start.2 = (f32[2,8,128,128]{3,2,1,0:T(8,128)S(1)}, f32[2,8,128,128]{3,2,1,0:T(8,128)}, u32[]{:S(2)}) copy-start(f32[2,8,128,128]{3,2,1,0:T(8,128)} %param.25) | copy-start | bytes 3145732
  62.8 22.7 %copy-start.6 = (bf16[32,1024]{1,0:T(8,128)(2,1)S(1)}, bf16[32,1024]{1,0:T(8,128)(2,1)}, u32[]{:S(2)}) copy-start(bf16[32,1024]{1,0:T(8,128)(2,1)} %get-tuple-element.21) | copy-start | bytes 196612
  62.8 22.7 %copy-start.7 = (bf16[128,32]{0,1:T(8,128)(2,1)S(1)}, bf16[128,32]{0,1:T(8,128)(2,1)}, u32[]{:S(2)}) copy-start(bf16[128,32]{0,1:T(8,128)(2,1)} %param.13) | copy-start | bytes 24580
  82.4 3.1 %collective-permute-start.1 = (f32[32,128]{1,0:T(8,128)S(1)}, f32[32,128]{1,0:T(8,128)S(1)}, u32[]{:S(2)}, u32[]{:S(2)}) collective-permute-start(f32[32,128]{1,0:T(8,128)S(1)} %fusion.25), channel_id=1, source_target_pairs={{0,1},{1,0},{2,3},{3,2},{4,5},{5,4},{6,7},{7,6},{8,9},{9,8},{10,11... | collective-permute-start | bytes 49160 | tf_op jit(solution)/shard_map/ppermute | solution.py:23
  109.8 3.2 %collective-permute-start.2 = (f32[257,128]{1,0:T(8,128)S(1)}, f32[257,128]{1,0:T(8,128)S(1)}, u32[]{:S(2)}, u32[]{:S(2)}) collective-permute-start(f32[257,128]{1,0:T(8,128)S(1)} %pad_maximum_fusion.2), channel_id=1, source_target_pairs={{0,1},{1,0},{2,3},{3,2},{4,5},{5,4},{6,7},{7,6},{8,9},{9,8},{10,11... | collective-permute-start | bytes 394760 | tf_op jit(solution)/shard_map/ppermute | solution.py:23

commit v7 on v6

--- a/solution.py
+++ b/solution.py
@@ -7,9 +7,11 @@
 from jax.sharding import PartitionSpec as P
 
 
-KV = ("kv_0", "kv_1")
-KV_TP = ("kv_0", "kv_1", "tp")
-DP_KV = ("dp", "kv_0", "kv_1")
+KV = ("kv_far", "kv_pair", "kv_near")
+PAIR = "kv_pair"
+SIDE = ("kv_far", "kv_near")
+KV_TP = (*KV, "tp")
+DP_KV = ("dp", *KV)
 
 
 EPSILON = 1e-06
@@ -23,9 +25,15 @@
     return lax.ppermute(x, "tp", [(0, 1), (1, 0)])
 
 
-def gathered(x):
-    chips = lax.axis_size(KV)
-    return lax.all_to_all(jnp.broadcast_to(x[None], (chips, *x.shape)), KV, 0, 0, tiled=True)
+def crossed(x, flip):
+    places = [(pair, core) for pair in range(2) for core in range(2)]
+    moves = [(2 * p + c, 2 * (1 - p) + (1 - c if flip else c)) for p, c in places]
+    return lax.ppermute(x, (PAIR, "tp"), moves)
+
+
+def gathered(x, axes=KV):
+    chips = lax.axis_size(axes)
+    return lax.all_to_all(jnp.broadcast_to(x[None], (chips, *x.shape)), axes, 0, 0, tiled=True)
 
 
 def contracted(left, right, dims):
@@ -62,44 +70,52 @@
     mix_gain_ref,
     ffn_gain_ref,
     mix_ref,
-    own_up_ref,
-    own_down_ref,
+    own_ref,
     own_out_ref,
+    near_ref,
+    cross_ref,
     other_ref,
 ):
-    core = core_ref[0]
+    core, pair = core_ref[0], core_ref[1]
     half = CHUNK // 2
     columns = query_ref.shape[0]
     hidden = down_ref.shape[0]
     span = out_ref.shape[1] // 2
     lines = out_ref.shape[0] // 2
-    first, second = 4 * columns, 4 * columns + hidden
+    first = 4 * columns
+    chunks = up_ref.shape[0] // CHUNK
     for own, index in ((True, core), (False, 1 - core)):
         chosen = selection(index, share)
-        for chunk in range(up_ref.shape[0] // CHUNK):
+        for chunk in range(chunks):
             source = pl.ds(chunk * CHUNK, CHUNK)
-            target = pl.ds(chunk * half, half)
             parts = [
                 part[:, source].astype(jnp.float32) * mix_gain_ref[:, source]
                 for part in (query_ref, forget_ref, input_ref, gate_ref)
             ]
-            parts.append(up_ref[source, :].astype(jnp.float32).T * ffn_gain_ref[:, source])
             rows = jnp.concatenate([part.astype(jnp.bfloat16) for part in parts], axis=0)
-            rows = jnp.concatenate([rows, down_ref[:, source]], axis=0)
             picked = jnp.dot(rows, chosen, preferred_element_type=jnp.float32)
-            picked = picked.astype(jnp.bfloat16)
-            if own:
-                mix_ref[:, target] = picked[:first]
-                own_up_ref[:, target] = picked[first:second]
-                own_down_ref[:, target] = picked[second:]
-            else:
-                other_ref[: second + hidden, target] = picked
+            target = mix_ref if own else other_ref
+            target[:first, pl.ds(chunk * half, half)] = picked.astype(jnp.bfloat16)
+        for side, ref in ((pair, own_ref if own else other_ref), (1 - pair, near_ref if own else cross_ref)):
+            offset = 0 if own or ref is cross_ref else first
+            for chunk in range(chunks // 2):
+                place = 4 * (chunk // 2) + 2 * side + chunk % 2
+                source = pl.ds(pl.multiple_of(place * CHUNK, CHUNK), CHUNK)
+                raised = up_ref[source, :].astype(jnp.float32).T * ffn_gain_ref[:, source]
+                rows = jnp.concatenate(
+                    [raised.astype(jnp.bfloat16), down_ref[:, source]], axis=0
+                )
+                picked = jnp.dot(rows, chosen, preferred_element_type=jnp.float32)
+                picked = picked.astype(jnp.bfloat16)
+                for part in range(2):
+                    lanes = pl.ds(part * chunks // 2 * half + chunk * half, half)
+                    ref[offset : offset + hidden, lanes] = picked[part * hidden : (part + 1) * hidden]
         start = pl.multiple_of(index * span, span)
         if own:
             own_out_ref[...] = out_ref[:, pl.ds(start, span)]
         else:
             for piece in range(2):
-                other_ref[second + hidden :, pl.ds(piece * span, span)] = out_ref[
+                other_ref[first + hidden :, pl.ds(piece * span, span)] = out_ref[
                     pl.ds(piece * lines, lines), pl.ds(start, span)
                 ]
 
@@ -107,14 +123,15 @@
 def split_weights(share, *operands):
     columns, hidden = operands[0].shape[0], operands[6].shape[0]
     lines, width = operands[4].shape[0], operands[0].shape[1] // 2
-    core = lax.axis_index("tp").astype(jnp.int32).reshape(1)
+    core = jnp.stack([lax.axis_index("tp"), lax.axis_index(PAIR)]).astype(jnp.int32)
     memory = pl.BlockSpec(memory_space=pltpu.VMEM)
     shapes = (
         (4 * columns, width),
         (hidden, width),
+        (lines, operands[4].shape[1] // 2),
         (hidden, width),
-        (lines, operands[4].shape[1] // 2),
-        (4 * columns + 2 * hidden + lines // 2, width),
+        (hidden, width),
+        (4 * columns + hidden + lines // 2, width),
     )
     return pl.pallas_call(
         lambda *refs: split_kernel(share, *refs),
@@ -151,7 +168,7 @@
     tp = lax.axis_index("tp")
 
     token_half = gathered(tokens_t).reshape(chips * share, rows)
-    own_mix, own_up, own_down, own_out, other = split_weights(
+    own_mix, own_mixer, own_out, near, cross, other = split_weights(
         share,
         *[w[:, 0, :].T for w in (w_query, w_forget, w_input, w_output_gate)],
         w_out.T,
@@ -162,13 +179,12 @@
     )
     lent = swapped(other)
     first = 4 * columns
-    second, third = first + hidden_local, first + 2 * hidden_local
+    second = first + hidden_local
     span = lent.shape[1] // 2
-    lent_out = jnp.concatenate([lent[third:, :span], lent[third:, span:]], axis=0)
-    up_both = jnp.concatenate([own_up, lent[first:second]], axis=0)
-    down_both = jnp.concatenate([own_down, lent[second:third]], axis=0)
-    lent_mix, own_mix, own_out, lent_out, up_both, down_both = lax.optimization_barrier(
-        (lent[:first], own_mix, own_out, lent_out, up_both, down_both)
+    lent_out = jnp.concatenate([lent[second:, :span], lent[second:, span:]], axis=0)
+    mixer_pair = jnp.concatenate([own_mixer, lent[first:second]], axis=0)
+    lent_mix, own_mix, own_out, lent_out, mixer_pair = lax.optimization_barrier(
+        (lent[:first], own_mix, own_out, lent_out, mixer_pair)
     )
     sums = square_sums(token_half)
     high = sums.astype(jnp.bfloat16).astype(jnp.float32)
@@ -181,6 +197,8 @@
         [jnp.concatenate([part, extra], axis=0).T for part in (first, second)]
     ).astype(jnp.bfloat16)
     raw = raw.reshape(cores * chips, seq_local, 128)
+    raw, near, cross = lax.optimization_barrier((raw, near, cross))
+    near = crossed(near, False)
     raw = lax.all_to_all(raw, ("tp", *KV), split_axis=0, concat_axis=0, tiled=True)
     raw, gate_floor, head_gain = lax.optimization_barrier((raw, gate_floor, head_gain))
     raw = raw.reshape(cores, chips, seq_local, 128).astype(jnp.float32).sum(axis=0)
@@ -197,28 +215,43 @@
     new_state = (
         forget_gate[..., None] * state + (1.0 - forget_gate)[..., None] * input_vec[:, :, None, :]
     )
+    new_state = lax.optimization_barrier(new_state)
     head_out = jnp.sum(query_vec[..., None] * new_state, axis=2)
     branch = rms_scale(head_out, head_gain) * jax.nn.silu(gate_vec)
     branch = branch.reshape(seq_local, heads_local * head_size).astype(jnp.bfloat16)
+
+    branch, near, cross = lax.optimization_barrier((branch, near, cross))
+    cross = crossed(cross, True)
 
     branch_half = gathered(branch).reshape(rows, heads_local * head_size)
     theirs = swapped(contracted(lent_out, branch_half, (1, 1)))
     projected = contracted(own_out, branch_half, (1, 1)) + theirs
     residual = (tokens_t.astype(jnp.float32) + projected).astype(jnp.bfloat16)
 
-    residual_half = gathered(residual).reshape(chips * share, rows)
-    partial = contracted(up_both, residual_half, (1, 0))
-    sums = square_sums(residual_half)
+    mixer = jnp.concatenate([mixer_pair, near, cross], axis=0)
+    quarter = mixer.shape[1] // 2
+    up, down = mixer[:, :quarter], mixer[:, quarter:]
+    residual, up, down = lax.optimization_barrier((residual, up, down))
+    residual_quarter = gathered(residual, SIDE).reshape(quarter, rows)
+    partial = contracted(up, residual_quarter, (1, 0))
+    sums = square_sums(residual_quarter)
+    units = partial.shape[0]
     arrived = swapped(jnp.concatenate([partial, sums], axis=0))
-    upward = partial + jnp.concatenate(
-        [arrived[hidden_local : 2 * hidden_local], arrived[:hidden_local]], axis=0
-    )
-    scale = lax.rsqrt((sums + arrived[-1:]) / width + EPSILON)
+    blocks = [arrived[n * hidden_local : (n + 1) * hidden_local] for n in (1, 0, 3, 2)]
+    paired = partial + jnp.concatenate(blocks, axis=0)
+    sums = sums + arrived[units:]
+    high = sums.astype(jnp.bfloat16).astype(jnp.float32)
+    arrived = crossed(
+        jnp.concatenate([paired, high, sums - high], axis=0).astype(jnp.bfloat16), False
+    ).astype(jnp.float32)
+    upward = paired + jnp.concatenate([arrived[units // 2 : units], arrived[: units // 2]], axis=0)
+    sums = sums + arrived[units : units + 1] + arrived[units + 1 :]
+    scale = lax.rsqrt(sums / width + EPSILON)
     hidden = jnp.square(jax.nn.relu(upward * scale)).astype(jnp.bfloat16)
 
-    terms = contracted(down_both, hidden, (0, 0)).astype(jnp.bfloat16)
+    terms = contracted(down, hidden, (0, 0)).astype(jnp.bfloat16)
     terms = lax.all_to_all(
-        terms.reshape(chips, share, rows), KV, split_axis=0, concat_axis=0, tiled=True
+        terms.reshape(-1, share, rows), SIDE, split_axis=0, concat_axis=0, tiled=True
     )
     summed = terms.astype(jnp.float32).sum(axis=0)
     mixed = (residual.astype(jnp.float32) + summed).astype(jnp.bfloat16).T
@@ -227,7 +260,7 @@
 
 def solution(mesh):
     torus = Mesh(
-        mesh.devices.reshape(mesh.shape["dp"], 8, 8, mesh.shape["tp"]), ("dp", "kv_0", "kv_1", "tp")
+        mesh.devices.reshape(mesh.shape["dp"], 4, 2, 8, mesh.shape["tp"]), ("dp", *KV_TP)
     )
     placed = (
         P("dp", KV_TP),

time: 140 us -> 162 us (1.16)
  the two profiles are of different devices: /device:TPU:6 before, /device:TPU:8 now
where the time goes in v7:
time: 162 us; the launch traced here: 161 us
  waiting for transfers between devices  49.6 us (31%)
  starting transfers between devices  49.5 us (31%)
  blocking collectives  42.7 us (26%)
  local copies, waits for them, and re-layouts  6.87 us (4%)
  Pallas kernels  4.77 us (3%)
  other arithmetic  4.45 us (3%)
  matrix products  1.75 us (1%)
    all_to_all x2, waiting for transfers between devices, gathered(): lax.all_to_all(jnp.broadcast_to(x[None], (chips, *x.shape)), axes, 0, 0,...  29.3 us
    all_to_all x2, starting transfers between devices, gathered(): lax.all_to_all(jnp.broadcast_to(x[None], (chips, *x.shape)), axes, 0, 0,...  28.6 us
    all_to_all x1, blocking collectives, gathered(): lax.all_to_all(jnp.broadcast_to(x[None], (chips, *x.shape)), axes, 0, 0,...  24.7 us
    all_to_all x1, blocking collectives, per_device(): lax.all_to_all(terms.reshape(-1, share, rows), SIDE, split_axis=0, concat...  18.1 us
    ppermute x3, waiting for transfers between devices, crossed(): return lax.ppermute(x, (PAIR, 'tp'), moves)  10.8 us
    ppermute x3, starting transfers between devices, crossed(): return lax.ppermute(x, (PAIR, 'tp'), moves)  8.68 us
    all_to_all x1, waiting for transfers between devices, per_device(): lax.all_to_all(raw, ('tp', *KV), split_axis=0, concat_axis=0, tiled=True)  8.07 us
    all_to_all x1, starting transfers between devices, per_device(): lax.all_to_all(raw, ('tp', *KV), split_axis=0, concat_axis=0, tiled=True)  6.28 us
  transfers between devices with their start and end apart: 9, of which 7 were waited for; matrix products, arithmetic and copies ran while one was open for 4% of the time, Pallas kernels for 0%

profile of v7, /device:TPU:8, one launch (start us, length us, event | category | flops | bytes accessed | tf_op | source)
XLA Modules:
  0.0 160.8 jit_solution(12349552004506913161)
XLA Ops:
  0.6 0.0 copy-start
  0.6 0.0 copy-start.8
  0.7 0.6 pad_add_fusion.refs_0_
  1.2 4.8 %shard_map.140 = (bf16[64,2048]{1,0:T(8,128)(2,1)}, bf16[128,2048]{1,0:T(8,128)(2,1)}, bf16[32,1024]{1,0:T(8,128)(2,1)}, bf16[128,2048]{1,0:T(8,128)(2,1)}, bf16...) custom-call(s32[2]{0:T(128)} %pad_add_fusion.refs_0_, bf16[16,4096]{1,0:T(8,128)(2,1)} %bitcast.87, ...), custom_call_target="tpu_custom_call" | custom-call | tf_op jit(solution)/shard_map/pallas_call | solution.py:136
  6.0 2.0 %collective-permute-start = (bf16[208,2048]{1,0:T(8,128)(2,1)}, bf16[208,2048]{1,0:T(8,128)(2,1)S(1)}, u32[]{:S(2)}, u32[]{:S(2)}) collective-permute-start(bf16[208,2048]{1,0:T(8,128)(2,1)} %get-tuple-element.25), channel_id=1, source_target_pairs={{0,1},{1,0},{2,3},{3,2},{4,5},{5,4},{6,7},{7,6},{8,9},{9,8},{10,11... | collective-permute-start | bytes 2555912 | tf_op jit(solution)/shard_map/ppermute | solution.py:25
  8.0 0.0 copy-done.8
  8.1 0.9 broadcast_in_dim.34
  8.9 16.6 %all-to-all-start = ((bf16[64,32,128]{2,1,0:T(8,128)(2,1)}), bf16[64,32,128]{2,1,0:T(8,128)(2,1)S(1)}, u32[]{:S(2)}, u32[]{:S(2)}) async-start(bf16[64,32,128]{2,1,0:T(8,128)(2,1)} %broadcast_in_dim.34), calls=%async_computation | async-start | bytes 1048576 | tf_op jit(solution)/shard_map/all_to_all | solution.py:36
  25.5 0.0 collective-permute-done
  25.6 0.0 copy-start.6
  25.7 0.0 copy-done.5
  25.7 1.1 pad_maximum_fusion
  26.7 18.7 %all-to-all-done = bf16[64,32,128]{2,1,0:T(8,128)(2,1)S(1)} async-done(((bf16[64,32,128]{2,1,0:T(8,128)(2,1)}), bf16[64,32,128]{2,1,0:T(8,128)(2,1)S(1)}, u32[]{:S(2)}, u32[]{:S(2)}) %all-to-all-start) | async-done | bytes 524320 | tf_op jit(solution)/shard_map/all_to_all | solution.py:36
  45.4 0.3 multiply_reduce_fusion.1
  45.7 0.2 fusion.27
  46.0 0.2 select_convert_fusion.2
  46.2 0.1 select_convert_fusion.1
  46.3 0.7 copy.32
  47.1 6.3 %all-to-all-start.1 = ((bf16[128,2,128]{2,1,0:T(2,128)(2,1)}), bf16[128,2,128]{2,1,0:T(2,128)(2,1)S(1)}, u32[]{:S(2)}, u32[]{:S(2)}) async-start(bf16[128,2,128]{2,1,0:T(2,128)(2,1)} %bitcast.19), calls=%async_computation.1 | async-start | bytes 131072 | tf_op jit(solution)/shard_map/all_to_all | solution.py:202
  53.4 3.4 %collective-permute-start.1 = (bf16[128,2048]{1,0:T(8,128)(2,1)S(1)}, bf16[128,2048]{1,0:T(8,128)(2,1)S(1)}, u32[]{:S(2)}, u32[]{:S(2)}) collective-permute-start(bf16[128,2048]{1,0:T(8,128)(2,1)S(1)} %copy-done.10), channel_id=1, source_target_pairs={{0,16},{1,17},{16,0},{17,1},{2,18},{3,19},{18,2},{19,3},{4,20},{5,... | collective-permute-start | bytes 1572872 | tf_op jit(solution)/shard_map/ppermute | solution.py:31
  56.7 8.1 %all-to-all-done.1 = bf16[128,2,128]{2,1,0:T(2,128)(2,1)S(1)} async-done(((bf16[128,2,128]{2,1,0:T(2,128)(2,1)}), bf16[128,2,128]{2,1,0:T(2,128)(2,1)S(1)}, u32[]{:S(2)}, u32[]{:S(2)}) %all-to-all-start.1) | async-done | bytes 65568 | tf_op jit(solution)/shard_map/all_to_all | solution.py:202
  64.8 0.1 convert_reduce_fusion.1
  64.9 0.2 slice_reduce_fusion
  65.1 0.1 copy_multiply_fusion
  65.1 0.1 copy.34
  65.3 0.1 copy.35
  65.4 0.1 mul.127
  65.5 0.1 copy.37
  65.6 0.1 mul.134
  65.6 0.1 copy.36
  65.7 0.1 div.32
  65.8 0.6 multiply_add_fusion
  66.4 0.0 copy-start.1
  66.5 0.3 multiply_reduce_fusion
  66.8 0.1 multiply_reduce_fusion.3
  66.9 0.1 copy.38
  67.0 0.1 squeeze.22
  67.1 0.1 multiply_bitcast_fusion
  67.2 3.1 %collective-permute-done.1 = bf16[128,2048]{1,0:T(8,128)(2,1)S(1)} collective-permute-done((bf16[128,2048]{1,0:T(8,128)(2,1)S(1)}, bf16[128,2048]{1,0:T(8,128)(2,1)S(1)}, u32[]{:S(2)}, u32[]{:S(2)}) %collective-permute-start.1) | collective-permute-done | bytes 524320 | tf_op jit(solution)/shard_map/ppermute | solution.py:31
  70.3 0.9 broadcast_in_dim.61
  71.2 12.1 %all-to-all-start.2 = ((bf16[64,2,1024]{2,1,0:T(2,128)(2,1)}), bf16[64,2,1024]{2,1,0:T(2,128)(2,1)S(1)}, u32[]{:S(2)}, u32[]{:S(2)}) async-start(bf16[64,2,1024]{2,1,0:T(2,128)(2,1)} %broadcast_in_dim.61), calls=%async_computation.2 | async-start | bytes 524288 | tf_op jit(solution)/shard_map/all_to_all | solution.py:36
  83.2 2.1 %collective-permute-start.3 = (bf16[128,2048]{1,0:T(8,128)(2,1)}, bf16[128,2048]{1,0:T(8,128)(2,1)}, u32[]{:S(2)}, u32[]{:S(2)}) collective-permute-start(bf16[128,2048]{1,0:T(8,128)(2,1)} %get-tuple-element.44), channel_id=1, source_target_pairs={{0,17},{1,16},{16,1},{17,0},{2,19},{3,18},{18,3},{19,2},{4,21},{5,... | collective-permute-start | bytes 1572872 | tf_op jit(solution)/shard_map/ppermute | solution.py:31
  85.4 1.4 constant_dynamic-update-slice_fusion.2
  86.8 10.6 %all-to-all-done.2 = bf16[64,2,1024]{2,1,0:T(2,128)(2,1)S(1)} async-done(((bf16[64,2,1024]{2,1,0:T(2,128)(2,1)}), bf16[64,2,1024]{2,1,0:T(2,128)(2,1)S(1)}, u32[]{:S(2)}, u32[]{:S(2)}) %all-to-all-start.2) | async-done | bytes 262176 | tf_op jit(solution)/shard_map/all_to_all | solution.py:36
  97.4 0.1 reshape.104
  97.5 0.2 fusion.28
  97.7 1.9 %collective-permute-start.2 = (f32[32,128]{1,0:T(8,128)S(1)}, f32[32,128]{1,0:T(8,128)S(1)}, u32[]{:S(2)}, u32[]{:S(2)}) collective-permute-start(f32[32,128]{1,0:T(8,128)S(1)} %fusion.28), channel_id=1, source_target_pairs={{0,1},{1,0},{2,3},{3,2},{4,5},{5,4},{6,7},{7,6},{8,9},{9,8},{10,11... | collective-permute-start | bytes 49160 | tf_op jit(solution)/shard_map/ppermute | solution.py:25
  99.6 3.4 %collective-permute-done.3 = bf16[128,2048]{1,0:T(8,128)(2,1)} collective-permute-done((bf16[128,2048]{1,0:T(8,128)(2,1)}, bf16[128,2048]{1,0:T(8,128)(2,1)}, u32[]{:S(2)}, u32[]{:S(2)}) %collective-permute-start.3) | collective-permute-done | bytes 524320 | tf_op jit(solution)/shard_map/ppermute | solution.py:31
  103.1 1.1 constant_dynamic-update-slice_fusion
  104.1 0.2 fusion.23
  104.3 0.0 collective-permute-done.2
  104.3 0.6 copy-done.7
  105.0 0.2 fusion.1
  105.1 0.1 broadcast_in_dim.62
  105.2 24.7 %all_to_all.25 = bf16[32,32,128]{2,1,0:T(8,128)(2,1)S(1)} all-to-all(bf16[32,32,128]{2,1,0:T(8,128)(2,1)S(1)} %broadcast_in_dim.62), channel_id=1, replica_groups=mesh['dp'=4,'kv_far'=4,'kv_pair'=2,'kv_near'=8,'tp'=2] {'kv_far','kv_near'}, dimensions={0} | all-to-all | bytes 524288 | tf_op jit(solution)/shard_map/all_to_all | solution.py:36
  129.9 0.4 fusion.29
  130.4 0.2 multiply_reduce_fusion.2
  130.5 1.9 %collective-permute-start.4 = (f32[513,128]{1,0:T(8,128)S(1)}, f32[513,128]{1,0:T(8,128)S(1)}, u32[]{:S(2)}, u32[]{:S(2)}) collective-permute-start(f32[513,128]{1,0:T(8,128)S(1)} %pad_maximum_fusion.1), channel_id=1, source_target_pairs={{0,1},{1,0},{2,3},{3,2},{4,5},{5,4},{6,7},{7,6},{8,9},{9,8},{10,11... | collective-permute-start | bytes 787976 | tf_op jit(solution)/shard_map/ppermute | solution.py:25
  132.5 1.5 collective-permute-done.4
  134.1 3.2 %collective-permute-start.5 = (bf16[514,128]{1,0:T(8,128)(2,1)S(1)}, bf16[514,128]{1,0:T(8,128)(2,1)S(1)}, u32[]{:S(2)}, u32[]{:S(2)}) collective-permute-start(bf16[514,128]{1,0:T(8,128)(2,1)S(1)} %pad_maximum_fusion.2), channel_id=1, source_target_pairs={{0,16},{1,17},{16,0},{17,1},{2,18},{3,19},{18,2},{19,3},{4,20},{5,... | collective-permute-start | bytes 394760 | tf_op jit(solution)/shard_map/ppermute | solution.py:31
  137.3 4.3 %collective-permute-done.5 = bf16[514,128]{1,0:T(8,128)(2,1)S(1)} collective-permute-done((bf16[514,128]{1,0:T(8,128)(2,1)S(1)}, bf16[514,128]{1,0:T(8,128)(2,1)S(1)}, u32[]{:S(2)}, u32[]{:S(2)}) %collective-permute-start.5) | collective-permute-done | bytes 131616 | tf_op jit(solution)/shard_map/ppermute | solution.py:31
  141.6 0.5 convolution_convert_fusion
  142.1 18.1 %all_to_all.26 = bf16[32,32,128]{2,1,0:T(8,128)(2,1)S(1)} all-to-all(bf16[32,32,128]{2,1,0:T(8,128)(2,1)S(1)} %bitcast.83), channel_id=1, replica_groups=mesh['dp'=4,'kv_far'=4,'kv_pair'=2,'kv_near'=8,'tp'=2] {'kv_far','kv_near'}, dimensions={0} | all-to-all | bytes 524288 | tf_op jit(solution)/shard_map/all_to_all | solution.py:253
  160.2 0.6 fusion.15
  (41 shorter events, 0.4 us)
Async XLA Ops:
  0.6 64.6 %copy-start = (f32[128]{0:T(128)S(1)}, f32[128]{0:T(128)}, u32[]{:S(2)}) copy-start(f32[128]{0:T(128)} %param.19) | copy-start | bytes 1540
  0.6 7.4 %copy-start.8 = (bf16[128,32]{0,1:T(8,128)(2,1)S(1)}, bf16[128,32]{0,1:T(8,128)(2,1)}, u32[]{:S(2)}) copy-start(bf16[128,32]{0,1:T(8,128)(2,1)} %param.13) | copy-start | bytes 24580
  6.0 19.7 %copy-start.5 = (bf16[128,2048]{1,0:T(8,128)(2,1)S(1)}, bf16[128,2048]{1,0:T(8,128)(2,1)}, u32[]{:S(2)}) copy-start(bf16[128,2048]{1,0:T(8,128)(2,1)} %get-tuple-element.28) | copy-start | bytes 1572868
  6.0 19.5 %collective-permute-start = (bf16[208,2048]{1,0:T(8,128)(2,1)}, bf16[208,2048]{1,0:T(8,128)(2,1)S(1)}, u32[]{:S(2)}, u32[]{:S(2)}) collective-permute-start(bf16[208,2048]{1,0:T(8,128)(2,1)} %get-tuple-element.25), channel_id=1, source_target_pairs={{0,1},{1,0},{2,3},{3,2},{4,5},{5,4},{6,7},{7,6},{8,9},{9,8},{10,11... | collective-permute-start | bytes 2555912 | tf_op jit(solution)/shard_map/ppermute | solution.py:25
  8.9 36.5 %all-to-all-start = ((bf16[64,32,128]{2,1,0:T(8,128)(2,1)}), bf16[64,32,128]{2,1,0:T(8,128)(2,1)S(1)}, u32[]{:S(2)}, u32[]{:S(2)}) async-start(bf16[64,32,128]{2,1,0:T(8,128)(2,1)} %broadcast_in_dim.34), calls=%async_computation | async-start | bytes 1048576 | tf_op jit(solution)/shard_map/all_to_all | solution.py:36
  25.6 20.3 %copy-start.6 = (bf16[64,2048]{1,0:T(8,128)(2,1)S(1)}, bf16[64,2048]{1,0:T(8,128)(2,1)}, u32[]{:S(2)}) copy-start(bf16[64,2048]{1,0:T(8,128)(2,1)} %get-tuple-element.30) | copy-start | bytes 786436
  25.7 27.7 %copy-start.10 = (bf16[128,2048]{1,0:T(8,128)(2,1)S(1)}, bf16[128,2048]{1,0:T(8,128)(2,1)}, u32[]{:S(2)}) copy-start(bf16[128,2048]{1,0:T(8,128)(2,1)} %get-tuple-element.38) | copy-start | bytes 1572868
  26.7 38.5 %copy-start.9 = (f32[1024]{0:T(1024)S(1)}, f32[1024]{0:T(1024)}, u32[]{:S(2)}) copy-start(f32[1024]{0:T(1024)} %param.18) | copy-start | bytes 12292
  26.7 39.1 %copy-start.2 = (f32[2,8,128,128]{3,2,1,0:T(8,128)S(1)}, f32[2,8,128,128]{3,2,1,0:T(8,128)}, u32[]{:S(2)}) copy-start(f32[2,8,128,128]{3,2,1,0:T(8,128)} %param.25) | copy-start | bytes 3145732
  47.1 17.8 %all-to-all-start.1 = ((bf16[128,2,128]{2,1,0:T(2,128)(2,1)}), bf16[128,2,128]{2,1,0:T(2,128)(2,1)S(1)}, u32[]{:S(2)}, u32[]{:S(2)}) async-start(bf16[128,2,128]{2,1,0:T(2,128)(2,1)} %bitcast.19), calls=%async_computation.1 | async-start | bytes 131072 | tf_op jit(solution)/shard_map/all_to_all | solution.py:202
  53.4 16.9 %collective-permute-start.1 = (bf16[128,2048]{1,0:T(8,128)(2,1)S(1)}, bf16[128,2048]{1,0:T(8,128)(2,1)S(1)}, u32[]{:S(2)}, u32[]{:S(2)}) collective-permute-start(bf16[128,2048]{1,0:T(8,128)(2,1)S(1)} %copy-done.10), channel_id=1, source_target_pairs={{0,16},{1,17},{16,0},{17,1},{2,18},{3,19},{18,2},{19,3},{4,20},{5,... | collective-permute-start | bytes 1572872 | tf_op jit(solution)/shard_map/ppermute | solution.py:31
  66.4 20.3 %copy-start.1 = (f32[2,8,128,128]{3,2,1,0:T(8,128)}, f32[2,8,128,128]{3,2,1,0:T(8,128)S(1)}, u32[]{:S(2)}) copy-start(f32[2,8,128,128]{3,2,1,0:T(8,128)S(1)} %multiply_add_fusion) | copy-start | bytes 3145732
  70.3 13.0 %copy-start.3 = (bf16[128,2048]{1,0:T(8,128)(2,1)}, bf16[128,2048]{1,0:T(8,128)(2,1)S(1)}, u32[]{:S(2)}) copy-start(bf16[128,2048]{1,0:T(8,128)(2,1)S(1)} %collective-permute-done.1) | copy-start | bytes 1572868
  71.2 26.2 %all-to-all-start.2 = ((bf16[64,2,1024]{2,1,0:T(2,128)(2,1)}), bf16[64,2,1024]{2,1,0:T(2,128)(2,1)S(1)}, u32[]{:S(2)}, u32[]{:S(2)}) async-start(bf16[64,2,1024]{2,1,0:T(2,128)(2,1)} %broadcast_in_dim.61), calls=%async_computation.2 | async-start | bytes 524288 | tf_op jit(solution)/shard_map/all_to_all | solution.py:36
  83.2 19.8 %collective-permute-start.3 = (bf16[128,2048]{1,0:T(8,128)(2,1)}, bf16[128,2048]{1,0:T(8,128)(2,1)}, u32[]{:S(2)}, u32[]{:S(2)}) collective-permute-start(bf16[128,2048]{1,0:T(8,128)(2,1)} %get-tuple-element.44), channel_id=1, source_target_pairs={{0,17},{1,16},{16,1},{17,0},{2,19},{3,18},{18,3},{19,2},{4,21},{5,... | collective-permute-start | bytes 1572872 | tf_op jit(solution)/shard_map/ppermute | solution.py:31
  85.4 1.4 copy-start.4
  97.7 6.6 %collective-permute-start.2 = (f32[32,128]{1,0:T(8,128)S(1)}, f32[32,128]{1,0:T(8,128)S(1)}, u32[]{:S(2)}, u32[]{:S(2)}) collective-permute-start(f32[32,128]{1,0:T(8,128)S(1)} %fusion.28), channel_id=1, source_target_pairs={{0,1},{1,0},{2,3},{3,2},{4,5},{5,4},{6,7},{7,6},{8,9},{9,8},{10,11... | collective-permute-start | bytes 49160 | tf_op jit(solution)/shard_map/ppermute | solution.py:25
  104.1 0.8 copy-start.7
  130.5 3.4 %collective-permute-start.4 = (f32[513,128]{1,0:T(8,128)S(1)}, f32[513,128]{1,0:T(8,128)S(1)}, u32[]{:S(2)}, u32[]{:S(2)}) collective-permute-start(f32[513,128]{1,0:T(8,128)S(1)} %pad_maximum_fusion.1), channel_id=1, source_target_pairs={{0,1},{1,0},{2,3},{3,2},{4,5},{5,4},{6,7},{7,6},{8,9},{9,8},{10,11... | collective-permute-start | bytes 787976 | tf_op jit(solution)/shard_map/ppermute | solution.py:25
  134.1 7.5 %collective-permute-start.5 = (bf16[514,128]{1,0:T(8,128)(2,1)S(1)}, bf16[514,128]{1,0:T(8,128)(2,1)S(1)}, u32[]{:S(2)}, u32[]{:S(2)}) collective-permute-start(bf16[514,128]{1,0:T(8,128)(2,1)S(1)} %pad_maximum_fusion.2), channel_id=1, source_target_pairs={{0,16},{1,17},{16,0},{17,1},{2,18},{3,19},{18,2},{19,3},{4,20},{5,... | collective-permute-start | bytes 394760 | tf_op jit(solution)/shard_map/ppermute | solution.py:31

commit v8 on v6

--- a/solution.py
+++ b/solution.py
@@ -7,9 +7,10 @@
 from jax.sharding import PartitionSpec as P
 
 
-KV = ("kv_0", "kv_1")
-KV_TP = ("kv_0", "kv_1", "tp")
-DP_KV = ("dp", "kv_0", "kv_1")
+KV = ("za", "zb", "zc", "ya", "yb", "yc")
+SPREAD = ("zc", "yc", "zb", "yb", "ya", "za")
+KV_TP = (*KV, "tp")
+DP_KV = ("dp", *KV)
 
 
 EPSILON = 1e-06
@@ -23,9 +24,9 @@
     return lax.ppermute(x, "tp", [(0, 1), (1, 0)])
 
 
-def gathered(x):
-    chips = lax.axis_size(KV)
-    return lax.all_to_all(jnp.broadcast_to(x[None], (chips, *x.shape)), KV, 0, 0, tiled=True)
+def gathered(x, axes=KV):
+    chips = lax.axis_size(axes)
+    return lax.all_to_all(jnp.broadcast_to(x[None], (chips, *x.shape)), axes, 0, 0, tiled=True)
 
 
 def contracted(left, right, dims):
@@ -39,14 +40,25 @@
     return jnp.sum(values * values, axis=0, keepdims=True)
 
 
-CHUNK = 256
+TILE = 128
 
 
 def selection(core, share):
-    source = lax.broadcasted_iota(jnp.int32, (CHUNK, CHUNK // 2), 0)
-    target = lax.broadcasted_iota(jnp.int32, (CHUNK, CHUNK // 2), 1)
-    wanted = (target // share) * (2 * share) + core * share + target % share
+    source = lax.broadcasted_iota(jnp.int32, (4 * TILE, 2 * TILE), 0)
+    target = lax.broadcasted_iota(jnp.int32, (4 * TILE, 2 * TILE), 1)
+    row, place = target // TILE, target % TILE
+    wanted = (place // share) * TILE + row * 2 * share + core * share + place % share
     return jnp.where(source == wanted, 1.0, 0.0).astype(jnp.bfloat16)
+
+
+def spread_tiles():
+    for zc in range(2):
+        for zb in range(2):
+            for yb in range(2):
+                chips = [
+                    32 * za + 16 * zb + 8 * zc + 4 * ya + 2 * yb for ya in range(2) for za in range(2)
+                ]
+                yield [chip // 2 for chip in chips], [8 * zc + 4 * yc + 2 * zb + yb for yc in range(2)]
 
 
 def split_kernel(
@@ -68,32 +80,37 @@
     other_ref,
 ):
     core = core_ref[0]
-    half = CHUNK // 2
     columns = query_ref.shape[0]
     hidden = down_ref.shape[0]
     span = out_ref.shape[1] // 2
     lines = out_ref.shape[0] // 2
     first, second = 4 * columns, 4 * columns + hidden
+    for tiles, places in spread_tiles():
+        spans = [pl.ds(tile * TILE, TILE) for tile in tiles]
+        mix_gain = jnp.concatenate([mix_gain_ref[:, part] for part in spans], axis=1)
+        ffn_gain = jnp.concatenate([ffn_gain_ref[:, part] for part in spans], axis=1)
+        parts = [
+            jnp.concatenate([ref[:, part] for part in spans], axis=1).astype(jnp.float32) * mix_gain
+            for ref in (query_ref, forget_ref, input_ref, gate_ref)
+        ]
+        raised = jnp.concatenate([up_ref[part, :] for part in spans], axis=0)
+        parts.append(raised.astype(jnp.float32).T * ffn_gain)
+        rows = [part.astype(jnp.bfloat16) for part in parts]
+        rows.append(jnp.concatenate([down_ref[:, part] for part in spans], axis=1))
+        rows = jnp.concatenate(rows, axis=0)
+        for own, index in ((True, core), (False, 1 - core)):
+            picked = jnp.dot(rows, selection(index, share), preferred_element_type=jnp.float32)
+            picked = picked.astype(jnp.bfloat16)
+            for row, place in enumerate(places):
+                block = picked[:, row * TILE : (row + 1) * TILE]
+                target = pl.ds(place * TILE, TILE)
+                if own:
+                    mix_ref[:, target] = block[:first]
+                    own_up_ref[:, target] = block[first:second]
+                    own_down_ref[:, target] = block[second:]
+                else:
+                    other_ref[: second + hidden, target] = block
     for own, index in ((True, core), (False, 1 - core)):
-        chosen = selection(index, share)
-        for chunk in range(up_ref.shape[0] // CHUNK):
-            source = pl.ds(chunk * CHUNK, CHUNK)
-            target = pl.ds(chunk * half, half)
-            parts = [
-                part[:, source].astype(jnp.float32) * mix_gain_ref[:, source]
-                for part in (query_ref, forget_ref, input_ref, gate_ref)
-            ]
-            parts.append(up_ref[source, :].astype(jnp.float32).T * ffn_gain_ref[:, source])
-            rows = jnp.concatenate([part.astype(jnp.bfloat16) for part in parts], axis=0)
-            rows = jnp.concatenate([rows, down_ref[:, source]], axis=0)
-            picked = jnp.dot(rows, chosen, preferred_element_type=jnp.float32)
-            picked = picked.astype(jnp.bfloat16)
-            if own:
-                mix_ref[:, target] = picked[:first]
-                own_up_ref[:, target] = picked[first:second]
-                own_down_ref[:, target] = picked[second:]
-            else:
-                other_ref[: second + hidden, target] = picked
         start = pl.multiple_of(index * span, span)
         if own:
             own_out_ref[...] = out_ref[:, pl.ds(start, span)]
@@ -150,7 +167,7 @@
 
     tp = lax.axis_index("tp")
 
-    token_half = gathered(tokens_t).reshape(chips * share, rows)
+    token_half = gathered(tokens_t, SPREAD).reshape(chips * share, rows)
     own_mix, own_up, own_down, own_out, other = split_weights(
         share,
         *[w[:, 0, :].T for w in (w_query, w_forget, w_input, w_output_gate)],
@@ -197,6 +214,7 @@
     new_state = (
         forget_gate[..., None] * state + (1.0 - forget_gate)[..., None] * input_vec[:, :, None, :]
     )
+    new_state = lax.optimization_barrier(new_state)
     head_out = jnp.sum(query_vec[..., None] * new_state, axis=2)
     branch = rms_scale(head_out, head_gain) * jax.nn.silu(gate_vec)
     branch = branch.reshape(seq_local, heads_local * head_size).astype(jnp.bfloat16)
@@ -206,7 +224,7 @@
     projected = contracted(own_out, branch_half, (1, 1)) + theirs
     residual = (tokens_t.astype(jnp.float32) + projected).astype(jnp.bfloat16)
 
-    residual_half = gathered(residual).reshape(chips * share, rows)
+    residual_half = gathered(residual, SPREAD).reshape(chips * share, rows)
     partial = contracted(up_both, residual_half, (1, 0))
     sums = square_sums(residual_half)
     arrived = swapped(jnp.concatenate([partial, sums], axis=0))
@@ -218,7 +236,7 @@
 
     terms = contracted(down_both, hidden, (0, 0)).astype(jnp.bfloat16)
     terms = lax.all_to_all(
-        terms.reshape(chips, share, rows), KV, split_axis=0, concat_axis=0, tiled=True
+        terms.reshape(chips, share, rows), SPREAD, split_axis=0, concat_axis=0, tiled=True
     )
     summed = terms.astype(jnp.float32).sum(axis=0)
     mixed = (residual.astype(jnp.float32) + summed).astype(jnp.bfloat16).T
@@ -227,7 +245,7 @@
 
 def solution(mesh):
     torus = Mesh(
-        mesh.devices.reshape(mesh.shape["dp"], 8, 8, mesh.shape["tp"]), ("dp", "kv_0", "kv_1", "tp")
+        mesh.devices.reshape(mesh.shape["dp"], *[2] * 6, mesh.shape["tp"]), ("dp", *KV_TP)
     )
     placed = (
         P("dp", KV_TP),

time: 140 us -> 142 us (1.014)
    add x0 -> x1, other arithmetic: none -> 1.83 us  [per_device(): forget_gate[..., None] * state]
where the time goes in v8:
time: 142 us; the launch traced here: 141 us
  blocking collectives  86.8 us (61%)
  starting transfers between devices  22.4 us (16%)
  waiting for transfers between devices  14.8 us (10%)
  local copies, waits for them, and re-layouts  5.63 us (4%)
  Pallas kernels  4.92 us (3%)
  other arithmetic  4.33 us (3%)
  matrix products  1.71 us (1%)
    all_to_all x2, blocking collectives, gathered(): lax.all_to_all(jnp.broadcast_to(x[None], (chips, *x.shape)), axes, 0, 0,...  43.2 us
    all_to_all x1, blocking collectives, per_device(): lax.all_to_all(terms.reshape(chips, share, rows), SPREAD, split_axis=0, c...  24.9 us
    all_to_all x1, blocking collectives, per_device(): lax.all_to_all(raw, ('tp', *KV), split_axis=0, concat_axis=0, tiled=True)  18.6 us
    all_to_all x1, starting transfers between devices, gathered(): lax.all_to_all(jnp.broadcast_to(x[None], (chips, *x.shape)), axes, 0, 0,...  16.6 us
    all_to_all x1, waiting for transfers between devices, gathered(): lax.all_to_all(jnp.broadcast_to(x[None], (chips, *x.shape)), axes, 0, 0,...  12.3 us
    ppermute x3, starting transfers between devices, swapped(): return lax.ppermute(x, 'tp', [(0, 1), (1, 0)])  5.77 us
    pallas_call x1, Pallas kernels, split_weights(): pl.pallas_call(lambda *refs: split_kernel(share, *refs), out_shape=[jax.S...  4.92 us
  transfers between devices with their start and end apart: 4, of which 3 were waited for; matrix products, arithmetic and copies ran while one was open for 0% of the time, Pallas kernels for 3%

profile of v8, /device:TPU:6, one launch (start us, length us, event | category | flops | bytes accessed | tf_op | source)
XLA Modules:
  0.0 141.5 jit_solution(16829092210753811725)
XLA Ops:
  0.6 0.0 copy-start
  0.6 1.6 %broadcast_in_dim.34 = bf16[64,32,128]{2,1,0:T(8,128)(2,1)} broadcast(bf16[32,128]{1,0:T(8,128)(2,1)} %bitcast.86), dimensions={1,2} | broadcast | bytes 532480 | tf_op jit(solution)/shard_map/broadcast_in_dim | solution.py:29
  2.2 16.6 %all-to-all-start = ((bf16[64,32,128]{2,1,0:T(8,128)(2,1)}), bf16[64,32,128]{2,1,0:T(8,128)(2,1)S(1)}, u32[]{:S(2)}, u32[]{:S(2)}) async-start(bf16[64,32,128]{2,1,0:T(8,128)(2,1)} %broadcast_in_dim.34), calls=%async_computation | async-start | bytes 1048576 | tf_op jit(solution)/shard_map/all_to_all | solution.py:29
  18.8 4.9 %shard_map.140 = (bf16[64,2048]{1,0:T(8,128)(2,1)}, bf16[128,2048]{1,0:T(8,128)(2,1)}, bf16[128,2048]{1,0:T(8,128)(2,1)}, bf16[32,1024]{1,0:T(8,128)(2,1)}, bf16[336,2048]{1,0:T(8,128)(2,1)}) custom-call(s32[1]{0:T(128)} %bitcast.1.refs_0_, bf16[16,4096]{1,0:T(8,128)(2,1)} %bitcast.81, bf16[16,4096]{1,0:T(8,128)(2,1)} %bitcast.82, ...), custom_call_target="tpu_custom_call" | custom-call | tf_op jit(solution)/shard_map/pallas_call | solution.py:136
  23.7 1.9 %collective-permute-start = (bf16[336,2048]{1,0:T(8,128)(2,1)}, bf16[336,2048]{1,0:T(8,128)(2,1)S(1)}, u32[]{:S(2)}, u32[]{:S(2)}) collective-permute-start(bf16[336,2048]{1,0:T(8,128)(2,1)} %get-tuple-element.16), channel_id=1, source_target_pairs={{0,1},{1,0},{2,3},{3,2},{4,5},{5,4},{6,7},{7,6},{8,9},{9,8},{10,11... | collective-permute-start | bytes 4128776 | tf_op jit(solution)/shard_map/ppermute | solution.py:24
  25.7 12.3 %all-to-all-done = bf16[64,32,128]{2,1,0:T(8,128)(2,1)S(1)} async-done(((bf16[64,32,128]{2,1,0:T(8,128)(2,1)}), bf16[64,32,128]{2,1,0:T(8,128)(2,1)S(1)}, u32[]{:S(2)}, u32[]{:S(2)}) %all-to-all-start) | async-done | bytes 524320 | tf_op jit(solution)/shard_map/all_to_all | solution.py:29
  38.0 0.0 copy-start.3
  38.0 0.3 multiply_reduce_fusion.2
  38.3 0.1 select_convert_fusion.1
  38.4 0.0 collective-permute-done
  38.4 0.0 copy-start.2
  38.4 0.1 fusion.21
  38.5 1.0 copy-done.2
  39.5 0.0 copy-done.3
  39.5 0.0 copy-done.4
  39.5 0.2 pad_maximum_fusion
  39.7 0.0 copy-start.5
  39.7 0.8 slice-done
  40.5 0.2 fusion.24
  40.7 0.0 copy-done.5
  40.7 0.0 copy-start.8
  40.7 0.2 select_convert_fusion.2
  41.0 0.1 copy.32
  41.1 18.6 %all_to_all.25 = bf16[128,2,128]{2,1,0:T(2,128)(2,1)S(1)} all-to-all(bf16[128,2,128]{2,1,0:T(2,128)(2,1)S(1)} %bitcast.79), channel_id=1, replica_groups=mesh['dp'=4,'za'=2,'zb'=2,'zc'=2,'ya'=2,'yb'=2,'yc'=2,'tp'=2] {'tp','za'..., dimensions={0} | all-to-all | bytes 131072 | tf_op jit(solution)/shard_map/all_to_all | solution.py:201
  59.7 0.1 convert_reduce_fusion.1
  59.8 0.2 slice_reduce_fusion
  60.0 0.1 copy_multiply_fusion
  60.1 0.1 copy.34
  60.2 0.1 copy.38
  60.3 0.1 squeeze.22
  60.4 0.1 copy.37
  60.5 0.1 mul.150
  60.5 0.1 copy.36
  60.6 0.1 div.36
  60.7 0.0 copy-done.8
  60.7 1.8 %multiply_add_fusion = f32[2,8,128,128]{3,2,1,0:T(8,128)S(1)} fusion(f32[2,8,128,128]{3,2,1,0:T(8,128)} %param.25, f32[2,8,128]{2,1,0:T(8,128)S(1)} %mul.150, f32[2,8,128]{2,1,0:T(8,128)S(1)} %get-tuple-element.30, f32[2,8,128]{2,1,0:T(8,128)S(1)} %get-tuple-element.31), kind=kLoop, calls=%fused_computation.9 | loop fusion | flops 786432 | bytes 2121728 | tf_op jit(solution)/shard_map/add | solution.py:215
  62.6 0.0 copy-start.1
  62.6 0.1 copy.35
  62.7 0.1 mul.143
  62.8 0.0 copy-start.7
  62.8 0.3 multiply_reduce_fusion.1
  63.1 0.1 multiply_reduce_fusion.3
  63.2 0.1 multiply_bitcast_fusion
  63.3 0.0 copy-done
  63.3 0.1 broadcast_in_dim.61
  63.5 19.6 %all_to_all.26 = bf16[64,2,1024]{2,1,0:T(2,128)(2,1)} all-to-all(bf16[64,2,1024]{2,1,0:T(2,128)(2,1)S(1)} %broadcast_in_dim.61), channel_id=1, replica_groups=mesh['dp'=4,'za'=2,'zb'=2,'zc'=2,'ya'=2,'yb'=2,'yc'=2,'tp'=2] {'za','zb'..., dimensions={0} | all-to-all | bytes 524288 | tf_op jit(solution)/shard_map/all_to_all | solution.py:29
  83.1 1.0 reshape.148
  84.2 0.2 fusion.25
  84.3 0.0 copy-done.1
  84.4 1.9 %collective-permute-start.1 = (f32[32,128]{1,0:T(8,128)S(1)}, f32[32,128]{1,0:T(8,128)S(1)}, u32[]{:S(2)}, u32[]{:S(2)}) collective-permute-start(f32[32,128]{1,0:T(8,128)S(1)} %fusion.25), channel_id=1, source_target_pairs={{0,1},{1,0},{2,3},{3,2},{4,5},{5,4},{6,7},{7,6},{8,9},{9,8},{10,11... | collective-permute-start | bytes 49160 | tf_op jit(solution)/shard_map/ppermute | solution.py:24
  86.3 1.1 collective-permute-done.1
  87.4 0.0 copy-done.6
  87.4 0.0 copy-done.7
  87.5 0.2 fusion.1
  87.6 0.1 broadcast_in_dim.62
  87.7 23.6 %all_to_all.27 = bf16[64,32,128]{2,1,0:T(8,128)(2,1)S(1)} all-to-all(bf16[64,32,128]{2,1,0:T(8,128)(2,1)S(1)} %broadcast_in_dim.62), channel_id=1, replica_groups=mesh['dp'=4,'za'=2,'zb'=2,'zc'=2,'ya'=2,'yb'=2,'yc'=2,'tp'=2] {'zc','yc'..., dimensions={0} | all-to-all | bytes 1048576 | tf_op jit(solution)/shard_map/all_to_all | solution.py:29
  111.3 0.4 fusion.26
  111.8 0.3 multiply_reduce_fusion
  112.1 1.9 %collective-permute-start.2 = (f32[257,128]{1,0:T(8,128)S(1)}, f32[257,128]{1,0:T(8,128)S(1)}, u32[]{:S(2)}, u32[]{:S(2)}) collective-permute-start(f32[257,128]{1,0:T(8,128)S(1)} %pad_maximum_fusion.2), channel_id=1, source_target_pairs={{0,1},{1,0},{2,3},{3,2},{4,5},{5,4},{6,7},{7,6},{8,9},{9,8},{10,11... | collective-permute-start | bytes 394760 | tf_op jit(solution)/shard_map/ppermute | solution.py:24
  114.0 1.3 collective-permute-done.2
  115.3 0.5 convolution_convert_fusion
  115.8 24.9 %all_to_all.28 = bf16[64,32,128]{2,1,0:T(8,128)(2,1)S(1)} all-to-all(bf16[64,32,128]{2,1,0:T(8,128)(2,1)S(1)} %bitcast.76), channel_id=1, replica_groups=mesh['dp'=4,'za'=2,'zb'=2,'zc'=2,'ya'=2,'yb'=2,'yc'=2,'tp'=2] {'zc','yc'..., dimensions={0} | all-to-all | bytes 1048576 | tf_op jit(solution)/shard_map/all_to_all | solution.py:238
  140.8 0.1 convert_reduce_fusion
  140.9 0.6 fusion.15
  (20 shorter events, 0.2 us)
Async XLA Ops:
  0.6 62.7 %copy-start = (f32[128]{0:T(128)S(1)}, f32[128]{0:T(128)}, u32[]{:S(2)}) copy-start(f32[128]{0:T(128)} %param.19) | copy-start | bytes 1540
  2.2 35.8 %all-to-all-start = ((bf16[64,32,128]{2,1,0:T(8,128)(2,1)}), bf16[64,32,128]{2,1,0:T(8,128)(2,1)S(1)}, u32[]{:S(2)}, u32[]{:S(2)}) async-start(bf16[64,32,128]{2,1,0:T(8,128)(2,1)} %broadcast_in_dim.34), calls=%async_computation | async-start | bytes 1048576 | tf_op jit(solution)/shard_map/all_to_all | solution.py:29
  23.7 14.7 %collective-permute-start = (bf16[336,2048]{1,0:T(8,128)(2,1)}, bf16[336,2048]{1,0:T(8,128)(2,1)S(1)}, u32[]{:S(2)}, u32[]{:S(2)}) collective-permute-start(bf16[336,2048]{1,0:T(8,128)(2,1)} %get-tuple-element.16), channel_id=1, source_target_pairs={{0,1},{1,0},{2,3},{3,2},{4,5},{5,4},{6,7},{7,6},{8,9},{9,8},{10,11... | collective-permute-start | bytes 4128776 | tf_op jit(solution)/shard_map/ppermute | solution.py:24
  38.0 1.5 %copy-start.3 = (bf16[128,2048]{1,0:T(8,128)(2,1)S(1)}, bf16[128,2048]{1,0:T(8,128)(2,1)}, u32[]{:S(2)}) copy-start(bf16[128,2048]{1,0:T(8,128)(2,1)} %get-tuple-element.19) | copy-start | bytes 1572868
  38.0 1.5 %copy-start.4 = (bf16[128,2048]{1,0:T(8,128)(2,1)S(1)}, bf16[128,2048]{1,0:T(8,128)(2,1)}, u32[]{:S(2)}) copy-start(bf16[128,2048]{1,0:T(8,128)(2,1)} %get-tuple-element.20) | copy-start | bytes 1572868
  38.4 1.1 copy-start.2
  39.5 1.0 slice-start
  39.7 1.0 copy-start.5
  40.7 20.0 %copy-start.8 = (f32[1024]{0:T(1024)S(1)}, f32[1024]{0:T(1024)}, u32[]{:S(2)}) copy-start(f32[1024]{0:T(1024)} %param.18) | copy-start | bytes 12292
  62.6 21.8 %copy-start.1 = (f32[2,8,128,128]{3,2,1,0:T(8,128)}, f32[2,8,128,128]{3,2,1,0:T(8,128)S(1)}, u32[]{:S(2)}) copy-start(f32[2,8,128,128]{3,2,1,0:T(8,128)S(1)} %multiply_add_fusion) | copy-start | bytes 3145732
  62.8 24.7 %copy-start.6 = (bf16[32,1024]{1,0:T(8,128)(2,1)S(1)}, bf16[32,1024]{1,0:T(8,128)(2,1)}, u32[]{:S(2)}) copy-start(bf16[32,1024]{1,0:T(8,128)(2,1)} %get-tuple-element.21) | copy-start | bytes 196612
  62.8 24.7 %copy-start.7 = (bf16[128,32]{0,1:T(8,128)(2,1)S(1)}, bf16[128,32]{0,1:T(8,128)(2,1)}, u32[]{:S(2)}) copy-start(bf16[128,32]{0,1:T(8,128)(2,1)} %param.13) | copy-start | bytes 24580
  84.4 3.1 %collective-permute-start.1 = (f32[32,128]{1,0:T(8,128)S(1)}, f32[32,128]{1,0:T(8,128)S(1)}, u32[]{:S(2)}, u32[]{:S(2)}) collective-permute-start(f32[32,128]{1,0:T(8,128)S(1)} %fusion.25), channel_id=1, source_target_pairs={{0,1},{1,0},{2,3},{3,2},{4,5},{5,4},{6,7},{7,6},{8,9},{9,8},{10,11... | collective-permute-start | bytes 49160 | tf_op jit(solution)/shard_map/ppermute | solution.py:24
  112.1 3.2 %collective-permute-start.2 = (f32[257,128]{1,0:T(8,128)S(1)}, f32[257,128]{1,0:T(8,128)S(1)}, u32[]{:S(2)}, u32[]{:S(2)}) collective-permute-start(f32[257,128]{1,0:T(8,128)S(1)} %pad_maximum_fusion.2), channel_id=1, source_target_pairs={{0,1},{1,0},{2,3},{3,2},{4,5},{5,4},{6,7},{7,6},{8,9},{9,8},{10,11... | collective-permute-start | bytes 394760 | tf_op jit(solution)/shard_map/ppermute | solution.py:24

commit v9 on v6

--- a/solution.py
+++ b/solution.py
@@ -165,17 +165,18 @@
     second, third = first + hidden_local, first + 2 * hidden_local
     span = lent.shape[1] // 2
     lent_out = jnp.concatenate([lent[third:, :span], lent[third:, span:]], axis=0)
+    mix_both = jnp.concatenate([own_mix, lent[:first]], axis=0)
     up_both = jnp.concatenate([own_up, lent[first:second]], axis=0)
     down_both = jnp.concatenate([own_down, lent[second:third]], axis=0)
-    lent_mix, own_mix, own_out, lent_out, up_both, down_both = lax.optimization_barrier(
-        (lent[:first], own_mix, own_out, lent_out, up_both, down_both)
+    mix_both, own_out, lent_out, up_both, down_both = lax.optimization_barrier(
+        (mix_both, own_out, lent_out, up_both, down_both)
     )
     sums = square_sums(token_half)
     high = sums.astype(jnp.bfloat16).astype(jnp.float32)
     place = lax.broadcasted_iota(jnp.int32, (128 - 4 * columns, rows), 0)
     extra = jnp.where(place == 0, high, jnp.where(place == 1, sums - high, 0.0))
-    own = contracted(own_mix, token_half, (1, 0))
-    theirs = contracted(lent_mix, token_half, (1, 0))
+    products = contracted(mix_both, token_half, (1, 0))
+    own, theirs = products[: 4 * columns], products[4 * columns :]
     first, second = jnp.where(tp == 0, own, theirs), jnp.where(tp == 0, theirs, own)
     raw = jnp.stack(
         [jnp.concatenate([part, extra], axis=0).T for part in (first, second)]
@@ -189,17 +190,25 @@
     raw = raw[:, :, : 4 * columns] * scale[None, :, None]
     raw = raw.reshape(chips, seq_local, 4, columns).transpose(2, 1, 0, 3)
     raw = raw.reshape(4, seq_local, heads_local, head_size)
+    raw = lax.optimization_barrier([raw[part] for part in range(4)])
     query_vec = raw[0] * head_size ** (-0.5)
     floor_heads = gate_floor.reshape(heads_local, head_size)
     forget_gate = floor_heads + (1.0 - floor_heads) * jax.nn.sigmoid(raw[1])
     input_vec = raw[2]
     gate_vec = raw[3]
-    new_state = (
-        forget_gate[..., None] * state + (1.0 - forget_gate)[..., None] * input_vec[:, :, None, :]
-    )
-    head_out = jnp.sum(query_vec[..., None] * new_state, axis=2)
+    kept = jnp.sum((query_vec * forget_gate)[..., None] * state, axis=2)
+    added = jnp.sum(query_vec * (1.0 - forget_gate), axis=-1, keepdims=True) * input_vec
+    head_out = lax.optimization_barrier(kept) + added
     branch = rms_scale(head_out, head_gain) * jax.nn.silu(gate_vec)
     branch = branch.reshape(seq_local, heads_local * head_size).astype(jnp.bfloat16)
+
+    branch, state, forget_gate, input_vec = lax.optimization_barrier(
+        (branch, state, forget_gate, input_vec)
+    )
+    new_state = (
+        forget_gate[..., None] * state
+        + (1.0 - forget_gate)[..., None] * input_vec[:, :, None, :]
+    )
 
     branch_half = gathered(branch).reshape(rows, heads_local * head_size)
     theirs = swapped(contracted(lent_out, branch_half, (1, 1)))

time: 140 us -> 141 us (level)
  the two profiles are of different devices: /device:TPU:6 before, /device:TPU:4 now
where the time goes in v9:
time: 141 us
  blocking collectives  60.3 us (43%)
  waiting for transfers between devices  33.9 us (24%)
  starting transfers between devices  28.3 us (20%)
  other arithmetic  6.23 us (4%)
  Pallas kernels  4.53 us (3%)
  local copies, waits for them, and re-layouts  4.03 us (3%)
  matrix products  2.36 us (2%)
    all_to_all x2, blocking collectives, gathered(): lax.all_to_all(jnp.broadcast_to(x[None], (chips, *x.shape)), KV, 0, 0, ti...  42.3 us
    all_to_all x1, waiting for transfers between devices, per_device(): lax.all_to_all(terms.reshape(chips, share, rows), KV, split_axis=0, conca...  18.2 us
    all_to_all x1, blocking collectives, per_device(): lax.all_to_all(raw, ('tp', *KV), split_axis=0, concat_axis=0, tiled=True)  18.1 us
    all_to_all x1, starting transfers between devices, gathered(): lax.all_to_all(jnp.broadcast_to(x[None], (chips, *x.shape)), KV, 0, 0, ti...  16.6 us
    all_to_all x1, waiting for transfers between devices, gathered(): lax.all_to_all(jnp.broadcast_to(x[None], (chips, *x.shape)), KV, 0, 0, ti...  13.3 us
    ppermute x3, starting transfers between devices, swapped(): return lax.ppermute(x, 'tp', [(0, 1), (1, 0)])  5.9 us
    all_to_all x1, starting transfers between devices, per_device(): lax.all_to_all(terms.reshape(chips, share, rows), KV, split_axis=0, conca...  5.83 us
    pallas_call x1, Pallas kernels, split_weights(): pl.pallas_call(lambda *refs: split_kernel(share, *refs), out_shape=[jax.S...  4.53 us
  transfers between devices with their start and end apart: 5, of which 4 were waited for; matrix products, arithmetic and copies ran while one was open for 1% of the time, Pallas kernels for 3%

profile of v9, /device:TPU:4, one launch (start us, length us, event | category | flops | bytes accessed | tf_op | source)
XLA Modules:
  0.0 140.6 jit_solution(15842469286848536830)
XLA Ops:
  0.6 1.6 %broadcast_in_dim.34 = bf16[64,32,128]{2,1,0:T(8,128)(2,1)} broadcast(bf16[32,128]{1,0:T(8,128)(2,1)} %bitcast.77), dimensions={1,2} | broadcast | bytes 532480 | tf_op jit(solution)/shard_map/broadcast_in_dim | solution.py:28
  2.2 16.6 %all-to-all-start = ((bf16[64,32,128]{2,1,0:T(8,128)(2,1)}), bf16[64,32,128]{2,1,0:T(8,128)(2,1)S(1)}, u32[]{:S(2)}, u32[]{:S(2)}) async-start(bf16[64,32,128]{2,1,0:T(8,128)(2,1)} %broadcast_in_dim.34), calls=%async_computation | async-start | bytes 1048576 | tf_op jit(solution)/shard_map/all_to_all | solution.py:28
  18.8 4.5 %shard_map.140 = (bf16[64,2048]{1,0:T(8,128)(2,1)}, bf16[128,2048]{1,0:T(8,128)(2,1)}, bf16[128,2048]{1,0:T(8,128)(2,1)}, bf16[32,1024]{1,0:T(8,128)(2,1)}, bf16[336,2048]{1,0:T(8,128)(2,1)}) custom-call(s32[1]{0:T(128)} %bitcast.1.refs_0_, bf16[16,4096]{1,0:T(8,128)(2,1)} %bitcast.72, bf16[16,4096]{1,0:T(8,128)(2,1)} %bitcast.73, ...), custom_call_target="tpu_custom_call" | custom-call | tf_op jit(solution)/shard_map/pallas_call | solution.py:119
  23.3 1.9 %collective-permute-start = (bf16[336,2048]{1,0:T(8,128)(2,1)}, bf16[336,2048]{1,0:T(8,128)(2,1)S(1)}, u32[]{:S(2)}, u32[]{:S(2)}) collective-permute-start(bf16[336,2048]{1,0:T(8,128)(2,1)} %get-tuple-element.24), channel_id=1, source_target_pairs={{0,1},{1,0},{2,3},{3,2},{4,5},{5,4},{6,7},{7,6},{8,9},{9,8},{10,11... | collective-permute-start | bytes 4128776 | tf_op jit(solution)/shard_map/ppermute | solution.py:23
  25.3 13.3 %all-to-all-done = bf16[64,32,128]{2,1,0:T(8,128)(2,1)S(1)} async-done(((bf16[64,32,128]{2,1,0:T(8,128)(2,1)}), bf16[64,32,128]{2,1,0:T(8,128)(2,1)S(1)}, u32[]{:S(2)}, u32[]{:S(2)}) %all-to-all-start) | async-done | bytes 524320 | tf_op jit(solution)/shard_map/all_to_all | solution.py:28
  38.5 0.3 multiply_reduce_fusion.2
  38.8 0.1 select_convert_fusion.1
  38.9 0.0 collective-permute-done
  38.9 1.0 pad_maximum_fusion.2
  39.9 0.0 copy-start.2
  39.9 0.0 copy-start.3
  40.0 0.1 fusion.23
  40.1 0.9 copy-done.2
  41.0 0.2 copy-done.3
  41.1 1.1 pad_maximum_fusion
  42.2 0.0 copy-start.6
  42.3 0.0 copy-start
  42.3 0.3 fusion.27
  42.6 0.0 copy-start.7
  42.6 0.1 copy.32
  42.7 18.1 %all_to_all.25 = bf16[128,2,128]{2,1,0:T(2,128)(2,1)S(1)} all-to-all(bf16[128,2,128]{2,1,0:T(2,128)(2,1)S(1)} %bitcast.70), channel_id=1, replica_groups=mesh['dp'=4,'kv_0'=8,'kv_1'=8,'tp'=2] {'tp','kv_0','kv_1'}, dimensions={0} | all-to-all | bytes 131072 | tf_op jit(solution)/shard_map/all_to_all | solution.py:185
  60.8 0.1 convert_reduce_fusion.1
  60.9 0.2 slice_reduce_fusion
  61.1 0.1 copy_multiply_fusion
  61.1 0.1 copy.34
  61.2 0.1 copy.35
  61.3 0.1 squeeze.29
  61.4 0.1 copy.36
  61.5 0.1 squeeze.30
  61.6 0.1 copy.37
  61.7 0.1 squeeze.31
  61.7 0.1 copy.38
  61.8 0.1 squeeze.32
  61.9 0.0 copy-done.6
  62.0 0.0 copy-done
  62.0 0.0 copy-start.4
  62.0 0.0 copy-start.5
  62.0 0.3 multiply_reduce_fusion.1
  62.3 0.3 multiply_reduce_fusion.3
  62.7 0.0 copy-done.7
  62.7 0.1 fusion.15
  62.8 0.1 broadcast_in_dim.38
  62.9 18.9 %all_to_all.26 = bf16[64,2,1024]{2,1,0:T(2,128)(2,1)S(1)} all-to-all(bf16[64,2,1024]{2,1,0:T(2,128)(2,1)S(1)} %broadcast_in_dim.38), channel_id=1, replica_groups=mesh['dp'=4,'kv_0'=8,'kv_1'=8,'tp'=2] {'kv_0','kv_1'}, dimensions={0} | all-to-all | bytes 524288 | tf_op jit(solution)/shard_map/all_to_all | solution.py:28
  81.9 0.1 reshape.81
  82.0 0.0 copy-start.1
  82.0 0.2 fusion.28
  82.2 2.1 %collective-permute-start.1 = (f32[32,128]{1,0:T(8,128)S(1)}, f32[32,128]{1,0:T(8,128)S(1)}, u32[]{:S(2)}, u32[]{:S(2)}) collective-permute-start(f32[32,128]{1,0:T(8,128)S(1)} %fusion.28), channel_id=1, source_target_pairs={{0,1},{1,0},{2,3},{3,2},{4,5},{5,4},{6,7},{7,6},{8,9},{9,8},{10,11... | collective-permute-start | bytes 49160 | tf_op jit(solution)/shard_map/ppermute | solution.py:23
  84.2 1.1 collective-permute-done.1
  85.4 0.0 copy-done.4
  85.4 0.0 copy-done.5
  85.4 0.2 fusion.2
  85.6 0.1 broadcast_in_dim.64
  85.7 23.3 %all_to_all.27 = bf16[64,32,128]{2,1,0:T(8,128)(2,1)S(1)} all-to-all(bf16[64,32,128]{2,1,0:T(8,128)(2,1)S(1)} %broadcast_in_dim.64), channel_id=1, replica_groups=mesh['dp'=4,'kv_0'=8,'kv_1'=8,'tp'=2] {'kv_0','kv_1'}, dimensions={0} | all-to-all | bytes 1048576 | tf_op jit(solution)/shard_map/all_to_all | solution.py:28
  109.0 0.0 copy-done.1
  109.0 0.4 fusion.29
  109.4 0.3 multiply_reduce_fusion
  109.7 1.9 %collective-permute-start.2 = (f32[257,128]{1,0:T(8,128)S(1)}, f32[257,128]{1,0:T(8,128)S(1)}, u32[]{:S(2)}, u32[]{:S(2)}) collective-permute-start(f32[257,128]{1,0:T(8,128)S(1)} %pad_maximum_fusion.3), channel_id=1, source_target_pairs={{0,1},{1,0},{2,3},{3,2},{4,5},{5,4},{6,7},{7,6},{8,9},{9,8},{10,11... | collective-permute-start | bytes 394760 | tf_op jit(solution)/shard_map/ppermute | solution.py:23
  111.7 1.3 collective-permute-done.2
  113.0 1.3 convolution_convert_fusion
  114.3 5.8 %all-to-all-start.4 = ((bf16[64,32,128]{2,1,0:T(8,128)(2,1)}), bf16[64,32,128]{2,1,0:T(8,128)(2,1)S(1)}, u32[]{:S(2)}, u32[]{:S(2)}) async-start(bf16[64,32,128]{2,1,0:T(8,128)(2,1)} %bitcast.27), calls=%async_computation.4 | async-start | bytes 1048576 | tf_op jit(solution)/shard_map/all_to_all | solution.py:229
  120.1 1.6 %multiply_add_fusion = f32[2,8,128,128]{3,2,1,0:T(8,128)} fusion(f32[2,8,128,128]{3,2,1,0:T(8,128)S(1)} %copy-done, f32[2,8,128]{2,1,0:T(8,128)S(1)} %squeeze.31, f32[2,8,128]{2,1,0:T(8,128)S(1)} %broadcast_subtract_fusion, f32[2,8,128]{2,1,0:T(8,128)S(1)} %get-tuple-element.41), kind=kLoop, calls=%fused_computation.9 | loop fusion | flops 786432 | bytes 2121728 | tf_op jit(solution)/shard_map/add | solution.py:209
  121.7 18.2 %all-to-all-done.4 = bf16[64,32,128]{2,1,0:T(8,128)(2,1)S(1)} async-done(((bf16[64,32,128]{2,1,0:T(8,128)(2,1)}), bf16[64,32,128]{2,1,0:T(8,128)(2,1)S(1)}, u32[]{:S(2)}, u32[]{:S(2)}) %all-to-all-start.4) | async-done | bytes 524320 | tf_op jit(solution)/shard_map/all_to_all | solution.py:229
  139.9 0.1 convert_reduce_fusion
  140.0 0.6 fusion.14
  (19 shorter events, 0.2 us)
Async XLA Ops:
  2.2 36.3 %all-to-all-start = ((bf16[64,32,128]{2,1,0:T(8,128)(2,1)}), bf16[64,32,128]{2,1,0:T(8,128)(2,1)S(1)}, u32[]{:S(2)}, u32[]{:S(2)}) async-start(bf16[64,32,128]{2,1,0:T(8,128)(2,1)} %broadcast_in_dim.34), calls=%async_computation | async-start | bytes 1048576 | tf_op jit(solution)/shard_map/all_to_all | solution.py:28
  23.3 15.6 %collective-permute-start = (bf16[336,2048]{1,0:T(8,128)(2,1)}, bf16[336,2048]{1,0:T(8,128)(2,1)S(1)}, u32[]{:S(2)}, u32[]{:S(2)}) collective-permute-start(bf16[336,2048]{1,0:T(8,128)(2,1)} %get-tuple-element.24), channel_id=1, source_target_pairs={{0,1},{1,0},{2,3},{3,2},{4,5},{5,4},{6,7},{7,6},{8,9},{9,8},{10,11... | collective-permute-start | bytes 4128776 | tf_op jit(solution)/shard_map/ppermute | solution.py:23
  39.9 1.0 copy-start.2
  39.9 1.2 copy-start.3
  42.2 19.7 %copy-start.6 = (f32[1024]{0:T(1024)S(1)}, f32[1024]{0:T(1024)}, u32[]{:S(2)}) copy-start(f32[1024]{0:T(1024)} %param.18) | copy-start | bytes 12292
  42.3 19.7 %copy-start = (f32[2,8,128,128]{3,2,1,0:T(8,128)S(1)}, f32[2,8,128,128]{3,2,1,0:T(8,128)}, u32[]{:S(2)}) copy-start(f32[2,8,128,128]{3,2,1,0:T(8,128)} %param.25) | copy-start | bytes 3145732
  42.6 20.1 %copy-start.7 = (f32[128]{0:T(128)S(1)}, f32[128]{0:T(128)}, u32[]{:S(2)}) copy-start(f32[128]{0:T(128)} %param.19) | copy-start | bytes 1540
  62.0 23.4 %copy-start.4 = (bf16[32,1024]{1,0:T(8,128)(2,1)S(1)}, bf16[32,1024]{1,0:T(8,128)(2,1)}, u32[]{:S(2)}) copy-start(bf16[32,1024]{1,0:T(8,128)(2,1)} %get-tuple-element.28) | copy-start | bytes 196612
  62.0 23.4 %copy-start.5 = (bf16[128,32]{0,1:T(8,128)(2,1)S(1)}, bf16[128,32]{0,1:T(8,128)(2,1)}, u32[]{:S(2)}) copy-start(bf16[128,32]{0,1:T(8,128)(2,1)} %param.13) | copy-start | bytes 24580
  82.0 27.0 %copy-start.1 = (bf16[256,2048]{1,0:T(8,128)(2,1)S(1)}, bf16[256,2048]{1,0:T(8,128)(2,1)}, u32[]{:S(2)}) copy-start(bf16[256,2048]{1,0:T(8,128)(2,1)} %get-tuple-element.40) | copy-start | bytes 3145732
  82.2 3.2 %collective-permute-start.1 = (f32[32,128]{1,0:T(8,128)S(1)}, f32[32,128]{1,0:T(8,128)S(1)}, u32[]{:S(2)}, u32[]{:S(2)}) collective-permute-start(f32[32,128]{1,0:T(8,128)S(1)} %fusion.28), channel_id=1, source_target_pairs={{0,1},{1,0},{2,3},{3,2},{4,5},{5,4},{6,7},{7,6},{8,9},{9,8},{10,11... | collective-permute-start | bytes 49160 | tf_op jit(solution)/shard_map/ppermute | solution.py:23
  109.7 3.2 %collective-permute-start.2 = (f32[257,128]{1,0:T(8,128)S(1)}, f32[257,128]{1,0:T(8,128)S(1)}, u32[]{:S(2)}, u32[]{:S(2)}) collective-permute-start(f32[257,128]{1,0:T(8,128)S(1)} %pad_maximum_fusion.3), channel_id=1, source_target_pairs={{0,1},{1,0},{2,3},{3,2},{4,5},{5,4},{6,7},{7,6},{8,9},{9,8},{10,11... | collective-permute-start | bytes 394760 | tf_op jit(solution)/shard_map/ppermute | solution.py:23
  114.3 25.6 %all-to-all-start.4 = ((bf16[64,32,128]{2,1,0:T(8,128)(2,1)}), bf16[64,32,128]{2,1,0:T(8,128)(2,1)S(1)}, u32[]{:S(2)}, u32[]{:S(2)}) async-start(bf16[64,32,128]{2,1,0:T(8,128)(2,1)} %bitcast.27), calls=%async_computation.4 | async-start | bytes 1048576 | tf_op jit(solution)/shard_map/all_to_all | solution.py:229

commit v10 on v6

--- a/solution.py
+++ b/solution.py
@@ -189,17 +189,23 @@
     raw = raw[:, :, : 4 * columns] * scale[None, :, None]
     raw = raw.reshape(chips, seq_local, 4, columns).transpose(2, 1, 0, 3)
     raw = raw.reshape(4, seq_local, heads_local, head_size)
+    raw = lax.optimization_barrier([raw[part] for part in range(4)])
     query_vec = raw[0] * head_size ** (-0.5)
     floor_heads = gate_floor.reshape(heads_local, head_size)
     forget_gate = floor_heads + (1.0 - floor_heads) * jax.nn.sigmoid(raw[1])
     input_vec = raw[2]
     gate_vec = raw[3]
-    new_state = (
-        forget_gate[..., None] * state + (1.0 - forget_gate)[..., None] * input_vec[:, :, None, :]
-    )
-    head_out = jnp.sum(query_vec[..., None] * new_state, axis=2)
+    kept = jnp.sum((query_vec * forget_gate)[..., None] * state, axis=2)
+    added = jnp.sum(query_vec * (1.0 - forget_gate), axis=-1, keepdims=True) * input_vec
+    head_out = lax.optimization_barrier(kept) + added
     branch = rms_scale(head_out, head_gain) * jax.nn.silu(gate_vec)
     branch = branch.reshape(seq_local, heads_local * head_size).astype(jnp.bfloat16)
+
+    branch, state, forget_gate, input_vec = lax.optimization_barrier(
+        (branch, state, forget_gate, input_vec)
+    )
+    given = input_vec[:, :, None, :]
+    new_state = given + forget_gate[..., None] * (state - given)
 
     branch_half = gathered(branch).reshape(rows, heads_local * head_size)
     theirs = swapped(contracted(lent_out, branch_half, (1, 1)))

time: 140 us -> 142 us (1.014)
  blocking collectives: 85.8 us -> 60.3 us
  waiting for transfers between devices: 15.7 us -> 34.1 us
  starting transfers between devices: 22.4 us -> 28.3 us
    all_to_all x1 -> x0, blocking collectives: 25.4 us -> none  [per_device(): lax.all_to_all(terms.reshape(chips, share, rows), KV, split_axis=0, conca...]
    all_to_all x0 -> x1, waiting for transfers between devices: none -> 18.5 us  [per_device(): lax.all_to_all(terms.reshape(chips, share, rows), KV, split_axis=0, conca...]
    all_to_all x0 -> x1, starting transfers between devices: none -> 5.83 us  [per_device(): lax.all_to_all(terms.reshape(chips, share, rows), KV, split_axis=0, conca...]
    reduce_sum x2 -> x1, other arithmetic: 1.85 us -> 0.35 us  [per_device(): kept = jnp.sum((query_vec * forget_gate)[..., None] * state, axis=2)]
  transfers between devices with their start and end apart: 4 -> 5, of which waited for: 3 -> 4; matrix products, arithmetic and copies ran while one was open for 0% -> 1% of each run, Pallas kernels for 3% -> 3%
where the time goes in v10:
time: 142 us
  blocking collectives  60.3 us (42%)
  waiting for transfers between devices  34.1 us (24%)
  starting transfers between devices  28.3 us (20%)
  local copies, waits for them, and re-layouts  5.95 us (4%)
  other arithmetic  5.02 us (4%)
  Pallas kernels  4.54 us (3%)
  matrix products  2.53 us (2%)
    all_to_all x2, blocking collectives, gathered(): lax.all_to_all(jnp.broadcast_to(x[None], (chips, *x.shape)), KV, 0, 0, ti...  42.3 us
    all_to_all x1, waiting for transfers between devices, per_device(): lax.all_to_all(terms.reshape(chips, share, rows), KV, split_axis=0, conca...  18.5 us
    all_to_all x1, blocking collectives, per_device(): lax.all_to_all(raw, ('tp', *KV), split_axis=0, concat_axis=0, tiled=True)  18.1 us
    all_to_all x1, starting transfers between devices, gathered(): lax.all_to_all(jnp.broadcast_to(x[None], (chips, *x.shape)), KV, 0, 0, ti...  16.6 us
    all_to_all x1, waiting for transfers between devices, gathered(): lax.all_to_all(jnp.broadcast_to(x[None], (chips, *x.shape)), KV, 0, 0, ti...  13.2 us
    ppermute x3, starting transfers between devices, swapped(): return lax.ppermute(x, 'tp', [(0, 1), (1, 0)])  5.9 us
    all_to_all x1, starting transfers between devices, per_device(): lax.all_to_all(terms.reshape(chips, share, rows), KV, split_axis=0, conca...  5.83 us
    pallas_call x1, Pallas kernels, split_weights(): pl.pallas_call(lambda *refs: split_kernel(share, *refs), out_shape=[jax.S...  4.54 us
  transfers between devices with their start and end apart: 5, of which 4 were waited for; matrix products, arithmetic and copies ran while one was open for 1% of the time, Pallas kernels for 3%

profile of v10, /device:TPU:6, one launch (start us, length us, event | category | flops | bytes accessed | tf_op | source)
XLA Modules:
  0.0 141.8 jit_solution(575507965890903360)
XLA Ops:
  0.6 1.6 %broadcast_in_dim.34 = bf16[64,32,128]{2,1,0:T(8,128)(2,1)} broadcast(bf16[32,128]{1,0:T(8,128)(2,1)} %bitcast.80), dimensions={1,2} | broadcast | bytes 532480 | tf_op jit(solution)/shard_map/broadcast_in_dim | solution.py:28
  2.2 16.6 %all-to-all-start = ((bf16[64,32,128]{2,1,0:T(8,128)(2,1)}), bf16[64,32,128]{2,1,0:T(8,128)(2,1)S(1)}, u32[]{:S(2)}, u32[]{:S(2)}) async-start(bf16[64,32,128]{2,1,0:T(8,128)(2,1)} %broadcast_in_dim.34), calls=%async_computation | async-start | bytes 1048576 | tf_op jit(solution)/shard_map/all_to_all | solution.py:28
  18.8 4.5 %shard_map.140 = (bf16[64,2048]{1,0:T(8,128)(2,1)}, bf16[128,2048]{1,0:T(8,128)(2,1)}, bf16[128,2048]{1,0:T(8,128)(2,1)}, bf16[32,1024]{1,0:T(8,128)(2,1)}, bf16[336,2048]{1,0:T(8,128)(2,1)}) custom-call(s32[1]{0:T(128)} %bitcast.1.refs_0_, bf16[16,4096]{1,0:T(8,128)(2,1)} %bitcast.75, bf16[16,4096]{1,0:T(8,128)(2,1)} %bitcast.76, ...), custom_call_target="tpu_custom_call" | custom-call | tf_op jit(solution)/shard_map/pallas_call | solution.py:119
  23.3 1.9 %collective-permute-start = (bf16[336,2048]{1,0:T(8,128)(2,1)}, bf16[336,2048]{1,0:T(8,128)(2,1)S(1)}, u32[]{:S(2)}, u32[]{:S(2)}) collective-permute-start(bf16[336,2048]{1,0:T(8,128)(2,1)} %get-tuple-element.24), channel_id=1, source_target_pairs={{0,1},{1,0},{2,3},{3,2},{4,5},{5,4},{6,7},{7,6},{8,9},{9,8},{10,11... | collective-permute-start | bytes 4128776 | tf_op jit(solution)/shard_map/ppermute | solution.py:23
  25.3 0.0 copy-start.3
  25.3 13.2 %all-to-all-done = bf16[64,32,128]{2,1,0:T(8,128)(2,1)S(1)} async-done(((bf16[64,32,128]{2,1,0:T(8,128)(2,1)}), bf16[64,32,128]{2,1,0:T(8,128)(2,1)S(1)}, u32[]{:S(2)}, u32[]{:S(2)}) %all-to-all-start) | async-done | bytes 524320 | tf_op jit(solution)/shard_map/all_to_all | solution.py:28
  38.5 0.3 multiply_reduce_fusion.2
  38.8 0.1 select_convert_fusion.1
  38.9 0.0 collective-permute-done
  38.9 0.0 copy-start.2
  38.9 1.1 copy-done.2
  40.0 1.3 fusion.23
  41.3 0.0 copy-done.3
  41.3 0.0 copy-done.4
  41.4 0.0 slice-start
  41.4 1.2 pad_maximum_fusion
  42.5 0.0 slice-done
  42.5 0.2 fusion.27
  42.8 0.7 copy-done.5
  43.5 0.2 select_convert_fusion.2
  43.7 0.0 copy-start.9
  43.8 0.1 copy.32
  43.9 18.1 %all_to_all.25 = bf16[128,2,128]{2,1,0:T(2,128)(2,1)S(1)} all-to-all(bf16[128,2,128]{2,1,0:T(2,128)(2,1)S(1)} %bitcast.73), channel_id=1, replica_groups=mesh['dp'=4,'kv_0'=8,'kv_1'=8,'tp'=2] {'tp','kv_0','kv_1'}, dimensions={0} | all-to-all | bytes 131072 | tf_op jit(solution)/shard_map/all_to_all | solution.py:184
  62.0 0.1 convert_reduce_fusion.1
  62.0 0.2 slice_reduce_fusion
  62.2 0.1 copy_multiply_fusion
  62.3 0.1 copy.34
  62.4 0.1 copy.35
  62.5 0.1 squeeze.29
  62.6 0.1 copy.36
  62.6 0.1 squeeze.30
  62.7 0.1 copy.37
  62.8 0.1 squeeze.31
  62.9 0.1 copy.38
  63.0 0.1 squeeze.32
  63.1 0.0 copy-done.8
  63.1 0.0 copy-done
  63.1 0.0 copy-start.6
  63.1 0.0 copy-start.7
  63.1 0.3 multiply_reduce_fusion.1
  63.5 0.3 multiply_reduce_fusion.3
  63.9 0.0 copy-done.9
  63.9 0.1 fusion.15
  64.0 0.1 broadcast_in_dim.62
  64.1 18.9 %all_to_all.26 = bf16[64,2,1024]{2,1,0:T(2,128)(2,1)S(1)} all-to-all(bf16[64,2,1024]{2,1,0:T(2,128)(2,1)S(1)} %broadcast_in_dim.62), channel_id=1, replica_groups=mesh['dp'=4,'kv_0'=8,'kv_1'=8,'tp'=2] {'kv_0','kv_1'}, dimensions={0} | all-to-all | bytes 524288 | tf_op jit(solution)/shard_map/all_to_all | solution.py:28
  83.0 0.1 reshape.80
  83.1 0.0 copy-start.1
  83.2 0.2 fusion.28
  83.3 2.1 %collective-permute-start.1 = (f32[32,128]{1,0:T(8,128)S(1)}, f32[32,128]{1,0:T(8,128)S(1)}, u32[]{:S(2)}, u32[]{:S(2)}) collective-permute-start(f32[32,128]{1,0:T(8,128)S(1)} %fusion.28), channel_id=1, source_target_pairs={{0,1},{1,0},{2,3},{3,2},{4,5},{5,4},{6,7},{7,6},{8,9},{9,8},{10,11... | collective-permute-start | bytes 49160 | tf_op jit(solution)/shard_map/ppermute | solution.py:23
  85.4 1.1 collective-permute-done.1
  86.6 0.0 copy-done.6
  86.6 0.2 fusion.2
  86.7 0.1 broadcast_in_dim.63
  86.8 23.3 %all_to_all.27 = bf16[64,32,128]{2,1,0:T(8,128)(2,1)S(1)} all-to-all(bf16[64,32,128]{2,1,0:T(8,128)(2,1)S(1)} %broadcast_in_dim.63), channel_id=1, replica_groups=mesh['dp'=4,'kv_0'=8,'kv_1'=8,'tp'=2] {'kv_0','kv_1'}, dimensions={0} | all-to-all | bytes 1048576 | tf_op jit(solution)/shard_map/all_to_all | solution.py:28
  110.2 0.4 fusion.29
  110.6 0.3 multiply_reduce_fusion
  110.9 1.9 %collective-permute-start.2 = (f32[257,128]{1,0:T(8,128)S(1)}, f32[257,128]{1,0:T(8,128)S(1)}, u32[]{:S(2)}, u32[]{:S(2)}) collective-permute-start(f32[257,128]{1,0:T(8,128)S(1)} %pad_maximum_fusion.2), channel_id=1, source_target_pairs={{0,1},{1,0},{2,3},{3,2},{4,5},{5,4},{6,7},{7,6},{8,9},{9,8},{10,11... | collective-permute-start | bytes 394760 | tf_op jit(solution)/shard_map/ppermute | solution.py:23
  112.8 1.3 collective-permute-done.2
  114.2 1.3 convolution_convert_fusion
  115.5 5.8 %all-to-all-start.4 = ((bf16[64,32,128]{2,1,0:T(8,128)(2,1)}), bf16[64,32,128]{2,1,0:T(8,128)(2,1)S(1)}, u32[]{:S(2)}, u32[]{:S(2)}) async-start(bf16[64,32,128]{2,1,0:T(8,128)(2,1)} %bitcast.27), calls=%async_computation.4 | async-start | bytes 1048576 | tf_op jit(solution)/shard_map/all_to_all | solution.py:226
  121.3 1.3 multiply_add_fusion
  122.6 18.5 %all-to-all-done.4 = bf16[64,32,128]{2,1,0:T(8,128)(2,1)S(1)} async-done(((bf16[64,32,128]{2,1,0:T(8,128)(2,1)}), bf16[64,32,128]{2,1,0:T(8,128)(2,1)S(1)}, u32[]{:S(2)}, u32[]{:S(2)}) %all-to-all-start.4) | async-done | bytes 524320 | tf_op jit(solution)/shard_map/all_to_all | solution.py:226
  141.1 0.1 convert_reduce_fusion
  141.2 0.6 fusion.14
  (22 shorter events, 0.1 us)
Async XLA Ops:
  2.2 36.3 %all-to-all-start = ((bf16[64,32,128]{2,1,0:T(8,128)(2,1)}), bf16[64,32,128]{2,1,0:T(8,128)(2,1)S(1)}, u32[]{:S(2)}, u32[]{:S(2)}) async-start(bf16[64,32,128]{2,1,0:T(8,128)(2,1)} %broadcast_in_dim.34), calls=%async_computation | async-start | bytes 1048576 | tf_op jit(solution)/shard_map/all_to_all | solution.py:28
  23.3 15.6 %collective-permute-start = (bf16[336,2048]{1,0:T(8,128)(2,1)}, bf16[336,2048]{1,0:T(8,128)(2,1)S(1)}, u32[]{:S(2)}, u32[]{:S(2)}) collective-permute-start(bf16[336,2048]{1,0:T(8,128)(2,1)} %get-tuple-element.24), channel_id=1, source_target_pairs={{0,1},{1,0},{2,3},{3,2},{4,5},{5,4},{6,7},{7,6},{8,9},{9,8},{10,11... | collective-permute-start | bytes 4128776 | tf_op jit(solution)/shard_map/ppermute | solution.py:23
  25.3 16.1 %copy-start.3 = (bf16[128,2048]{1,0:T(8,128)(2,1)S(1)}, bf16[128,2048]{1,0:T(8,128)(2,1)}, u32[]{:S(2)}) copy-start(bf16[128,2048]{1,0:T(8,128)(2,1)} %get-tuple-element.27) | copy-start | bytes 1572868
  38.5 2.8 %copy-start.4 = (bf16[128,2048]{1,0:T(8,128)(2,1)S(1)}, bf16[128,2048]{1,0:T(8,128)(2,1)}, u32[]{:S(2)}) copy-start(bf16[128,2048]{1,0:T(8,128)(2,1)} %get-tuple-element.28) | copy-start | bytes 1572868
  38.9 1.1 copy-start.2
  41.4 1.2 slice-start
  42.5 0.9 copy-start.5
  43.5 19.6 %copy-start.8 = (f32[1024]{0:T(1024)S(1)}, f32[1024]{0:T(1024)}, u32[]{:S(2)}) copy-start(f32[1024]{0:T(1024)} %param.18) | copy-start | bytes 12292
  43.5 19.6 %copy-start = (f32[2,8,128,128]{3,2,1,0:T(8,128)S(1)}, f32[2,8,128,128]{3,2,1,0:T(8,128)}, u32[]{:S(2)}) copy-start(f32[2,8,128,128]{3,2,1,0:T(8,128)} %param.25) | copy-start | bytes 3145732
  43.7 20.1 %copy-start.9 = (f32[128]{0:T(128)S(1)}, f32[128]{0:T(128)}, u32[]{:S(2)}) copy-start(f32[128]{0:T(128)} %param.19) | copy-start | bytes 1540
  63.1 23.4 %copy-start.6 = (bf16[32,1024]{1,0:T(8,128)(2,1)S(1)}, bf16[32,1024]{1,0:T(8,128)(2,1)}, u32[]{:S(2)}) copy-start(bf16[32,1024]{1,0:T(8,128)(2,1)} %get-tuple-element.29) | copy-start | bytes 196612
  63.1 23.4 %copy-start.7 = (bf16[128,32]{0,1:T(8,128)(2,1)S(1)}, bf16[128,32]{0,1:T(8,128)(2,1)}, u32[]{:S(2)}) copy-start(bf16[128,32]{0,1:T(8,128)(2,1)} %param.13) | copy-start | bytes 24580
  83.1 27.0 %copy-start.1 = (bf16[256,2048]{1,0:T(8,128)(2,1)S(1)}, bf16[256,2048]{1,0:T(8,128)(2,1)}, u32[]{:S(2)}) copy-start(bf16[256,2048]{1,0:T(8,128)(2,1)} %get-tuple-element.42) | copy-start | bytes 3145732
  83.3 3.2 %collective-permute-start.1 = (f32[32,128]{1,0:T(8,128)S(1)}, f32[32,128]{1,0:T(8,128)S(1)}, u32[]{:S(2)}, u32[]{:S(2)}) collective-permute-start(f32[32,128]{1,0:T(8,128)S(1)} %fusion.28), channel_id=1, source_target_pairs={{0,1},{1,0},{2,3},{3,2},{4,5},{5,4},{6,7},{7,6},{8,9},{9,8},{10,11... | collective-permute-start | bytes 49160 | tf_op jit(solution)/shard_map/ppermute | solution.py:23
  110.9 3.2 %collective-permute-start.2 = (f32[257,128]{1,0:T(8,128)S(1)}, f32[257,128]{1,0:T(8,128)S(1)}, u32[]{:S(2)}, u32[]{:S(2)}) collective-permute-start(f32[257,128]{1,0:T(8,128)S(1)} %pad_maximum_fusion.2), channel_id=1, source_target_pairs={{0,1},{1,0},{2,3},{3,2},{4,5},{5,4},{6,7},{7,6},{8,9},{9,8},{10,11... | collective-permute-start | bytes 394760 | tf_op jit(solution)/shard_map/ppermute | solution.py:23
  115.5 25.6 %all-to-all-start.4 = ((bf16[64,32,128]{2,1,0:T(8,128)(2,1)}), bf16[64,32,128]{2,1,0:T(8,128)(2,1)S(1)}, u32[]{:S(2)}, u32[]{:S(2)}) async-start(bf16[64,32,128]{2,1,0:T(8,128)(2,1)} %bitcast.27), calls=%async_computation.4 | async-start | bytes 1048576 | tf_op jit(solution)/shard_map/all_to_all | solution.py:226

commit v11 on v10

--- a/solution.py
+++ b/solution.py
@@ -165,10 +165,9 @@
     second, third = first + hidden_local, first + 2 * hidden_local
     span = lent.shape[1] // 2
     lent_out = jnp.concatenate([lent[third:, :span], lent[third:, span:]], axis=0)
-    up_both = jnp.concatenate([own_up, lent[first:second]], axis=0)
     down_both = jnp.concatenate([own_down, lent[second:third]], axis=0)
-    lent_mix, own_mix, own_out, lent_out, up_both, down_both = lax.optimization_barrier(
-        (lent[:first], own_mix, own_out, lent_out, up_both, down_both)
+    lent_mix, lent_up, own_mix, own_up, own_out, lent_out, down_both = lax.optimization_barrier(
+        (lent[:first], lent[first:second], own_mix, own_up, own_out, lent_out, down_both)
     )
     sums = square_sums(token_half)
     high = sums.astype(jnp.bfloat16).astype(jnp.float32)
@@ -213,7 +212,9 @@
     residual = (tokens_t.astype(jnp.float32) + projected).astype(jnp.bfloat16)
 
     residual_half = gathered(residual).reshape(chips * share, rows)
-    partial = contracted(up_both, residual_half, (1, 0))
+    partial = jnp.concatenate(
+        [contracted(up, residual_half, (1, 0)) for up in (own_up, lent_up)], axis=0
+    )
     sums = square_sums(residual_half)
     arrived = swapped(jnp.concatenate([partial, sums], axis=0))
     upward = partial + jnp.concatenate(

time: 142 us -> 142 us (level)
  the two profiles are of different devices: /device:TPU:6 before, /device:TPU:4 now
where the time goes in v11:
time: 142 us; the launch traced here: 141 us
  blocking collectives  60.4 us (43%)
  waiting for transfers between devices  34.2 us (24%)
  starting transfers between devices  28.2 us (20%)
  local copies, waits for them, and re-layouts  6.02 us (4%)
  Pallas kernels  4.52 us (3%)
  other arithmetic  3.94 us (3%)
  matrix products  2.66 us (2%)
    all_to_all x2, blocking collectives, gathered(): lax.all_to_all(jnp.broadcast_to(x[None], (chips, *x.shape)), KV, 0, 0, ti...  42.4 us
    all_to_all x1, waiting for transfers between devices, per_device(): lax.all_to_all(terms.reshape(chips, share, rows), KV, split_axis=0, conca...  18.5 us
    all_to_all x1, blocking collectives, per_device(): lax.all_to_all(raw, ('tp', *KV), split_axis=0, concat_axis=0, tiled=True)  18.1 us
    all_to_all x1, starting transfers between devices, gathered(): lax.all_to_all(jnp.broadcast_to(x[None], (chips, *x.shape)), KV, 0, 0, ti...  16.6 us
    all_to_all x1, waiting for transfers between devices, gathered(): lax.all_to_all(jnp.broadcast_to(x[None], (chips, *x.shape)), KV, 0, 0, ti...  13.3 us
    all_to_all x1, starting transfers between devices, per_device(): lax.all_to_all(terms.reshape(chips, share, rows), KV, split_axis=0, conca...  5.83 us
    ppermute x3, starting transfers between devices, swapped(): return lax.ppermute(x, 'tp', [(0, 1), (1, 0)])  5.77 us
    pallas_call x1, Pallas kernels, split_weights(): pl.pallas_call(lambda *refs: split_kernel(share, *refs), out_shape=[jax.S...  4.52 us
  transfers between devices with their start and end apart: 5, of which 4 were waited for; matrix products, arithmetic and copies ran while one was open for 1% of the time, Pallas kernels for 3%

profile of v11, /device:TPU:4, one launch (start us, length us, event | category | flops | bytes accessed | tf_op | source)
XLA Modules:
  0.0 140.9 jit_solution(17809172734116867136)
XLA Ops:
  0.6 1.6 %broadcast_in_dim.34 = bf16[64,32,128]{2,1,0:T(8,128)(2,1)} broadcast(bf16[32,128]{1,0:T(8,128)(2,1)} %bitcast.83), dimensions={1,2} | broadcast | bytes 532480 | tf_op jit(solution)/shard_map/broadcast_in_dim | solution.py:28
  2.2 16.6 %all-to-all-start = ((bf16[64,32,128]{2,1,0:T(8,128)(2,1)}), bf16[64,32,128]{2,1,0:T(8,128)(2,1)S(1)}, u32[]{:S(2)}, u32[]{:S(2)}) async-start(bf16[64,32,128]{2,1,0:T(8,128)(2,1)} %broadcast_in_dim.34), calls=%async_computation | async-start | bytes 1048576 | tf_op jit(solution)/shard_map/all_to_all | solution.py:28
  18.8 4.5 %shard_map.140 = (bf16[64,2048]{1,0:T(8,128)(2,1)}, bf16[128,2048]{1,0:T(8,128)(2,1)}, bf16[128,2048]{1,0:T(8,128)(2,1)}, bf16[32,1024]{1,0:T(8,128)(2,1)}, bf16[336,2048]{1,0:T(8,128)(2,1)}) custom-call(s32[1]{0:T(128)} %bitcast.1.refs_0_, bf16[16,4096]{1,0:T(8,128)(2,1)} %bitcast.78, bf16[16,4096]{1,0:T(8,128)(2,1)} %bitcast.79, ...), custom_call_target="tpu_custom_call" | custom-call | tf_op jit(solution)/shard_map/pallas_call | solution.py:119
  23.3 1.9 %collective-permute-start = (bf16[336,2048]{1,0:T(8,128)(2,1)}, bf16[336,2048]{1,0:T(8,128)(2,1)S(1)}, u32[]{:S(2)}, u32[]{:S(2)}) collective-permute-start(bf16[336,2048]{1,0:T(8,128)(2,1)} %get-tuple-element.25), channel_id=1, source_target_pairs={{0,1},{1,0},{2,3},{3,2},{4,5},{5,4},{6,7},{7,6},{8,9},{9,8},{10,11... | collective-permute-start | bytes 4128776 | tf_op jit(solution)/shard_map/ppermute | solution.py:23
  25.3 13.3 %all-to-all-done = bf16[64,32,128]{2,1,0:T(8,128)(2,1)S(1)} async-done(((bf16[64,32,128]{2,1,0:T(8,128)(2,1)}), bf16[64,32,128]{2,1,0:T(8,128)(2,1)S(1)}, u32[]{:S(2)}, u32[]{:S(2)}) %all-to-all-start) | async-done | bytes 524320 | tf_op jit(solution)/shard_map/all_to_all | solution.py:28
  38.5 0.3 multiply_reduce_fusion.2
  38.8 0.1 select_convert_fusion.1
  38.9 0.0 collective-permute-done
  38.9 0.0 copy-start.1
  38.9 1.1 copy-done.1
  40.0 1.3 fusion.23
  41.3 0.0 slice-start
  41.3 0.0 copy-done.3
  41.3 0.0 copy-start.4
  41.3 0.1 pad_maximum_fusion
  41.4 0.8 slice-done
  42.2 0.2 fusion.27
  42.5 0.0 copy-done.4
  42.5 0.0 copy-start.7
  42.5 0.0 copy-start
  42.5 0.2 select_convert_fusion.2
  42.7 0.0 copy-start.8
  42.8 0.1 copy.32
  42.9 18.1 %all_to_all.25 = bf16[128,2,128]{2,1,0:T(2,128)(2,1)S(1)} all-to-all(bf16[128,2,128]{2,1,0:T(2,128)(2,1)S(1)} %bitcast.76), channel_id=1, replica_groups=mesh['dp'=4,'kv_0'=8,'kv_1'=8,'tp'=2] {'tp','kv_0','kv_1'}, dimensions={0} | all-to-all | bytes 131072 | tf_op jit(solution)/shard_map/all_to_all | solution.py:183
  61.0 0.1 convert_reduce_fusion.1
  61.0 0.2 slice_reduce_fusion
  61.2 0.1 copy_multiply_fusion
  61.3 0.1 copy.34
  61.4 0.1 copy.35
  61.5 0.1 squeeze.29
  61.6 0.1 copy.36
  61.7 0.1 squeeze.30
  61.7 0.1 copy.37
  61.8 0.1 squeeze.31
  61.9 0.1 copy.38
  62.0 0.1 squeeze.32
  62.1 0.0 copy-done.7
  62.1 0.0 copy-done
  62.1 0.0 copy-start.5
  62.1 0.0 copy-start.6
  62.2 0.3 multiply_reduce_fusion.1
  62.5 0.3 multiply_reduce_fusion.3
  62.9 0.1 fusion.15
  63.0 0.1 broadcast_in_dim.62
  63.1 18.9 %all_to_all.26 = bf16[64,2,1024]{2,1,0:T(2,128)(2,1)S(1)} all-to-all(bf16[64,2,1024]{2,1,0:T(2,128)(2,1)S(1)} %broadcast_in_dim.62), channel_id=1, replica_groups=mesh['dp'=4,'kv_0'=8,'kv_1'=8,'tp'=2] {'kv_0','kv_1'}, dimensions={0} | all-to-all | bytes 524288 | tf_op jit(solution)/shard_map/all_to_all | solution.py:28
  82.0 0.1 reshape.80
  82.1 0.2 fusion.28
  82.3 1.9 %collective-permute-start.1 = (f32[32,128]{1,0:T(8,128)S(1)}, f32[32,128]{1,0:T(8,128)S(1)}, u32[]{:S(2)}, u32[]{:S(2)}) collective-permute-start(f32[32,128]{1,0:T(8,128)S(1)} %fusion.28), channel_id=1, source_target_pairs={{0,1},{1,0},{2,3},{3,2},{4,5},{5,4},{6,7},{7,6},{8,9},{9,8},{10,11... | collective-permute-start | bytes 49160 | tf_op jit(solution)/shard_map/ppermute | solution.py:23
  84.3 1.1 collective-permute-done.1
  85.4 0.2 fusion.2
  85.6 0.0 copy-start.2
  85.6 0.1 broadcast_in_dim.63
  85.7 23.4 %all_to_all.27 = bf16[64,32,128]{2,1,0:T(8,128)(2,1)S(1)} all-to-all(bf16[64,32,128]{2,1,0:T(8,128)(2,1)S(1)} %broadcast_in_dim.63), channel_id=1, replica_groups=mesh['dp'=4,'kv_0'=8,'kv_1'=8,'tp'=2] {'kv_0','kv_1'}, dimensions={0} | all-to-all | bytes 1048576 | tf_op jit(solution)/shard_map/all_to_all | solution.py:28
  109.1 0.3 fusion.30
  109.5 0.3 fusion.29
  109.7 0.3 multiply_reduce_fusion
  110.0 1.9 %collective-permute-start.2 = (f32[257,128]{1,0:T(8,128)S(1)}, f32[257,128]{1,0:T(8,128)S(1)}, u32[]{:S(2)}, u32[]{:S(2)}) collective-permute-start(f32[257,128]{1,0:T(8,128)S(1)} %pad_maximum_fusion.1), channel_id=1, source_target_pairs={{0,1},{1,0},{2,3},{3,2},{4,5},{5,4},{6,7},{7,6},{8,9},{9,8},{10,11... | collective-permute-start | bytes 394760 | tf_op jit(solution)/shard_map/ppermute | solution.py:23
  112.0 1.3 collective-permute-done.2
  113.3 1.3 convolution_convert_fusion
  114.6 5.8 %all-to-all-start.4 = ((bf16[64,32,128]{2,1,0:T(8,128)(2,1)}), bf16[64,32,128]{2,1,0:T(8,128)(2,1)S(1)}, u32[]{:S(2)}, u32[]{:S(2)}) async-start(bf16[64,32,128]{2,1,0:T(8,128)(2,1)} %bitcast.27), calls=%async_computation.4 | async-start | bytes 1048576 | tf_op jit(solution)/shard_map/all_to_all | solution.py:227
  120.5 1.3 multiply_add_fusion
  121.8 18.5 %all-to-all-done.4 = bf16[64,32,128]{2,1,0:T(8,128)(2,1)S(1)} async-done(((bf16[64,32,128]{2,1,0:T(8,128)(2,1)}), bf16[64,32,128]{2,1,0:T(8,128)(2,1)S(1)}, u32[]{:S(2)}, u32[]{:S(2)}) %all-to-all-start.4) | async-done | bytes 524320 | tf_op jit(solution)/shard_map/all_to_all | solution.py:227
  140.2 0.1 convert_reduce_fusion
  140.3 0.6 fusion.14
  (21 shorter events, 0.1 us)
Async XLA Ops:
  2.2 36.3 %all-to-all-start = ((bf16[64,32,128]{2,1,0:T(8,128)(2,1)}), bf16[64,32,128]{2,1,0:T(8,128)(2,1)S(1)}, u32[]{:S(2)}, u32[]{:S(2)}) async-start(bf16[64,32,128]{2,1,0:T(8,128)(2,1)} %broadcast_in_dim.34), calls=%async_computation | async-start | bytes 1048576 | tf_op jit(solution)/shard_map/all_to_all | solution.py:28
  23.3 15.6 %collective-permute-start = (bf16[336,2048]{1,0:T(8,128)(2,1)}, bf16[336,2048]{1,0:T(8,128)(2,1)S(1)}, u32[]{:S(2)}, u32[]{:S(2)}) collective-permute-start(bf16[336,2048]{1,0:T(8,128)(2,1)} %get-tuple-element.25), channel_id=1, source_target_pairs={{0,1},{1,0},{2,3},{3,2},{4,5},{5,4},{6,7},{7,6},{8,9},{9,8},{10,11... | collective-permute-start | bytes 4128776 | tf_op jit(solution)/shard_map/ppermute | solution.py:23
  38.5 2.8 %copy-start.3 = (bf16[128,2048]{1,0:T(8,128)(2,1)S(1)}, bf16[128,2048]{1,0:T(8,128)(2,1)}, u32[]{:S(2)}) copy-start(bf16[128,2048]{1,0:T(8,128)(2,1)} %get-tuple-element.29) | copy-start | bytes 1572868
  38.9 1.1 copy-start.1
  41.3 1.0 slice-start
  41.3 1.2 copy-start.4
  42.5 19.6 %copy-start.7 = (f32[1024]{0:T(1024)S(1)}, f32[1024]{0:T(1024)}, u32[]{:S(2)}) copy-start(f32[1024]{0:T(1024)} %param.18) | copy-start | bytes 12292
  42.5 19.6 %copy-start = (f32[2,8,128,128]{3,2,1,0:T(8,128)S(1)}, f32[2,8,128,128]{3,2,1,0:T(8,128)}, u32[]{:S(2)}) copy-start(f32[2,8,128,128]{3,2,1,0:T(8,128)} %param.25) | copy-start | bytes 3145732
  42.7 20.1 %copy-start.8 = (f32[128]{0:T(128)S(1)}, f32[128]{0:T(128)}, u32[]{:S(2)}) copy-start(f32[128]{0:T(128)} %param.19) | copy-start | bytes 1540
  62.1 23.3 %copy-start.5 = (bf16[32,1024]{1,0:T(8,128)(2,1)S(1)}, bf16[32,1024]{1,0:T(8,128)(2,1)}, u32[]{:S(2)}) copy-start(bf16[32,1024]{1,0:T(8,128)(2,1)} %get-tuple-element.30) | copy-start | bytes 196612
  62.1 23.3 %copy-start.6 = (bf16[128,32]{0,1:T(8,128)(2,1)S(1)}, bf16[128,32]{0,1:T(8,128)(2,1)}, u32[]{:S(2)}) copy-start(bf16[128,32]{0,1:T(8,128)(2,1)} %param.13) | copy-start | bytes 24580
  82.3 3.1 %collective-permute-start.1 = (f32[32,128]{1,0:T(8,128)S(1)}, f32[32,128]{1,0:T(8,128)S(1)}, u32[]{:S(2)}, u32[]{:S(2)}) collective-permute-start(f32[32,128]{1,0:T(8,128)S(1)} %fusion.28), channel_id=1, source_target_pairs={{0,1},{1,0},{2,3},{3,2},{4,5},{5,4},{6,7},{7,6},{8,9},{9,8},{10,11... | collective-permute-start | bytes 49160 | tf_op jit(solution)/shard_map/ppermute | solution.py:23
  85.6 23.9 %copy-start.2 = (bf16[128,2048]{1,0:T(8,128)(2,1)S(1)}, bf16[128,2048]{1,0:T(8,128)(2,1)}, u32[]{:S(2)}) copy-start(bf16[128,2048]{1,0:T(8,128)(2,1)} %get-tuple-element.43) | copy-start | bytes 1572868
  110.0 3.2 %collective-permute-start.2 = (f32[257,128]{1,0:T(8,128)S(1)}, f32[257,128]{1,0:T(8,128)S(1)}, u32[]{:S(2)}, u32[]{:S(2)}) collective-permute-start(f32[257,128]{1,0:T(8,128)S(1)} %pad_maximum_fusion.1), channel_id=1, source_target_pairs={{0,1},{1,0},{2,3},{3,2},{4,5},{5,4},{6,7},{7,6},{8,9},{9,8},{10,11... | collective-permute-start | bytes 394760 | tf_op jit(solution)/shard_map/ppermute | solution.py:23
  114.6 25.6 %all-to-all-start.4 = ((bf16[64,32,128]{2,1,0:T(8,128)(2,1)}), bf16[64,32,128]{2,1,0:T(8,128)(2,1)S(1)}, u32[]{:S(2)}, u32[]{:S(2)}) async-start(bf16[64,32,128]{2,1,0:T(8,128)(2,1)} %bitcast.27), calls=%async_computation.4 | async-start | bytes 1048576 | tf_op jit(solution)/shard_map/all_to_all | solution.py:227

commit v12 on v11

--- a/solution.py
+++ b/solution.py
@@ -66,6 +66,8 @@
     own_down_ref,
     own_out_ref,
     other_ref,
+    other_up_ref,
+    other_down_ref,
 ):
     core = core_ref[0]
     half = CHUNK // 2
@@ -93,13 +95,15 @@
                 own_up_ref[:, target] = picked[first:second]
                 own_down_ref[:, target] = picked[second:]
             else:
-                other_ref[: second + hidden, target] = picked
+                other_ref[:first, target] = picked[:first]
+                other_up_ref[:, target] = picked[first:second]
+                other_down_ref[:, target] = picked[second:]
         start = pl.multiple_of(index * span, span)
         if own:
             own_out_ref[...] = out_ref[:, pl.ds(start, span)]
         else:
             for piece in range(2):
-                other_ref[second + hidden :, pl.ds(piece * span, span)] = out_ref[
+                other_ref[first:, pl.ds(piece * span, span)] = out_ref[
                     pl.ds(piece * lines, lines), pl.ds(start, span)
                 ]
 
@@ -114,7 +118,9 @@
         (hidden, width),
         (hidden, width),
         (lines, operands[4].shape[1] // 2),
-        (4 * columns + 2 * hidden + lines // 2, width),
+        (4 * columns + lines // 2, width),
+        (hidden, width),
+        (hidden, width),
     )
     return pl.pallas_call(
         lambda *refs: split_kernel(share, *refs),
@@ -151,7 +157,7 @@
     tp = lax.axis_index("tp")
 
     token_half = gathered(tokens_t).reshape(chips * share, rows)
-    own_mix, own_up, own_down, own_out, other = split_weights(
+    own_mix, own_up, own_down, own_out, other, other_up, other_down = split_weights(
         share,
         *[w[:, 0, :].T for w in (w_query, w_forget, w_input, w_output_gate)],
         w_out.T,
@@ -162,13 +168,12 @@
     )
     lent = swapped(other)
     first = 4 * columns
-    second, third = first + hidden_local, first + 2 * hidden_local
     span = lent.shape[1] // 2
-    lent_out = jnp.concatenate([lent[third:, :span], lent[third:, span:]], axis=0)
-    down_both = jnp.concatenate([own_down, lent[second:third]], axis=0)
-    lent_mix, lent_up, own_mix, own_up, own_out, lent_out, down_both = lax.optimization_barrier(
-        (lent[:first], lent[first:second], own_mix, own_up, own_out, lent_out, down_both)
-    )
+    lent_out = jnp.concatenate([lent[first:, :span], lent[first:, span:]], axis=0)
+    lent_mix, own_mix, own_out, lent_out = lax.optimization_barrier(
+        (lent[:first], own_mix, own_out, lent_out)
+    )
+    lent_up, lent_down = swapped(other_up), swapped(other_down)
     sums = square_sums(token_half)
     high = sums.astype(jnp.bfloat16).astype(jnp.float32)
     place = lax.broadcasted_iota(jnp.int32, (128 - 4 * columns, rows), 0)
@@ -223,6 +228,7 @@
     scale = lax.rsqrt((sums + arrived[-1:]) / width + EPSILON)
     hidden = jnp.square(jax.nn.relu(upward * scale)).astype(jnp.bfloat16)
 
+    down_both = jnp.concatenate([own_down, lent_down], axis=0)
     terms = contracted(down_both, hidden, (0, 0)).astype(jnp.bfloat16)
     terms = lax.all_to_all(
         terms.reshape(chips, share, rows), KV, split_axis=0, concat_axis=0, tiled=True

time: 142 us -> 143 us (level)
  the two profiles are of different devices: /device:TPU:4 before, /device:TPU:12 now
where the time goes in v12:
time: 143 us; the launch traced here: 142 us
  waiting for transfers between devices  52 us (36%)
  starting transfers between devices  37.5 us (26%)
  blocking collectives  36.9 us (26%)
  Pallas kernels  4.45 us (3%)
  other arithmetic  3.86 us (3%)
  local copies, waits for them, and re-layouts  3.68 us (3%)
  matrix products  2.64 us (2%)
    all_to_all x2, waiting for transfers between devices, gathered(): lax.all_to_all(jnp.broadcast_to(x[None], (chips, *x.shape)), KV, 0, 0, ti...  29.1 us
    all_to_all x2, starting transfers between devices, gathered(): lax.all_to_all(jnp.broadcast_to(x[None], (chips, *x.shape)), KV, 0, 0, ti...  21.7 us
    all_to_all x1, blocking collectives, gathered(): lax.all_to_all(jnp.broadcast_to(x[None], (chips, *x.shape)), KV, 0, 0, ti...  19.3 us
    all_to_all x1, waiting for transfers between devices, per_device(): lax.all_to_all(terms.reshape(chips, share, rows), KV, split_axis=0, conca...  18.4 us
    all_to_all x1, blocking collectives, per_device(): lax.all_to_all(raw, ('tp', *KV), split_axis=0, concat_axis=0, tiled=True)  17.5 us
    ppermute x5, starting transfers between devices, swapped(): return lax.ppermute(x, 'tp', [(0, 1), (1, 0)])  10.2 us
    all_to_all x1, starting transfers between devices, per_device(): lax.all_to_all(terms.reshape(chips, share, rows), KV, split_axis=0, conca...  5.54 us
    pallas_call x1, Pallas kernels, split_weights(): pl.pallas_call(lambda *refs: split_kernel(share, *refs), out_shape=[jax.S...  4.45 us
  transfers between devices with their start and end apart: 8, of which 6 were waited for; matrix products, arithmetic and copies ran while one was open for 1% of the time, Pallas kernels for 3%

profile of v12, /device:TPU:12, one launch (start us, length us, event | category | flops | bytes accessed | tf_op | source)
XLA Modules:
  0.0 141.9 jit_solution(8413522917910697763)
XLA Ops:
  0.6 1.6 %broadcast_in_dim.34 = bf16[64,32,128]{2,1,0:T(8,128)(2,1)} broadcast(bf16[32,128]{1,0:T(8,128)(2,1)} %bitcast.82), dimensions={1,2} | broadcast | bytes 532480 | tf_op jit(solution)/shard_map/broadcast_in_dim | solution.py:28
  2.2 16.6 %all-to-all-start = ((bf16[64,32,128]{2,1,0:T(8,128)(2,1)}), bf16[64,32,128]{2,1,0:T(8,128)(2,1)S(1)}, u32[]{:S(2)}, u32[]{:S(2)}) async-start(bf16[64,32,128]{2,1,0:T(8,128)(2,1)} %broadcast_in_dim.34), calls=%async_computation | async-start | bytes 1048576 | tf_op jit(solution)/shard_map/all_to_all | solution.py:28
  18.8 4.4 %shard_map.140 = (bf16[64,2048]{1,0:T(8,128)(2,1)}, bf16[128,2048]{1,0:T(8,128)(2,1)}, bf16[128,2048]{1,0:T(8,128)(2,1)}, bf16[32,1024]{1,0:T(8,128)(2,1)}, bf16...) custom-call(s32[1]{0:T(128)} %bitcast.1.refs_0_, bf16[16,4096]{1,0:T(8,128)(2,1)} %bitcast.77, ...), custom_call_target="tpu_custom_call" | custom-call | tf_op jit(solution)/shard_map/pallas_call | solution.py:125
  23.2 1.9 %collective-permute-start = (bf16[80,2048]{1,0:T(8,128)(2,1)}, bf16[80,2048]{1,0:T(8,128)(2,1)S(1)}, u32[]{:S(2)}, u32[]{:S(2)}) collective-permute-start(bf16[80,2048]{1,0:T(8,128)(2,1)} %get-tuple-element.24), channel_id=1, source_target_pairs={{0,1},{1,0},{2,3},{3,2},{4,5},{5,4},{6,7},{7,6},{8,9},{9,8},{10,11... | collective-permute-start | bytes 983048 | tf_op jit(solution)/shard_map/ppermute | solution.py:23
  25.2 0.0 copy-start.2
  25.2 1.8 %collective-permute-done = bf16[80,2048]{1,0:T(8,128)(2,1)S(1)} collective-permute-done((bf16[80,2048]{1,0:T(8,128)(2,1)}, bf16[80,2048]{1,0:T(8,128)(2,1)S(1)}, u32[]{:S(2)}, u32[]{:S(2)}) %collective-permute-start) | collective-permute-done | bytes 327712 | tf_op jit(solution)/shard_map/ppermute | solution.py:23
  27.0 11.2 %all-to-all-done = bf16[64,32,128]{2,1,0:T(8,128)(2,1)S(1)} async-done(((bf16[64,32,128]{2,1,0:T(8,128)(2,1)}), bf16[64,32,128]{2,1,0:T(8,128)(2,1)S(1)}, u32[]{:S(2)}, u32[]{:S(2)}) %all-to-all-start) | async-done | bytes 524320 | tf_op jit(solution)/shard_map/all_to_all | solution.py:28
  38.2 0.3 multiply_reduce_fusion.2
  38.5 0.2 fusion.30
  38.7 0.0 copy-done.2
  38.7 0.0 copy-start.5
  38.7 0.2 select_convert_fusion.2
  39.0 0.0 copy-start
  39.0 0.1 select_convert_fusion.1
  39.1 0.1 copy.32
  39.2 17.5 %all_to_all.25 = bf16[128,2,128]{2,1,0:T(2,128)(2,1)S(1)} all-to-all(bf16[128,2,128]{2,1,0:T(2,128)(2,1)S(1)} %bitcast.75), channel_id=1, replica_groups=mesh['dp'=4,'kv_0'=8,'kv_1'=8,'tp'=2] {'tp','kv_0','kv_1'}, dimensions={0} | all-to-all | bytes 131072 | tf_op jit(solution)/shard_map/all_to_all | solution.py:188
  56.8 0.1 convert_reduce_fusion.1
  56.8 0.2 slice_reduce_fusion
  57.0 0.1 copy_multiply_fusion
  57.1 0.1 copy.34
  57.2 0.0 copy-done.5
  57.2 0.1 copy.38
  57.3 0.1 squeeze.32
  57.4 0.1 copy.37
  57.5 0.1 squeeze.31
  57.6 0.1 copy.36
  57.7 0.1 squeeze.30
  57.7 0.1 copy.35
  57.8 0.1 squeeze.29
  57.9 0.0 copy-done
  57.9 0.3 multiply_reduce_fusion.1
  58.3 0.0 copy-start.4
  58.3 0.3 multiply_reduce_fusion.3
  58.7 0.1 fusion.18
  58.8 0.1 broadcast_in_dim.62
  58.9 19.3 %all_to_all.26 = bf16[64,2,1024]{2,1,0:T(2,128)(2,1)S(1)} all-to-all(bf16[64,2,1024]{2,1,0:T(2,128)(2,1)S(1)} %broadcast_in_dim.62), channel_id=1, replica_groups=mesh['dp'=4,'kv_0'=8,'kv_1'=8,'tp'=2] {'kv_0','kv_1'}, dimensions={0} | all-to-all | bytes 524288 | tf_op jit(solution)/shard_map/all_to_all | solution.py:28
  78.2 0.1 reshape.80
  78.3 0.2 fusion.31
  78.5 2.1 %collective-permute-start.1 = (f32[32,128]{1,0:T(8,128)S(1)}, f32[32,128]{1,0:T(8,128)S(1)}, u32[]{:S(2)}, u32[]{:S(2)}) collective-permute-start(f32[32,128]{1,0:T(8,128)S(1)} %fusion.31), channel_id=1, source_target_pairs={{0,1},{1,0},{2,3},{3,2},{4,5},{5,4},{6,7},{7,6},{8,9},{9,8},{10,11... | collective-permute-start | bytes 49160 | tf_op jit(solution)/shard_map/ppermute | solution.py:23
  80.6 1.1 collective-permute-done.1
  81.7 0.0 copy-done.3
  81.7 0.2 fusion.2
  81.9 0.0 copy-start.1
  81.9 0.9 broadcast_in_dim.63
  82.8 5.1 %all-to-all-start.3 = ((bf16[64,32,128]{2,1,0:T(8,128)(2,1)}), bf16[64,32,128]{2,1,0:T(8,128)(2,1)S(1)}, u32[]{:S(2)}, u32[]{:S(2)}) async-start(bf16[64,32,128]{2,1,0:T(8,128)(2,1)} %broadcast_in_dim.63), calls=%async_computation.3 | async-start | bytes 1048576 | tf_op jit(solution)/shard_map/all_to_all | solution.py:28
  87.9 1.9 %collective-permute-start.3 = (bf16[128,2048]{1,0:T(8,128)(2,1)S(1)}, bf16[128,2048]{1,0:T(8,128)(2,1)S(1)}, u32[]{:S(2)}, u32[]{:S(2)}) collective-permute-start(bf16[128,2048]{1,0:T(8,128)(2,1)S(1)} %copy-done.9), channel_id=1, source_target_pairs={{0,1},{1,0},{2,3},{3,2},{4,5},{5,4},{6,7},{7,6},{8,9},{9,8},{10,11... | collective-permute-start | bytes 1572872 | tf_op jit(solution)/shard_map/ppermute | solution.py:23
  89.9 18.0 %all-to-all-done.3 = bf16[64,32,128]{2,1,0:T(8,128)(2,1)S(1)} async-done(((bf16[64,32,128]{2,1,0:T(8,128)(2,1)}), bf16[64,32,128]{2,1,0:T(8,128)(2,1)S(1)}, u32[]{:S(2)}, u32[]{:S(2)}) %all-to-all-start.3) | async-done | bytes 524320 | tf_op jit(solution)/shard_map/all_to_all | solution.py:28
  107.8 0.3 multiply_reduce_fusion
  108.1 0.0 copy-done.1
  108.1 0.3 fusion.32
  108.4 0.0 copy-start.7
  108.4 0.0 collective-permute-done.3
  108.4 0.3 fusion.33
  108.7 1.9 %collective-permute-start.4 = (f32[257,128]{1,0:T(8,128)S(1)}, f32[257,128]{1,0:T(8,128)S(1)}, u32[]{:S(2)}, u32[]{:S(2)}) collective-permute-start(f32[257,128]{1,0:T(8,128)S(1)} %pad_maximum_fusion), channel_id=1, source_target_pairs={{0,1},{1,0},{2,3},{3,2},{4,5},{5,4},{6,7},{7,6},{8,9},{9,8},{10,11... | collective-permute-start | bytes 394760 | tf_op jit(solution)/shard_map/ppermute | solution.py:23
  110.7 0.0 copy-done.8
  110.7 2.4 %collective-permute-start.2 = (bf16[128,2048]{1,0:T(8,128)(2,1)S(1)}, bf16[128,2048]{1,0:T(8,128)(2,1)S(1)}, u32[]{:S(2)}, u32[]{:S(2)}) collective-permute-start(bf16[128,2048]{1,0:T(8,128)(2,1)S(1)} %copy-done.8), channel_id=1, source_target_pairs={{0,1},{1,0},{2,3},{3,2},{4,5},{5,4},{6,7},{7,6},{8,9},{9,8},{10,11... | collective-permute-start | bytes 1572872 | tf_op jit(solution)/shard_map/ppermute | solution.py:23
  113.1 0.0 collective-permute-done.4
  113.1 1.5 %collective-permute-done.2 = bf16[128,2048]{1,0:T(8,128)(2,1)S(1)} collective-permute-done((bf16[128,2048]{1,0:T(8,128)(2,1)S(1)}, bf16[128,2048]{1,0:T(8,128)(2,1)S(1)}, u32[]{:S(2)}, u32[]{:S(2)}) %collective-permute-start.2) | collective-permute-done | bytes 524320 | tf_op jit(solution)/shard_map/ppermute | solution.py:23
  114.6 1.3 convolution_convert_fusion
  115.9 5.5 %all-to-all-start.4 = ((bf16[64,32,128]{2,1,0:T(8,128)(2,1)}), bf16[64,32,128]{2,1,0:T(8,128)(2,1)S(1)}, u32[]{:S(2)}, u32[]{:S(2)}) async-start(bf16[64,32,128]{2,1,0:T(8,128)(2,1)} %bitcast.27), calls=%async_computation.4 | async-start | bytes 1048576 | tf_op jit(solution)/shard_map/all_to_all | solution.py:233
  121.5 1.3 multiply_add_fusion
  122.8 18.4 %all-to-all-done.4 = bf16[64,32,128]{2,1,0:T(8,128)(2,1)S(1)} async-done(((bf16[64,32,128]{2,1,0:T(8,128)(2,1)}), bf16[64,32,128]{2,1,0:T(8,128)(2,1)S(1)}, u32[]{:S(2)}, u32[]{:S(2)}) %all-to-all-start.4) | async-done | bytes 524320 | tf_op jit(solution)/shard_map/all_to_all | solution.py:233
  141.2 0.1 convert_reduce_fusion
  141.3 0.6 fusion.17
  (25 shorter events, 0.2 us)
Async XLA Ops:
  2.2 36.0 %all-to-all-start = ((bf16[64,32,128]{2,1,0:T(8,128)(2,1)}), bf16[64,32,128]{2,1,0:T(8,128)(2,1)S(1)}, u32[]{:S(2)}, u32[]{:S(2)}) async-start(bf16[64,32,128]{2,1,0:T(8,128)(2,1)} %broadcast_in_dim.34), calls=%async_computation | async-start | bytes 1048576 | tf_op jit(solution)/shard_map/all_to_all | solution.py:28
  23.2 3.7 %collective-permute-start = (bf16[80,2048]{1,0:T(8,128)(2,1)}, bf16[80,2048]{1,0:T(8,128)(2,1)S(1)}, u32[]{:S(2)}, u32[]{:S(2)}) collective-permute-start(bf16[80,2048]{1,0:T(8,128)(2,1)} %get-tuple-element.24), channel_id=1, source_target_pairs={{0,1},{1,0},{2,3},{3,2},{4,5},{5,4},{6,7},{7,6},{8,9},{9,8},{10,11... | collective-permute-start | bytes 983048 | tf_op jit(solution)/shard_map/ppermute | solution.py:23
  25.2 13.5 %copy-start.2 = (bf16[64,2048]{1,0:T(8,128)(2,1)S(1)}, bf16[64,2048]{1,0:T(8,128)(2,1)}, u32[]{:S(2)}) copy-start(bf16[64,2048]{1,0:T(8,128)(2,1)} %get-tuple-element.28) | copy-start | bytes 786436
  38.7 18.5 %copy-start.5 = (f32[1024]{0:T(1024)S(1)}, f32[1024]{0:T(1024)}, u32[]{:S(2)}) copy-start(f32[1024]{0:T(1024)} %param.18) | copy-start | bytes 12292
  39.0 19.0 %copy-start = (f32[2,8,128,128]{3,2,1,0:T(8,128)S(1)}, f32[2,8,128,128]{3,2,1,0:T(8,128)}, u32[]{:S(2)}) copy-start(f32[2,8,128,128]{3,2,1,0:T(8,128)} %param.25) | copy-start | bytes 3145732
  57.1 1.6 %copy-start.6 = (f32[128]{0:T(128)S(1)}, f32[128]{0:T(128)}, u32[]{:S(2)}) copy-start(f32[128]{0:T(128)} %param.19) | copy-start | bytes 1540
  58.3 23.4 %copy-start.3 = (bf16[32,1024]{1,0:T(8,128)(2,1)S(1)}, bf16[32,1024]{1,0:T(8,128)(2,1)}, u32[]{:S(2)}) copy-start(bf16[32,1024]{1,0:T(8,128)(2,1)} %get-tuple-element.27) | copy-start | bytes 196612
  58.3 23.4 %copy-start.4 = (bf16[128,32]{0,1:T(8,128)(2,1)S(1)}, bf16[128,32]{0,1:T(8,128)(2,1)}, u32[]{:S(2)}) copy-start(bf16[128,32]{0,1:T(8,128)(2,1)} %param.13) | copy-start | bytes 24580
  78.5 9.4 %copy-start.9 = (bf16[128,2048]{1,0:T(8,128)(2,1)S(1)}, bf16[128,2048]{1,0:T(8,128)(2,1)}, u32[]{:S(2)}) copy-start(bf16[128,2048]{1,0:T(8,128)(2,1)} %get-tuple-element.42) | copy-start | bytes 1572868
  78.5 3.2 %collective-permute-start.1 = (f32[32,128]{1,0:T(8,128)S(1)}, f32[32,128]{1,0:T(8,128)S(1)}, u32[]{:S(2)}, u32[]{:S(2)}) collective-permute-start(f32[32,128]{1,0:T(8,128)S(1)} %fusion.31), channel_id=1, source_target_pairs={{0,1},{1,0},{2,3},{3,2},{4,5},{5,4},{6,7},{7,6},{8,9},{9,8},{10,11... | collective-permute-start | bytes 49160 | tf_op jit(solution)/shard_map/ppermute | solution.py:23
  81.9 26.2 %copy-start.1 = (bf16[128,2048]{1,0:T(8,128)(2,1)S(1)}, bf16[128,2048]{1,0:T(8,128)(2,1)}, u32[]{:S(2)}) copy-start(bf16[128,2048]{1,0:T(8,128)(2,1)} %get-tuple-element.41) | copy-start | bytes 1572868
  82.8 25.0 %all-to-all-start.3 = ((bf16[64,32,128]{2,1,0:T(8,128)(2,1)}), bf16[64,32,128]{2,1,0:T(8,128)(2,1)S(1)}, u32[]{:S(2)}, u32[]{:S(2)}) async-start(bf16[64,32,128]{2,1,0:T(8,128)(2,1)} %broadcast_in_dim.63), calls=%async_computation.3 | async-start | bytes 1048576 | tf_op jit(solution)/shard_map/all_to_all | solution.py:28
  87.9 20.5 %collective-permute-start.3 = (bf16[128,2048]{1,0:T(8,128)(2,1)S(1)}, bf16[128,2048]{1,0:T(8,128)(2,1)S(1)}, u32[]{:S(2)}, u32[]{:S(2)}) collective-permute-start(bf16[128,2048]{1,0:T(8,128)(2,1)S(1)} %copy-done.9), channel_id=1, source_target_pairs={{0,1},{1,0},{2,3},{3,2},{4,5},{5,4},{6,7},{7,6},{8,9},{9,8},{10,11... | collective-permute-start | bytes 1572872 | tf_op jit(solution)/shard_map/ppermute | solution.py:23
  108.1 2.6 %copy-start.8 = (bf16[128,2048]{1,0:T(8,128)(2,1)S(1)}, bf16[128,2048]{1,0:T(8,128)(2,1)}, u32[]{:S(2)}) copy-start(bf16[128,2048]{1,0:T(8,128)(2,1)} %get-tuple-element.40) | copy-start | bytes 1572868
  108.4 6.2 %copy-start.7 = (bf16[128,2048]{1,0:T(8,128)(2,1)S(1)}, bf16[128,2048]{1,0:T(8,128)(2,1)}, u32[]{:S(2)}) copy-start(bf16[128,2048]{1,0:T(8,128)(2,1)} %get-tuple-element.39) | copy-start | bytes 1572868
  108.7 4.4 %collective-permute-start.4 = (f32[257,128]{1,0:T(8,128)S(1)}, f32[257,128]{1,0:T(8,128)S(1)}, u32[]{:S(2)}, u32[]{:S(2)}) collective-permute-start(f32[257,128]{1,0:T(8,128)S(1)} %pad_maximum_fusion), channel_id=1, source_target_pairs={{0,1},{1,0},{2,3},{3,2},{4,5},{5,4},{6,7},{7,6},{8,9},{9,8},{10,11... | collective-permute-start | bytes 394760 | tf_op jit(solution)/shard_map/ppermute | solution.py:23
  110.7 3.9 %collective-permute-start.2 = (bf16[128,2048]{1,0:T(8,128)(2,1)S(1)}, bf16[128,2048]{1,0:T(8,128)(2,1)S(1)}, u32[]{:S(2)}, u32[]{:S(2)}) collective-permute-start(bf16[128,2048]{1,0:T(8,128)(2,1)S(1)} %copy-done.8), channel_id=1, source_target_pairs={{0,1},{1,0},{2,3},{3,2},{4,5},{5,4},{6,7},{7,6},{8,9},{9,8},{10,11... | collective-permute-start | bytes 1572872 | tf_op jit(solution)/shard_map/ppermute | solution.py:23
  115.9 25.3 %all-to-all-start.4 = ((bf16[64,32,128]{2,1,0:T(8,128)(2,1)}), bf16[64,32,128]{2,1,0:T(8,128)(2,1)S(1)}, u32[]{:S(2)}, u32[]{:S(2)}) async-start(bf16[64,32,128]{2,1,0:T(8,128)(2,1)} %bitcast.27), calls=%async_computation.4 | async-start | bytes 1048576 | tf_op jit(solution)/shard_map/all_to_all | solution.py:233

commit v13 on v12

--- a/solution.py
+++ b/solution.py
@@ -188,12 +188,12 @@
     raw = lax.all_to_all(raw, ("tp", *KV), split_axis=0, concat_axis=0, tiled=True)
     raw, gate_floor, head_gain = lax.optimization_barrier((raw, gate_floor, head_gain))
     raw = raw.reshape(cores, chips, seq_local, 128).astype(jnp.float32).sum(axis=0)
-    sums = raw[0, :, 4 * columns : 4 * columns + 2].sum(axis=1)
+    sums = raw[:1, :, 4 * columns : 4 * columns + 1] + raw[:1, :, 4 * columns + 1 : 4 * columns + 2]
     scale = lax.rsqrt(sums / width + EPSILON)
-    raw = raw[:, :, : 4 * columns] * scale[None, :, None]
+    raw = raw[:, :, : 4 * columns] * scale
     raw = raw.reshape(chips, seq_local, 4, columns).transpose(2, 1, 0, 3)
     raw = raw.reshape(4, seq_local, heads_local, head_size)
-    raw = lax.optimization_barrier([raw[part] for part in range(4)])
+    raw = lax.optimization_barrier(raw)
     query_vec = raw[0] * head_size ** (-0.5)
     floor_heads = gate_floor.reshape(heads_local, head_size)
     forget_gate = floor_heads + (1.0 - floor_heads) * jax.nn.sigmoid(raw[1])

time: 143 us -> 142 us (level)
  the two profiles are of different devices: /device:TPU:12 before, /device:TPU:10 now
where the time goes in v13:
time: 142 us; the launch traced here: 141 us
  waiting for transfers between devices  52 us (37%)
  starting transfers between devices  37.5 us (26%)
  blocking collectives  36.7 us (26%)
  Pallas kernels  4.44 us (3%)
  other arithmetic  3.84 us (3%)
  local copies, waits for them, and re-layouts  3.23 us (2%)
  matrix products  2.63 us (2%)
    all_to_all x2, waiting for transfers between devices, gathered(): lax.all_to_all(jnp.broadcast_to(x[None], (chips, *x.shape)), KV, 0, 0, ti...  29.1 us
    all_to_all x2, starting transfers between devices, gathered(): lax.all_to_all(jnp.broadcast_to(x[None], (chips, *x.shape)), KV, 0, 0, ti...  21.7 us
    all_to_all x1, blocking collectives, gathered(): lax.all_to_all(jnp.broadcast_to(x[None], (chips, *x.shape)), KV, 0, 0, ti...  19.3 us
    all_to_all x1, waiting for transfers between devices, per_device(): lax.all_to_all(terms.reshape(chips, share, rows), KV, split_axis=0, conca...  18.4 us
    all_to_all x1, blocking collectives, per_device(): lax.all_to_all(raw, ('tp', *KV), split_axis=0, concat_axis=0, tiled=True)  17.4 us
    ppermute x5, starting transfers between devices, swapped(): return lax.ppermute(x, 'tp', [(0, 1), (1, 0)])  10.2 us
    all_to_all x1, starting transfers between devices, per_device(): lax.all_to_all(terms.reshape(chips, share, rows), KV, split_axis=0, conca...  5.55 us
    pallas_call x1, Pallas kernels, split_weights(): pl.pallas_call(lambda *refs: split_kernel(share, *refs), out_shape=[jax.S...  4.44 us
  transfers between devices with their start and end apart: 8, of which 6 were waited for; matrix products, arithmetic and copies ran while one was open for 1% of the time, Pallas kernels for 3%

profile of v13, /device:TPU:10, one launch (start us, length us, event | category | flops | bytes accessed | tf_op | source)
XLA Modules:
  0.0 141.3 jit_solution(1080500890584017342)
XLA Ops:
  0.6 1.6 %broadcast_in_dim.34 = bf16[64,32,128]{2,1,0:T(8,128)(2,1)} broadcast(bf16[32,128]{1,0:T(8,128)(2,1)} %bitcast.104), dimensions={1,2} | broadcast | bytes 532480 | tf_op jit(solution)/shard_map/broadcast_in_dim | solution.py:28
  2.2 16.6 %all-to-all-start = ((bf16[64,32,128]{2,1,0:T(8,128)(2,1)}), bf16[64,32,128]{2,1,0:T(8,128)(2,1)S(1)}, u32[]{:S(2)}, u32[]{:S(2)}) async-start(bf16[64,32,128]{2,1,0:T(8,128)(2,1)} %broadcast_in_dim.34), calls=%async_computation | async-start | bytes 1048576 | tf_op jit(solution)/shard_map/all_to_all | solution.py:28
  18.8 4.4 %shard_map.140 = (bf16[64,2048]{1,0:T(8,128)(2,1)}, bf16[128,2048]{1,0:T(8,128)(2,1)}, bf16[128,2048]{1,0:T(8,128)(2,1)}, bf16[32,1024]{1,0:T(8,128)(2,1)}, bf16...) custom-call(s32[1]{0:T(128)} %bitcast.1.refs_0_, bf16[16,4096]{1,0:T(8,128)(2,1)} %bitcast.99, ...), custom_call_target="tpu_custom_call" | custom-call | tf_op jit(solution)/shard_map/pallas_call | solution.py:125
  23.2 1.9 %collective-permute-start = (bf16[80,2048]{1,0:T(8,128)(2,1)}, bf16[80,2048]{1,0:T(8,128)(2,1)S(1)}, u32[]{:S(2)}, u32[]{:S(2)}) collective-permute-start(bf16[80,2048]{1,0:T(8,128)(2,1)} %get-tuple-element.20), channel_id=1, source_target_pairs={{0,1},{1,0},{2,3},{3,2},{4,5},{5,4},{6,7},{7,6},{8,9},{9,8},{10,11... | collective-permute-start | bytes 983048 | tf_op jit(solution)/shard_map/ppermute | solution.py:23
  25.1 0.0 copy-start.2
  25.2 1.8 %collective-permute-done = bf16[80,2048]{1,0:T(8,128)(2,1)S(1)} collective-permute-done((bf16[80,2048]{1,0:T(8,128)(2,1)}, bf16[80,2048]{1,0:T(8,128)(2,1)S(1)}, u32[]{:S(2)}, u32[]{:S(2)}) %collective-permute-start) | collective-permute-done | bytes 327712 | tf_op jit(solution)/shard_map/ppermute | solution.py:23
  27.0 11.2 %all-to-all-done = bf16[64,32,128]{2,1,0:T(8,128)(2,1)S(1)} async-done(((bf16[64,32,128]{2,1,0:T(8,128)(2,1)}), bf16[64,32,128]{2,1,0:T(8,128)(2,1)S(1)}, u32[]{:S(2)}, u32[]{:S(2)}) %all-to-all-start) | async-done | bytes 524320 | tf_op jit(solution)/shard_map/all_to_all | solution.py:28
  38.2 0.3 multiply_reduce_fusion.2
  38.5 0.2 fusion.42
  38.7 0.0 copy-done.2
  38.7 0.0 copy-start.5
  38.7 0.0 copy-start
  38.7 0.2 select_convert_fusion.2
  39.0 0.1 select_convert_fusion.1
  39.1 0.1 copy.27
  39.2 17.4 %all_to_all.25 = bf16[128,2,128]{2,1,0:T(2,128)(2,1)S(1)} all-to-all(bf16[128,2,128]{2,1,0:T(2,128)(2,1)S(1)} %bitcast.97), channel_id=1, replica_groups=mesh['dp'=4,'kv_0'=8,'kv_1'=8,'tp'=2] {'tp','kv_0','kv_1'}, dimensions={0} | all-to-all | bytes 131072 | tf_op jit(solution)/shard_map/all_to_all | solution.py:188
  56.6 0.1 convert_reduce_fusion.1
  56.7 0.0 copy-start.6
  56.7 0.2 fusion.31
  56.9 0.1 copy_multiply_fusion
  57.0 0.1 copy.29
  57.1 0.0 copy-done.5
  57.1 0.1 copy.30
  57.2 0.1 reshape.92
  57.4 0.0 copy-done
  57.4 0.3 multiply_reduce_fusion.1
  57.7 0.0 copy-start.3
  57.8 0.0 copy-start.4
  57.8 0.3 multiply_reduce_fusion.3
  58.1 0.0 copy-done.6
  58.1 0.1 fusion.26
  58.2 0.1 broadcast_in_dim.61
  58.4 19.3 %all_to_all.26 = bf16[64,2,1024]{2,1,0:T(2,128)(2,1)S(1)} all-to-all(bf16[64,2,1024]{2,1,0:T(2,128)(2,1)S(1)} %broadcast_in_dim.61), channel_id=1, replica_groups=mesh['dp'=4,'kv_0'=8,'kv_1'=8,'tp'=2] {'kv_0','kv_1'}, dimensions={0} | all-to-all | bytes 524288 | tf_op jit(solution)/shard_map/all_to_all | solution.py:28
  77.7 0.1 reshape.93
  77.8 0.2 fusion.43
  77.9 2.1 %collective-permute-start.1 = (f32[32,128]{1,0:T(8,128)S(1)}, f32[32,128]{1,0:T(8,128)S(1)}, u32[]{:S(2)}, u32[]{:S(2)}) collective-permute-start(f32[32,128]{1,0:T(8,128)S(1)} %fusion.43), channel_id=1, source_target_pairs={{0,1},{1,0},{2,3},{3,2},{4,5},{5,4},{6,7},{7,6},{8,9},{9,8},{10,11... | collective-permute-start | bytes 49160 | tf_op jit(solution)/shard_map/ppermute | solution.py:23
  80.0 1.1 collective-permute-done.1
  81.2 0.0 copy-done.3
  81.2 0.0 copy-done.4
  81.2 0.2 fusion.2
  81.4 0.0 copy-start.1
  81.4 0.9 broadcast_in_dim.62
  82.2 5.1 %all-to-all-start.3 = ((bf16[64,32,128]{2,1,0:T(8,128)(2,1)}), bf16[64,32,128]{2,1,0:T(8,128)(2,1)S(1)}, u32[]{:S(2)}, u32[]{:S(2)}) async-start(bf16[64,32,128]{2,1,0:T(8,128)(2,1)} %broadcast_in_dim.62), calls=%async_computation.3 | async-start | bytes 1048576 | tf_op jit(solution)/shard_map/all_to_all | solution.py:28
  87.4 0.0 copy-done.9
  87.4 1.9 %collective-permute-start.3 = (bf16[128,2048]{1,0:T(8,128)(2,1)S(1)}, bf16[128,2048]{1,0:T(8,128)(2,1)S(1)}, u32[]{:S(2)}, u32[]{:S(2)}) collective-permute-start(bf16[128,2048]{1,0:T(8,128)(2,1)S(1)} %copy-done.9), channel_id=1, source_target_pairs={{0,1},{1,0},{2,3},{3,2},{4,5},{5,4},{6,7},{7,6},{8,9},{9,8},{10,11... | collective-permute-start | bytes 1572872 | tf_op jit(solution)/shard_map/ppermute | solution.py:23
  89.3 18.0 %all-to-all-done.3 = bf16[64,32,128]{2,1,0:T(8,128)(2,1)S(1)} async-done(((bf16[64,32,128]{2,1,0:T(8,128)(2,1)}), bf16[64,32,128]{2,1,0:T(8,128)(2,1)S(1)}, u32[]{:S(2)}, u32[]{:S(2)}) %all-to-all-start.3) | async-done | bytes 524320 | tf_op jit(solution)/shard_map/all_to_all | solution.py:28
  107.3 0.3 multiply_reduce_fusion
  107.5 0.0 copy-done.1
  107.6 0.3 fusion.44
  107.8 0.0 copy-start.7
  107.9 0.0 collective-permute-done.3
  107.9 0.3 fusion.45
  108.2 1.9 %collective-permute-start.4 = (f32[257,128]{1,0:T(8,128)S(1)}, f32[257,128]{1,0:T(8,128)S(1)}, u32[]{:S(2)}, u32[]{:S(2)}) collective-permute-start(f32[257,128]{1,0:T(8,128)S(1)} %pad_maximum_fusion), channel_id=1, source_target_pairs={{0,1},{1,0},{2,3},{3,2},{4,5},{5,4},{6,7},{7,6},{8,9},{9,8},{10,11... | collective-permute-start | bytes 394760 | tf_op jit(solution)/shard_map/ppermute | solution.py:23
  110.1 0.0 copy-done.8
  110.1 2.4 %collective-permute-start.2 = (bf16[128,2048]{1,0:T(8,128)(2,1)S(1)}, bf16[128,2048]{1,0:T(8,128)(2,1)S(1)}, u32[]{:S(2)}, u32[]{:S(2)}) collective-permute-start(bf16[128,2048]{1,0:T(8,128)(2,1)S(1)} %copy-done.8), channel_id=1, source_target_pairs={{0,1},{1,0},{2,3},{3,2},{4,5},{5,4},{6,7},{7,6},{8,9},{9,8},{10,11... | collective-permute-start | bytes 1572872 | tf_op jit(solution)/shard_map/ppermute | solution.py:23
  112.5 0.0 collective-permute-done.4
  112.6 1.5 %collective-permute-done.2 = bf16[128,2048]{1,0:T(8,128)(2,1)S(1)} collective-permute-done((bf16[128,2048]{1,0:T(8,128)(2,1)S(1)}, bf16[128,2048]{1,0:T(8,128)(2,1)S(1)}, u32[]{:S(2)}, u32[]{:S(2)}) %collective-permute-start.2) | collective-permute-done | bytes 524320 | tf_op jit(solution)/shard_map/ppermute | solution.py:23
  114.0 0.0 copy-done.7
  114.0 1.3 convolution_convert_fusion
  115.3 5.5 %all-to-all-start.4 = ((bf16[64,32,128]{2,1,0:T(8,128)(2,1)}), bf16[64,32,128]{2,1,0:T(8,128)(2,1)S(1)}, u32[]{:S(2)}, u32[]{:S(2)}) async-start(bf16[64,32,128]{2,1,0:T(8,128)(2,1)} %bitcast.30), calls=%async_computation.4 | async-start | bytes 1048576 | tf_op jit(solution)/shard_map/all_to_all | solution.py:233
  120.9 1.3 multiply_add_fusion
  122.2 18.4 %all-to-all-done.4 = bf16[64,32,128]{2,1,0:T(8,128)(2,1)S(1)} async-done(((bf16[64,32,128]{2,1,0:T(8,128)(2,1)}), bf16[64,32,128]{2,1,0:T(8,128)(2,1)S(1)}, u32[]{:S(2)}, u32[]{:S(2)}) %all-to-all-start.4) | async-done | bytes 524320 | tf_op jit(solution)/shard_map/all_to_all | solution.py:233
  140.6 0.1 convert_reduce_fusion
  140.7 0.6 fusion.17
  (18 shorter events, 0.1 us)
Async XLA Ops:
  2.2 36.0 %all-to-all-start = ((bf16[64,32,128]{2,1,0:T(8,128)(2,1)}), bf16[64,32,128]{2,1,0:T(8,128)(2,1)S(1)}, u32[]{:S(2)}, u32[]{:S(2)}) async-start(bf16[64,32,128]{2,1,0:T(8,128)(2,1)} %broadcast_in_dim.34), calls=%async_computation | async-start | bytes 1048576 | tf_op jit(solution)/shard_map/all_to_all | solution.py:28
  23.2 3.7 %collective-permute-start = (bf16[80,2048]{1,0:T(8,128)(2,1)}, bf16[80,2048]{1,0:T(8,128)(2,1)S(1)}, u32[]{:S(2)}, u32[]{:S(2)}) collective-permute-start(bf16[80,2048]{1,0:T(8,128)(2,1)} %get-tuple-element.20), channel_id=1, source_target_pairs={{0,1},{1,0},{2,3},{3,2},{4,5},{5,4},{6,7},{7,6},{8,9},{9,8},{10,11... | collective-permute-start | bytes 983048 | tf_op jit(solution)/shard_map/ppermute | solution.py:23
  25.1 13.5 %copy-start.2 = (bf16[64,2048]{1,0:T(8,128)(2,1)S(1)}, bf16[64,2048]{1,0:T(8,128)(2,1)}, u32[]{:S(2)}) copy-start(bf16[64,2048]{1,0:T(8,128)(2,1)} %get-tuple-element.24) | copy-start | bytes 786436
  38.7 18.4 %copy-start.5 = (f32[1024]{0:T(1024)S(1)}, f32[1024]{0:T(1024)}, u32[]{:S(2)}) copy-start(f32[1024]{0:T(1024)} %param.18) | copy-start | bytes 12292
  38.7 18.7 %copy-start = (f32[2,8,128,128]{3,2,1,0:T(8,128)S(1)}, f32[2,8,128,128]{3,2,1,0:T(8,128)}, u32[]{:S(2)}) copy-start(f32[2,8,128,128]{3,2,1,0:T(8,128)} %param.25) | copy-start | bytes 3145732
  56.7 1.4 %copy-start.6 = (f32[128]{0:T(128)S(1)}, f32[128]{0:T(128)}, u32[]{:S(2)}) copy-start(f32[128]{0:T(128)} %param.19) | copy-start | bytes 1540
  57.7 23.4 %copy-start.3 = (bf16[32,1024]{1,0:T(8,128)(2,1)S(1)}, bf16[32,1024]{1,0:T(8,128)(2,1)}, u32[]{:S(2)}) copy-start(bf16[32,1024]{1,0:T(8,128)(2,1)} %get-tuple-element.23) | copy-start | bytes 196612
  57.8 23.4 %copy-start.4 = (bf16[128,32]{0,1:T(8,128)(2,1)S(1)}, bf16[128,32]{0,1:T(8,128)(2,1)}, u32[]{:S(2)}) copy-start(bf16[128,32]{0,1:T(8,128)(2,1)} %param.13) | copy-start | bytes 24580
  77.9 9.4 %copy-start.9 = (bf16[128,2048]{1,0:T(8,128)(2,1)S(1)}, bf16[128,2048]{1,0:T(8,128)(2,1)}, u32[]{:S(2)}) copy-start(bf16[128,2048]{1,0:T(8,128)(2,1)} %get-tuple-element.34) | copy-start | bytes 1572868
  77.9 3.2 %collective-permute-start.1 = (f32[32,128]{1,0:T(8,128)S(1)}, f32[32,128]{1,0:T(8,128)S(1)}, u32[]{:S(2)}, u32[]{:S(2)}) collective-permute-start(f32[32,128]{1,0:T(8,128)S(1)} %fusion.43), channel_id=1, source_target_pairs={{0,1},{1,0},{2,3},{3,2},{4,5},{5,4},{6,7},{7,6},{8,9},{9,8},{10,11... | collective-permute-start | bytes 49160 | tf_op jit(solution)/shard_map/ppermute | solution.py:23
  81.4 26.2 %copy-start.1 = (bf16[128,2048]{1,0:T(8,128)(2,1)S(1)}, bf16[128,2048]{1,0:T(8,128)(2,1)}, u32[]{:S(2)}) copy-start(bf16[128,2048]{1,0:T(8,128)(2,1)} %get-tuple-element.33) | copy-start | bytes 1572868
  82.2 25.0 %all-to-all-start.3 = ((bf16[64,32,128]{2,1,0:T(8,128)(2,1)}), bf16[64,32,128]{2,1,0:T(8,128)(2,1)S(1)}, u32[]{:S(2)}, u32[]{:S(2)}) async-start(bf16[64,32,128]{2,1,0:T(8,128)(2,1)} %broadcast_in_dim.62), calls=%async_computation.3 | async-start | bytes 1048576 | tf_op jit(solution)/shard_map/all_to_all | solution.py:28
  87.4 20.5 %collective-permute-start.3 = (bf16[128,2048]{1,0:T(8,128)(2,1)S(1)}, bf16[128,2048]{1,0:T(8,128)(2,1)S(1)}, u32[]{:S(2)}, u32[]{:S(2)}) collective-permute-start(bf16[128,2048]{1,0:T(8,128)(2,1)S(1)} %copy-done.9), channel_id=1, source_target_pairs={{0,1},{1,0},{2,3},{3,2},{4,5},{5,4},{6,7},{7,6},{8,9},{9,8},{10,11... | collective-permute-start | bytes 1572872 | tf_op jit(solution)/shard_map/ppermute | solution.py:23
  107.5 2.6 %copy-start.8 = (bf16[128,2048]{1,0:T(8,128)(2,1)S(1)}, bf16[128,2048]{1,0:T(8,128)(2,1)}, u32[]{:S(2)}) copy-start(bf16[128,2048]{1,0:T(8,128)(2,1)} %get-tuple-element.32) | copy-start | bytes 1572868
  107.8 6.2 %copy-start.7 = (bf16[128,2048]{1,0:T(8,128)(2,1)S(1)}, bf16[128,2048]{1,0:T(8,128)(2,1)}, u32[]{:S(2)}) copy-start(bf16[128,2048]{1,0:T(8,128)(2,1)} %get-tuple-element.31) | copy-start | bytes 1572868
  108.2 4.4 %collective-permute-start.4 = (f32[257,128]{1,0:T(8,128)S(1)}, f32[257,128]{1,0:T(8,128)S(1)}, u32[]{:S(2)}, u32[]{:S(2)}) collective-permute-start(f32[257,128]{1,0:T(8,128)S(1)} %pad_maximum_fusion), channel_id=1, source_target_pairs={{0,1},{1,0},{2,3},{3,2},{4,5},{5,4},{6,7},{7,6},{8,9},{9,8},{10,11... | collective-permute-start | bytes 394760 | tf_op jit(solution)/shard_map/ppermute | solution.py:23
  110.1 3.9 %collective-permute-start.2 = (bf16[128,2048]{1,0:T(8,128)(2,1)S(1)}, bf16[128,2048]{1,0:T(8,128)(2,1)S(1)}, u32[]{:S(2)}, u32[]{:S(2)}) collective-permute-start(bf16[128,2048]{1,0:T(8,128)(2,1)S(1)} %copy-done.8), channel_id=1, source_target_pairs={{0,1},{1,0},{2,3},{3,2},{4,5},{5,4},{6,7},{7,6},{8,9},{9,8},{10,11... | collective-permute-start | bytes 1572872 | tf_op jit(solution)/shard_map/ppermute | solution.py:23
  115.3 25.3 %all-to-all-start.4 = ((bf16[64,32,128]{2,1,0:T(8,128)(2,1)}), bf16[64,32,128]{2,1,0:T(8,128)(2,1)S(1)}, u32[]{:S(2)}, u32[]{:S(2)}) async-start(bf16[64,32,128]{2,1,0:T(8,128)(2,1)} %bitcast.30), calls=%async_computation.4 | async-start | bytes 1048576 | tf_op jit(solution)/shard_map/all_to_all | solution.py:233
